TPU v7x, 32 devices: a whole 2x2x4 slice. The times are simulated.
32 devices in a mesh: grp: 2 (over x), sp: 8 (over z, y), tp: 2 (over core).
Axes of the slice: x: 2, y: 2, z: 4, core: 2. Of those that a mesh axis runs over, the one named last changes fastest.
Arguments:
- tokens: bfloat16 [8192, 2048], P(('grp', 'sp', 'tp')), parts along dimension 0, may hold values from -60 to 60
- query_weight: bfloat16 [2048, 1024], P(None, 'tp'), may hold values from -0.125 to 0.125
- key_weight: bfloat16 [2048, 1024], P(None, 'tp'), may hold values from -0.125 to 0.125
- value_weight: bfloat16 [2048, 1024], P(None, 'tp'), may hold values from -0.125 to 0.125
- output_weight: bfloat16 [1024, 2048], P(None, 'tp'), may hold values from -1.5 to 1.5
Outputs:
- attended: bfloat16 [8192, 2048], P(('grp', 'sp'), 'tp'), parts along dimension 0
There are 2 independent parts, one for each index of `grp`. A program takes and returns all parts, laid end to end along the dimension named above; an argument that names none is the same for every part. Nothing has to cross between parts.
All inputs are finite; a program needn't handle non-finite values.
Results may differ from a plain program's by a relative error of at most 0.012.
The roundings to bfloat16 on the way count: a program that leaves them out, or rounds other values in their place, can miss the bound.
Values may be sent and summed in bfloat16 or wider, within the bound.
No kernel may reach another device: no remote copies, remote signals or barrier semaphores. Data moves between devices by JAX's collectives and lax.ppermute only.
A program may use at most 128 MiB of HBM per device.

v0:
```python
import functools

import jax
import jax.numpy as jnp
import numpy as np
from jax import lax
from jax.experimental import pallas as pl
from jax.experimental.pallas import tpu as pltpu
from jax.sharding import PartitionSpec as P

HEAD = 128
REACH_STEPS = 128
MIDDLE_DILATION = 4
FAR_DILATION = 16
THETA_BASE = 500000.0
TILE = 16
MASKED = -1e30
SCALE = HEAD ** -0.5 * 1.4426950408889634
F32 = jnp.float32
BF16 = jnp.bfloat16


def in_vmem(count):
    return [pl.BlockSpec(memory_space=pltpu.VMEM)] * count


def rotated(val, cos, sin):
    return val * cos + pltpu.roll(val, HEAD // 2, 1) * sin


def place(out_ref, lead, val, buf_ref, slot, first):
    nq_half = val.shape[0] // FAR_DILATION
    buf_ref[slot] = val
    for r in range(FAR_DILATION):
        piece = buf_ref[slot, pl.ds(r, nq_half, stride=FAR_DILATION), :]
        at = r * nq_half if first is None else pl.multiple_of((2 * r + first) * nq_half, TILE)
        out_ref[lead + (pl.ds(at, nq_half), slice(None))] = piece.astype(BF16)


def kv_half(x_ref, w_ref, keep_ref, send_ref, cos_ref, sin_ref, buf_ref, part, ready=None):
    cos, sin = cos_ref.at[part], sin_ref.at[part]
    slot = 0
    for side, out_ref in enumerate((keep_ref, send_ref)):
        for which in (1, 0):
            if ready is not None:
                ready(side, which)
            acc = jnp.dot(x_ref[...], w_ref[side, which], preferred_element_type=F32)
            for h in range(acc.shape[1] // HEAD):
                val = acc[:, h * HEAD:(h + 1) * HEAD]
                if which == 0:
                    val = rotated(val, cos[...], sin[...])
                place(out_ref, (h, which), val, buf_ref, slot, None)
                slot += 1


def own_kernel(sc_ref, x_hbm, wk_hbm, wv_hbm, inv_ref,
               keep_ref, send_ref, w_ref, cos_ref, sin_ref, x_ref, buf_ref, sems):
    tp, par, sp = sc_ref[0], sc_ref[1], sc_ref[3]
    half = x_ref.shape[0]
    width = w_ref.shape[3]
    copies = {}
    copies["x"] = pltpu.make_async_copy(x_hbm, x_ref, sems.at[0])
    copies["x"].start()
    for side in range(2):
        column = pl.multiple_of((par if side == 0 else 1 - par) * width, width)
        for which, hbm in ((1, wv_hbm), (0, wk_hbm)):
            copy = pltpu.make_async_copy(hbm.at[:, pl.ds(column, width)], w_ref.at[side, which],
                                         sems.at[1 + 2 * side + which])
            copy.start()
            copies[side, which] = copy
    steps = half // FAR_DILATION
    lane = lax.broadcasted_iota(jnp.int32, (2 * steps, HEAD), 1)
    row = lax.broadcasted_iota(jnp.int32, (2 * steps, HEAD), 0)
    part = jnp.where(row < steps, tp, 1 - tp)
    position = sp * (2 * half) + part * half + (row % steps) * FAR_DILATION
    coarse = position.astype(F32) * inv_ref[...]
    fine = lax.broadcasted_iota(jnp.int32, (FAR_DILATION, HEAD), 0).astype(F32) * inv_ref[...]
    cos_c, sin_c = jnp.cos(coarse)[:, None, :], jnp.sin(coarse)[:, None, :]
    cos_f, sin_f = jnp.cos(fine)[None], jnp.sin(fine)[None]
    sign = jnp.where(lane[:1] < HEAD // 2, -1.0, 1.0)[None]
    cos_ref[...] = (cos_c * cos_f - sin_c * sin_f).reshape(2, half, HEAD)
    sin_ref[...] = ((sin_c * cos_f + cos_c * sin_f) * sign).reshape(2, half, HEAD)
    copies["x"].wait()
    kv_half(x_ref, w_ref, keep_ref, send_ref, cos_ref, sin_ref, buf_ref, 0,
            lambda side, which: copies[side, which].wait())


def rest_kernel(sc_ref, x_ref, w_ref, cos_ref, sin_ref, keep_ref, send_ref, buf_ref):
    kv_half(x_ref, w_ref, keep_ref, send_ref, cos_ref, sin_ref, buf_ref, 1)


def q_kernel(sc_ref, xo_ref, xp_ref, cos_ref, sin_ref, w_ref, keepa_ref, keepb_ref, send_ref, buf_ref):
    tp, par = sc_ref[0], sc_ref[1]
    heads = send_ref.shape[0]
    width = heads * HEAD
    slot = 0
    for side in (1, 0):
        w = w_ref[:, pl.ds(pl.multiple_of((1 - par if side else par) * width, width), width)]
        for part, x_ref in enumerate((xo_ref, xp_ref)):
            acc = jnp.dot(x_ref[...], w, preferred_element_type=F32)
            for h in range(heads):
                val = rotated(acc[:, h * HEAD:(h + 1) * HEAD], cos_ref[part], sin_ref[part])
                if side:
                    place(send_ref, (h,), val, buf_ref, slot, tp if part == 0 else 1 - tp)
                else:
                    place((keepa_ref, keepb_ref)[part], (h,), val, buf_ref, slot, None)
                slot += 1


def call(kernel, scalars, inputs, outputs, scratch, flops, aliases={}, limit=28, hbm=()):
    spaces = [pltpu.HBM if i in hbm else pltpu.VMEM for i in range(len(inputs))]
    return pl.pallas_call(
        kernel,
        in_specs=[pl.BlockSpec(memory_space=pltpu.SMEM)] + [pl.BlockSpec(memory_space=m) for m in spaces],
        out_specs=in_vmem(len(outputs)),
        out_shape=outputs,
        scratch_shapes=scratch,
        input_output_aliases=aliases,
        compiler_params=pltpu.CompilerParams(vmem_limit_bytes=limit * 2 ** 20),
        cost_estimate=pl.CostEstimate(flops=flops, transcendentals=0, bytes_accessed=0),
    )(scalars, *[pltpu.with_memory_space_constraint(x, pltpu.HBM) if i in hbm else x for i, x in enumerate(inputs)])


def gather(dst_ref, nq, sources):
    for r in range(FAR_DILATION):
        for source, block, half in sources:
            rows = nq if half is None else nq // 2
            start = 0 if half is None else half * (nq // 2)
            at = pl.multiple_of(r * 2 * nq + block * nq + start, TILE)
            dst_ref[pl.ds(at, rows), :] = source[r * rows:(r + 1) * rows, :]


def gather_kv(k_ref, v_ref, refs, nq, tp, par):
    places = ((par, tp), (par, 1 - tp), (1 - par, tp), (1 - par, 1 - tp))
    for which, dst_ref in enumerate((k_ref, v_ref)):
        gather(dst_ref, nq, [(ref.at[which], block, half) for ref, (block, half) in zip(refs, places)])


def scores_of(q, k):
    return lax.dot_general(q, k, (((1,), (1,)), ((), ())), preferred_element_type=F32)


def take(ref, rows):
    parts = [ref[a:a + n, :] for a, n in rows]
    return parts[0] if len(parts) == 1 else jnp.concatenate(parts, axis=0)


def put(ref, rows, value):
    at = 0
    for a, n in rows:
        ref[a:a + n, :] = value[at:at + n]
        at += n


def widened(stat, columns):
    return jnp.concatenate([stat] * (columns // HEAD), axis=1) if columns > HEAD else stat


def scored(item, q_ref, k_ref, s_ref, m_ref, fresh):
    rows, keys, bias, at = item
    s = scores_of(take(q_ref, rows), take(k_ref, keys))
    if bias is not None:
        s = s + bias
    n, columns = s.shape
    s_ref[at:at + n, :columns] = s
    top = jnp.broadcast_to(jnp.max(s, axis=-1, keepdims=True), (n, HEAD))
    put(m_ref, rows, top if fresh else jnp.maximum(take(m_ref, rows), top))


def weighed(item, v_ref, s_ref, m_ref, columns):
    rows, keys, _, at = item
    n = sum(c for _, c in rows)
    p = jnp.exp2((s_ref[at:at + n, :columns] - widened(take(m_ref, rows), columns)) * SCALE).astype(BF16)
    v = take(v_ref, keys)
    return jnp.dot(p, jnp.concatenate([v, jnp.ones_like(v)], axis=1), preferred_element_type=F32)


def length(rows):
    return sum(n for _, n in rows)


def group_rows(r4, nq):
    return [((r4 + MIDDLE_DILATION * j) * 2 * nq, 2 * nq) for j in range(FAR_DILATION // MIDDLE_DILATION)]


def near_rows(c, nq):
    return [(r * 2 * nq + c * TILE, TILE) for r in range(FAR_DILATION)]


def pair_rows(i, nq):
    return [(i * 4 * nq, 4 * nq)]


def near_of(tq, tk):
    return (tq - tk >= 0) & (tq - tk <= REACH_STEPS)


def every(tq, tk, step):
    return (tq % step == tk % step) & (tq - tk >= 0) & (tq - tk <= REACH_STEPS * step)


def bias_of(count):
    return np.where(count > 0, np.log2(np.maximum(count, 1)) / SCALE, MASKED).astype(np.float32)


def biases(nq):
    group = 2 * nq * FAR_DILATION
    j = np.arange(FAR_DILATION // MIDDLE_DILATION)[:, None]
    t = (np.arange(2 * nq)[None, :] * FAR_DILATION + j * MIDDLE_DILATION).reshape(-1)
    tq, tk = t[:, None], t[None, :]
    both = lambda tq, tk: every(tq, tk, MIDDLE_DILATION).astype(int) + every(tq, tk, FAR_DILATION)
    group0, group1 = both(tq, tk), both(tq + group, tk)
    r = np.arange(FAR_DILATION)[:, None]
    t = (np.arange(TILE)[None, :] * FAR_DILATION + r).reshape(-1)
    tq, tk = t[:, None], t[None, :]
    near0, near1 = near_of(tq, tk), near_of(tq + TILE * FAR_DILATION, tk)
    r = np.arange(2)[:, None]
    t = (np.arange(2 * nq)[None, :] * FAR_DILATION + r).reshape(-1)
    pair2 = every(t[:, None] + 2 * group, t[None, :], FAR_DILATION)
    return [bias_of(np.asarray(x, int)) for x in (group0, group1, near0, near1, pair2)]


def local_kernel(sc_ref, qa_ref, qb_ref, qy_ref, kva_ref, kvb_ref, kvya_ref, kvyb_ref, group_ref, near0_ref, near1_ref,
                 q_ref, m_ref, l_ref, o_ref, k_s, v_s, s_s):
    tp, par = sc_ref[0], sc_ref[1]
    nq = qy_ref.shape[1] // FAR_DILATION
    for h in range(q_ref.shape[0]):
        q, m, l, o, k, v, sh = (x.at[h] for x in (q_ref, m_ref, l_ref, o_ref, k_s, v_s, s_s))
        gather(q, nq, [(qa_ref.at[h], par, tp), (qb_ref.at[h], par, 1 - tp), (qy_ref.at[h], 1 - par, None)])
        gather_kv(k, v, [x.at[h] for x in (kva_ref, kvb_ref, kvya_ref, kvyb_ref)], nq, tp, par)
        at = 0
        items = []
        for r4 in range(MIDDLE_DILATION):
            rows = group_rows(r4, nq)
            items.append((rows, rows, group_ref[...], at))
            scored(items[-1], q, k, sh, m, True)
            at += length(rows)
        for c in range(2 * nq // TILE):
            rows = near_rows(c, nq)
            keys, bias = rows, near0_ref[...]
            if c:
                keys = near_rows(c - 1, nq) + rows
                bias = jnp.concatenate([near1_ref[...], bias], axis=1)
            items.append((rows, keys, bias, at))
            scored(items[-1], q, k, sh, m, False)
            at += length(rows)
        for i, item in enumerate(items):
            ol = weighed(item, v, sh, m, length(item[1]))
            if i < MIDDLE_DILATION:
                put(o, item[0], ol[:, :HEAD])
                put(l, item[0], ol[:, HEAD:])
            else:
                put(o, item[0], take(o, item[0]) + ol[:, :HEAD])
                put(l, item[0], take(l, item[0]) + ol[:, HEAD:])


def one_kernel(sc_ref, q_ref, m_in, l_in, o_in, kva_ref, kvb_ref, kvya_ref, kvyb_ref, group_ref, near_ref,
               m_ref, l_ref, o_ref, k_s, v_s, s_s, n_s):
    tp, par = sc_ref[0], sc_ref[1]
    nq = kvya_ref.shape[2] // FAR_DILATION * 2

    @pl.when(sc_ref[2] >= 1)
    def _():
        for h in range(q_ref.shape[0]):
            q, mi, li, oi, m, l, o, k, v, sh, n = (x.at[h] for x in (
                q_ref, m_in, l_in, o_in, m_ref, l_ref, o_ref, k_s, v_s, s_s, n_s))
            gather_kv(k, v, [x.at[h] for x in (kva_ref, kvb_ref, kvya_ref, kvyb_ref)], nq, tp, par)
            near = (near_rows(0, nq), near_rows(2 * nq // TILE - 1, nq), near_ref[...], 0)
            at = length(near[0])
            items = []
            for r4 in range(MIDDLE_DILATION):
                rows = group_rows(r4, nq)
                items.append((rows, rows, group_ref[...], at))
                scored(items[-1], q, k, sh, n, True)
                at += length(rows)
            scored(near, q, k, sh, n, False)
            for item in items:
                rows = item[0]
                old = take(mi, rows)
                new = jnp.maximum(old, take(n, rows))
                keep = jnp.exp2((old - new) * SCALE)
                put(m, rows, new)
                ol = weighed(item, v, sh, m, length(item[1]))
                put(o, rows, take(oi, rows) * keep + ol[:, :HEAD])
                put(l, rows, take(li, rows) * keep + ol[:, HEAD:])
            ol = weighed(near, v, sh, m, length(near[1]))
            put(o, near[0], take(o, near[0]) + ol[:, :HEAD])
            put(l, near[0], take(l, near[0]) + ol[:, HEAD:])


def two_kernel(sc_ref, q_ref, m_ref, l_ref, o_ref, kva_ref, kvb_ref, kvy_ref, pair_ref,
               keep_ref, send_ref, k_s, v_s, s_s, n_s, mix_s, *, head):
    tp, par = sc_ref[0], sc_ref[1]
    nq = kvy_ref.shape[2] // FAR_DILATION * 2
    q, m, l, o = (x.at[head] for x in (q_ref, m_ref, l_ref, o_ref))
    pairs = [pair_rows(i, nq) for i in range(FAR_DILATION // 2)]

    def settle(i, val):
        for part in range(4):
            r, block = 2 * i + part // 2, part % 2
            mix_s[block, pl.ds(r, nq, stride=FAR_DILATION), :] = val[part * nq:(part + 1) * nq]

    @pl.when(sc_ref[2] >= 2)
    def _():
        gather_kv(k_s, v_s, [kva_ref.at[head], kvb_ref.at[head], kvy_ref.at[0], kvy_ref.at[1]], nq, tp, par)
        items = [(rows, rows, pair_ref[...], i * length(rows)) for i, rows in enumerate(pairs)]
        for item in items:
            put(n_s, item[0], take(m, item[0]))
            scored(item, q, k_s, s_s, n_s, False)
        for i, item in enumerate(items):
            rows = item[0]
            ol = weighed(item, v_s, s_s, n_s, length(rows))
            keep = jnp.exp2((take(m, rows) - take(n_s, rows)) * SCALE)
            settle(i, (take(o, rows) * keep + ol[:, :HEAD]) / (take(l, rows) * keep + ol[:, HEAD:]))

    @pl.when(sc_ref[2] < 2)
    def _():
        for i, rows in enumerate(pairs):
            settle(i, take(o, rows) / take(l, rows))

    keep_ref[...] = mix_s[pl.ds(par, 1)][0].astype(BF16)
    send_ref[...] = mix_s[pl.ds(1 - par, 1)][0].astype(BF16)


def out_terms(sc_ref, x_refs, w_ref, column, block, head):
    tp, par = sc_ref[0], sc_ref[1]
    heads = w_ref.shape[0] // HEAD // 4
    order = (2 * tp + par, 2 * tp + 1 - par, 2 * (1 - tp) + par, 2 * (1 - tp) + 1 - par)
    x = jnp.concatenate([x_ref[...] for x_ref in x_refs], axis=1)
    w = jnp.concatenate([w_ref[pl.ds(pl.multiple_of((i * heads + head) * HEAD, HEAD), HEAD), pl.ds(column, block)]
                         for i in order], axis=0)
    return jnp.dot(x, w, preferred_element_type=F32)


def out_first_kernel(sc_ref, a_ref, b_ref, c_ref, d_ref, w_ref, o_ref):
    block = 2 * HEAD
    for j in range(o_ref.shape[1] // block):
        o_ref[:, j * block:(j + 1) * block] = out_terms(
            sc_ref, (a_ref, b_ref, c_ref, d_ref), w_ref, j * block, block, 0)


def out_last_kernel(sc_ref, a_ref, b_ref, c_ref, d_ref, w_ref, t_ref, o_ref):
    block = o_ref.shape[1]
    column = pl.multiple_of(pl.program_id(0) * block, block)
    total = out_terms(sc_ref, (a_ref, b_ref, c_ref, d_ref), w_ref, column, block, 1)
    o_ref[...] = (t_ref[:, pl.ds(column, block)] + total).astype(BF16)


def out_last(scalars, parts, weight, total):
    rows, columns = total.shape
    steps = columns // (2 * HEAD)
    return pl.pallas_call(
        out_last_kernel,
        grid=(steps,),
        in_specs=[pl.BlockSpec(memory_space=pltpu.SMEM)] + in_vmem(6),
        out_specs=pl.BlockSpec((rows, columns // steps), lambda j: (0, j)),
        out_shape=jax.ShapeDtypeStruct((rows, columns), BF16),
        compiler_params=pltpu.CompilerParams(vmem_limit_bytes=16 * 2 ** 20),
        cost_estimate=pl.CostEstimate(flops=rows * weight.size, transcendentals=0, bytes_accessed=0),
        name="out_last",
    )(scalars, *parts, weight, total)


def swap(x, axis):
    return lax.ppermute(x, axis, [(i, i ^ 1) for i in range(lax.axis_size(axis))])


def onward(x):
    n = lax.axis_size("sp")
    return lax.ppermute(x, "sp", [(i, i + 2) for i in range(n - 2)])


def body(tokens, query_weight, key_weight, value_weight, output_weight):
    half, depth = tokens.shape
    rows = 2 * half
    group = 2 * rows
    nq = rows // FAR_DILATION
    assert 2 * group == FAR_DILATION * REACH_STEPS
    heads = query_weight.shape[1] // HEAD // 2
    width = heads * HEAD
    flops = 2 * rows * depth * width
    sp, tp = lax.axis_index("sp"), lax.axis_index("tp")
    scalars = jnp.stack([tp, sp % 2, sp // 2, sp]).astype(jnp.int32)
    inverse = THETA_BASE ** (-jnp.arange(HEAD // 2, dtype=F32) / (HEAD // 2))
    inverse = jnp.concatenate([inverse, inverse])[None]
    group0, group1, near0, near1, pair2 = biases(nq)
    shape = jax.ShapeDtypeStruct
    kv = shape((heads, 2, half, HEAD), BF16)
    q_shape, q_half = shape((heads, rows, HEAD), BF16), shape((heads, half, HEAD), BF16)
    table = shape((2, half, HEAD), F32)
    buffers = pltpu.VMEM((4 * heads, half, HEAD), F32)

    partner = swap(tokens, "tp")
    kv_a, send_a, weights, cosine, sine = call(
        own_kernel, scalars, [tokens, key_weight, value_weight, inverse],
        [kv, kv, shape((2, 2, depth, width), BF16), table, table],
        [pltpu.VMEM((half, depth), BF16), buffers, pltpu.SemaphoreType.DMA((5,))],
        2 * flops, hbm=(0, 1, 2))
    kv1_a = onward(kv_a)
    kv_ya = swap(send_a, "sp")
    kv_b, send_b = call(
        rest_kernel, scalars, [partner, weights, cosine, sine], [kv, kv], [buffers], 2 * flops)
    kv1_b = onward(kv_b)
    kv_yb = swap(send_b, "sp")
    q_a, q_b, q_send = call(
        q_kernel, scalars, [tokens, partner, cosine, sine, query_weight], [q_half, q_half, q_shape],
        [buffers], 2 * flops)
    q_y = swap(q_send, "sp")
    kv1_ya = onward(kv_ya)
    kv1_yb = onward(kv_yb)
    kv2_a = onward(kv1_a)
    kv2_b = onward(kv1_b)
    kv2_y = []
    for h in range(heads):
        kv2_y.append(onward(jnp.stack([kv1_ya[h], kv1_yb[h]])))
    state = shape((heads, group, HEAD), F32)
    kv_scratch = [pltpu.VMEM((heads, group, HEAD), BF16)] * 2
    q, m, l, o = call(
        local_kernel, scalars, [q_a, q_b, q_y, kv_a, kv_b, kv_ya, kv_yb, group0, near0, near1],
        [shape((heads, group, HEAD), BF16), state, state, state],
        kv_scratch + [pltpu.VMEM((heads, 2 * group, 4 * HEAD), F32)], 3 * 10 ** 9)
    m, l, o = call(
        one_kernel, scalars, [q, m, l, o, kv1_a, kv1_b, kv1_ya, kv1_yb, group1, near1], [state, state, state],
        kv_scratch + [pltpu.VMEM((heads, 2 * group, 2 * HEAD), F32), pltpu.VMEM((heads, group, HEAD), F32)],
        10 ** 9, {2: 0, 3: 1, 4: 2})
    mixed = shape((rows, HEAD), BF16)
    parts = []
    for h in range(heads):
        keep, send = call(
            functools.partial(two_kernel, head=h), scalars, [q, m, l, o, kv2_a, kv2_b, kv2_y[h], pair2], [mixed, mixed],
            [pltpu.VMEM((group, HEAD), BF16)] * 2 + [pltpu.VMEM((group, HEAD), F32)] * 2
            + [pltpu.VMEM((2, rows, HEAD), F32)], 10 ** 9)
        keep_tp = swap(keep, "tp")
        from_y = swap(send, "sp")
        parts.append([keep, from_y, keep_tp, swap(from_y, "tp")])
    total = call(out_first_kernel, scalars, parts[0] + [output_weight],
                 [shape((rows, output_weight.shape[1]), F32)], [], rows * output_weight.size, limit=16)[0]
    return out_last(scalars, parts[1], output_weight, total)


def solution(mesh):
    in_specs = (
        P(("grp", "sp", "tp"), None),
        P(None, "tp"),
        P(None, "tp"),
        P(None, "tp"),
        P(None, "tp"),
    )
    out_specs = P(("grp", "sp"), "tp")

    return jax.shard_map(body, mesh=mesh, in_specs=in_specs, out_specs=out_specs, check_vma=False)
```

profile of v0, /device:TPU:0, one launch (start us, length us, event | category | flops | bytes accessed | tf_op | source)
XLA Modules:
  0.0 68.5 jit_solution(9388217242493338403)
XLA Ops:
  0.0 0.5 collective-permute-start
  0.5 0.1 maximum_bitcast_fusion.inv_ref
  0.6 0.1 pad_add_fusion.sc_ref
  0.7 5.3 %shard_map.100 = (bf16[2,2,256,128]{3,2,1,0:T(8,128)(2,1)S(1)}, bf16[2,2,256,128]{3,2,1,0:T(8,128)(2,1)S(1)}, bf16[2,2,2048,256]{3,2,1,0:T(8,128)(2,1)S(1)}, f32...) custom-call(s32[4]{0:T(128)S(1)} %pad_add_fusion.sc_ref, bf16[256,2048]{1,0:T(8,128)(2,1)} %xo_ref.1, bf16[2048,512]{1,0:T(8,128)(2,1)} %wk_hbm.1, ...), custom_call_target="tpu_custom_call" | custom-call | flops 1073741824 | tf_op jit(solution)/shard_map/pallas_call | solution.py:112
  6.0 2.6 %collective-permute-start.2 = (bf16[2,2,256,128]{3,2,1,0:T(8,128)(2,1)S(1)}, bf16[2,2,256,128]{3,2,1,0:T(8,128)(2,1)S(1)}, u32[]{:S(2)}, u32[]{:S(2)}) collective-permute-start(bf16[2,2,256,128]{3,2,1,0:T(8,128)(2,1)S(1)} %get-tuple-element.34), channel_id=1, source_target_pairs={{0,2},{2,0},{4,6},{6,4},{8,10},{10,8},{12,14},{14,12},{1,3},{3,1},... | collective-permute-start | bytes 786440 | tf_op jit(solution)/shard_map/ppermute | solution.py:365
  8.6 3.5 %collective-permute-start.4 = (bf16[2,2,256,128]{3,2,1,0:T(8,128)(2,1)S(1)}, bf16[2,2,256,128]{3,2,1,0:T(8,128)(2,1)S(1)}, u32[]{:S(2)}, u32[]{:S(2)}) collective-permute-start(bf16[2,2,256,128]{3,2,1,0:T(8,128)(2,1)S(1)} %get-tuple-element.31.kva_ref), channel_id=1, source_target_pairs={{0,4},{2,6},{4,8},{6,10},{8,12},{10,14},{1,5},{3,7},{5,9},{7,11},{... | collective-permute-start | bytes 786440 | tf_op jit(solution)/shard_map/ppermute | solution.py:370
  12.1 0.0 collective-permute-done.xp_ref.x_ref
  12.1 0.0 copy-start.1
  12.1 0.0 copy-start.2
  12.1 2.3 %shard_map.102 = (bf16[2,2,256,128]{3,2,1,0:T(8,128)(2,1)S(1)}, bf16[2,2,256,128]{3,2,1,0:T(8,128)(2,1)S(1)}) custom-call(s32[4]{0:T(128)S(1)} %pad_add_fusion.sc_ref, bf16[256,2048]{1,0:T(8,128)(2,1)S(1)} %collective-permute-done.xp_ref.x_ref, bf16[2,2,2048,256]{3,2,1,0:T(8,128)(2,1)S(1)} %get-tuple-element.32.w_ref, ...), custom_call_target="tpu_custom_call" | custom-call | flops 1073741824 | tf_op jit(solution)/shard_map/pallas_call | solution.py:112
  14.4 0.6 collective-permute-start.3
  15.0 0.6 collective-permute-done.2.kvya_ref
  15.5 3.7 %collective-permute-start.6 = (bf16[2,2,256,128]{3,2,1,0:T(8,128)(2,1)S(1)}, bf16[2,2,256,128]{3,2,1,0:T(8,128)(2,1)S(1)}, u32[]{:S(2)}, u32[]{:S(2)}) collective-permute-start(bf16[2,2,256,128]{3,2,1,0:T(8,128)(2,1)S(1)} %collective-permute-done.2.kvya_ref), channel_id=1, source_target_pairs={{0,4},{2,6},{4,8},{6,10},{8,12},{10,14},{1,5},{3,7},{5,9},{7,11},{... | collective-permute-start | bytes 786440 | tf_op jit(solution)/shard_map/ppermute | solution.py:370
  19.3 0.0 collective-permute-done.4.kva_ref
  19.3 3.5 %collective-permute-start.8 = (bf16[2,2,256,128]{3,2,1,0:T(8,128)(2,1)S(1)}, bf16[2,2,256,128]{3,2,1,0:T(8,128)(2,1)S(1)}, u32[]{:S(2)}, u32[]{:S(2)}) collective-permute-start(bf16[2,2,256,128]{3,2,1,0:T(8,128)(2,1)S(1)} %collective-permute-done.4.kva_ref), channel_id=1, source_target_pairs={{0,4},{2,6},{4,8},{6,10},{8,12},{10,14},{1,5},{3,7},{5,9},{7,11},{... | collective-permute-start | bytes 786440 | tf_op jit(solution)/shard_map/ppermute | solution.py:370
  22.8 3.9 %collective-permute-start.5 = (bf16[2,2,256,128]{3,2,1,0:T(8,128)(2,1)S(1)}, bf16[2,2,256,128]{3,2,1,0:T(8,128)(2,1)S(1)}, u32[]{:S(2)}, u32[]{:S(2)}) collective-permute-start(bf16[2,2,256,128]{3,2,1,0:T(8,128)(2,1)S(1)} %get-tuple-element.33.kvb_ref), channel_id=1, source_target_pairs={{0,4},{2,6},{4,8},{6,10},{8,12},{10,14},{1,5},{3,7},{5,9},{7,11},{... | collective-permute-start | bytes 786440 | tf_op jit(solution)/shard_map/ppermute | solution.py:370
  26.7 0.0 collective-permute-done.3.kvyb_ref
  26.7 2.6 %collective-permute-start.7 = (bf16[2,2,256,128]{3,2,1,0:T(8,128)(2,1)S(1)}, bf16[2,2,256,128]{3,2,1,0:T(8,128)(2,1)S(1)}, u32[]{:S(2)}, u32[]{:S(2)}) collective-permute-start(bf16[2,2,256,128]{3,2,1,0:T(8,128)(2,1)S(1)} %collective-permute-done.3.kvyb_ref), channel_id=1, source_target_pairs={{0,4},{2,6},{4,8},{6,10},{8,12},{10,14},{1,5},{3,7},{5,9},{7,11},{... | collective-permute-start | bytes 786440 | tf_op jit(solution)/shard_map/ppermute | solution.py:370
  29.4 0.0 collective-permute-done.6.kvya_ref
  29.4 0.0 copy-done.1
  29.4 0.0 copy-done.2
  29.4 0.0 copy-start.4
  29.4 0.0 copy-start.6
  29.5 0.0 copy-start.7
  29.5 2.4 %shard_map.101 = (bf16[2,256,128]{2,1,0:T(8,128)(2,1)S(1)}, bf16[2,256,128]{2,1,0:T(8,128)(2,1)S(1)}, bf16[2,512,128]{2,1,0:T(8,128)(2,1)S(1)}) custom-call(s32[4]{0:T(128)S(1)} %pad_add_fusion.sc_ref, bf16[256,2048]{1,0:T(8,128)(2,1)S(1)} %copy-done.1, bf16[256,2048]{1,0:T(8,128)(2,1)S(1)} %collective-permute-done.xp_ref.x_ref, ...), custom_call_target="tpu_custom_call" | custom-call | flops 1073741824 | tf_op jit(solution)/shard_map/pallas_call | solution.py:112
  31.9 0.9 %collective-permute-start.1 = (bf16[2,512,128]{2,1,0:T(8,128)(2,1)S(1)}, bf16[2,512,128]{2,1,0:T(8,128)(2,1)S(1)}, u32[]{:S(2)}, u32[]{:S(2)}) collective-permute-start(bf16[2,512,128]{2,1,0:T(8,128)(2,1)S(1)} %get-tuple-element.30), channel_id=1, source_target_pairs={{0,2},{2,0},{4,6},{6,4},{8,10},{10,8},{12,14},{14,12},{1,3},{3,1},... | collective-permute-start | bytes 786440 | tf_op jit(solution)/shard_map/ppermute | solution.py:365
  32.7 4.4 %collective-permute-done.5.kvb_ref = bf16[2,2,256,128]{3,2,1,0:T(8,128)(2,1)S(1)} collective-permute-done((bf16[2,2,256,128]{3,2,1,0:T(8,128)(2,1)S(1)}, bf16[2,2,256,128]{3,2,1,0:T(8,128)(2,1)S(1)}, u32[]{:S(2)}, u32[]{:S(2)}) %collective-permute-start.5) | collective-permute-done | bytes 262176 | tf_op jit(solution)/shard_map/ppermute | solution.py:370
  37.2 4.4 %collective-permute-start.9 = (bf16[2,2,256,128]{3,2,1,0:T(8,128)(2,1)S(1)}, bf16[2,2,256,128]{3,2,1,0:T(8,128)(2,1)S(1)}, u32[]{:S(2)}, u32[]{:S(2)}) collective-permute-start(bf16[2,2,256,128]{3,2,1,0:T(8,128)(2,1)S(1)} %collective-permute-done.5.kvb_ref), channel_id=1, source_target_pairs={{0,4},{2,6},{4,8},{6,10},{8,12},{10,14},{1,5},{3,7},{5,9},{7,11},{... | collective-permute-start | bytes 786440 | tf_op jit(solution)/shard_map/ppermute | solution.py:370
  41.6 1.2 %collective-permute-done.7.kvyb_ref = bf16[2,2,256,128]{3,2,1,0:T(8,128)(2,1)S(1)} collective-permute-done((bf16[2,2,256,128]{3,2,1,0:T(8,128)(2,1)S(1)}, bf16[2,2,256,128]{3,2,1,0:T(8,128)(2,1)S(1)}, u32[]{:S(2)}, u32[]{:S(2)}) %collective-permute-start.7) | collective-permute-done | bytes 262176 | tf_op jit(solution)/shard_map/ppermute | solution.py:370
  42.8 4.4 %collective-permute-start.14 = (bf16[2,2,256,128]{3,2,1,0:T(8,128)(2,1)S(1)}, bf16[2,2,256,128]{3,2,1,0:T(8,128)(2,1)S(1)}, u32[]{:S(2)}, u32[]{:S(2)}) collective-permute-start(bf16[2,2,256,128]{3,2,1,0:T(8,128)(2,1)S(1)} %pad_maximum_fusion.1), channel_id=1, source_target_pairs={{0,4},{2,6},{4,8},{6,10},{8,12},{10,14},{1,5},{3,7},{5,9},{7,11},{... | collective-permute-start | bytes 786440 | tf_op jit(solution)/shard_map/ppermute | solution.py:370
  47.3 3.5 %collective-permute-start.10 = (bf16[2,2,256,128]{3,2,1,0:T(8,128)(2,1)S(1)}, bf16[2,2,256,128]{3,2,1,0:T(8,128)(2,1)S(1)}, u32[]{:S(2)}, u32[]{:S(2)}) collective-permute-start(bf16[2,2,256,128]{3,2,1,0:T(8,128)(2,1)S(1)} %pad_maximum_fusion), channel_id=1, source_target_pairs={{0,4},{2,6},{4,8},{6,10},{8,12},{10,14},{1,5},{3,7},{5,9},{7,11},{... | collective-permute-start | bytes 786440 | tf_op jit(solution)/shard_map/ppermute | solution.py:370
  50.8 0.0 collective-permute-done.1.qy_ref
  50.8 0.0 copy-done.4
  50.8 0.0 copy-done.6
  50.8 0.0 copy-done.7
  50.8 0.0 copy-start.5
  50.8 3.5 %shard_map.103 = (bf16[2,1024,128]{2,1,0:T(8,128)(2,1)S(1)}, f32[2,1024,128]{2,1,0:T(8,128)S(1)}, f32[2,1024,128]{2,1,0:T(8,128)S(1)}, f32[2,1024,128]{2,1,0:T(8,128)S(1)}) custom-call(s32[4]{0:T(128)S(1)} %pad_add_fusion.sc_ref, bf16[2,256,128]{2,1,0:T(8,128)(2,1)S(1)} %get-tuple-element.28.qa_ref, bf16[2,256,128]{2,1,0:T(8,128)(2,1)S(1)} %get-tuple-element.29.qb_ref, ...), custom_call_target="tpu_custom_call" | custom-call | flops 3000000000 | tf_op jit(solution)/shard_map/pallas_call | solution.py:112
  54.3 0.0 copy-done.5
  54.3 0.0 copy-start.3
  54.3 0.6 shard_map.104
  54.9 0.0 collective-permute-done.8.kva_ref
  54.9 0.0 collective-permute-done.9.kvb_ref
  54.9 0.0 collective-permute-done.14.kvy_ref
  54.9 0.2 copy-done.3
  55.2 0.9 %shard_map.106 = (bf16[512,128]{1,0:T(8,128)(2,1)S(1)}, bf16[512,128]{1,0:T(8,128)(2,1)S(1)}) custom-call(s32[4]{0:T(128)S(1)} %pad_add_fusion.sc_ref, bf16[2,1024,128]{2,1,0:T(8,128)(2,1)S(1)} %get-tuple-element.36.q_ref, f32[2,1024,128]{2,1,0:T(8,128)S(1)} %get-tuple-element.40.m_ref, f32[2,1024,128]{2,1,0:T(8,128)S(1)} %get-tuple-element.41.l_ref, ...), custom_call_target="tpu_custom_call" | custom-call | flops 1000000000 | tf_op jit(solution)/shard_map/pallas_call | solution.py:112
  56.0 0.0 copy-start
  56.0 1.6 %collective-permute-start.15 = (bf16[512,128]{1,0:T(8,128)(2,1)S(1)}, bf16[512,128]{1,0:T(8,128)(2,1)S(1)}, u32[]{:S(2)}, u32[]{:S(2)}) collective-permute-start(bf16[512,128]{1,0:T(8,128)(2,1)S(1)} %get-tuple-element.46), channel_id=1, source_target_pairs={{0,2},{2,0},{4,6},{6,4},{8,10},{10,8},{12,14},{14,12},{1,3},{3,1},... | collective-permute-start | bytes 393224 | tf_op jit(solution)/shard_map/ppermute | solution.py:365
  57.6 0.7 collective-permute-done.10.kvy_ref
  58.3 0.9 %shard_map.105 = (bf16[512,128]{1,0:T(8,128)(2,1)S(1)}, bf16[512,128]{1,0:T(8,128)(2,1)S(1)}) custom-call(s32[4]{0:T(128)S(1)} %pad_add_fusion.sc_ref, bf16[2,1024,128]{2,1,0:T(8,128)(2,1)S(1)} %get-tuple-element.36.q_ref, f32[2,1024,128]{2,1,0:T(8,128)S(1)} %get-tuple-element.40.m_ref, f32[2,1024,128]{2,1,0:T(8,128)S(1)} %get-tuple-element.41.l_ref, ...), custom_call_target="tpu_custom_call" | custom-call | flops 1000000000 | tf_op jit(solution)/shard_map/pallas_call | solution.py:112
  59.2 1.6 %collective-permute-start.11 = (bf16[512,128]{1,0:T(8,128)(2,1)S(1)}, bf16[512,128]{1,0:T(8,128)(2,1)S(1)}, u32[]{:S(2)}, u32[]{:S(2)}) collective-permute-start(bf16[512,128]{1,0:T(8,128)(2,1)S(1)} %get-tuple-element.44), channel_id=1, source_target_pairs={{0,2},{2,0},{4,6},{6,4},{8,10},{10,8},{12,14},{14,12},{1,3},{3,1},... | collective-permute-start | bytes 393224 | tf_op jit(solution)/shard_map/ppermute | solution.py:365
  60.8 0.0 collective-permute-start.16
  60.8 0.8 %collective-permute-done.15.b_ref = bf16[512,128]{1,0:T(8,128)(2,1)S(1)} collective-permute-done((bf16[512,128]{1,0:T(8,128)(2,1)S(1)}, bf16[512,128]{1,0:T(8,128)(2,1)S(1)}, u32[]{:S(2)}, u32[]{:S(2)}) %collective-permute-start.15) | collective-permute-done | bytes 131104 | tf_op jit(solution)/shard_map/ppermute | solution.py:365
  61.5 0.0 collective-permute-start.17
  61.5 0.5 collective-permute-start.12
  62.0 2.2 %collective-permute-done.11.b_ref = bf16[512,128]{1,0:T(8,128)(2,1)S(1)} collective-permute-done((bf16[512,128]{1,0:T(8,128)(2,1)S(1)}, bf16[512,128]{1,0:T(8,128)(2,1)S(1)}, u32[]{:S(2)}, u32[]{:S(2)}) %collective-permute-start.11) | collective-permute-done | bytes 131104 | tf_op jit(solution)/shard_map/ppermute | solution.py:365
  64.2 0.0 collective-permute-start.13
  64.2 0.0 collective-permute-done.16.c_ref
  64.2 0.0 collective-permute-done.17.d_ref
  64.2 0.0 copy-done
  64.2 1.3 %shard_map.107.t_ref = f32[512,1024]{1,0:T(8,128)S(1)} custom-call(s32[4]{0:T(128)S(1)} %pad_add_fusion.sc_ref, bf16[512,128]{1,0:T(8,128)(2,1)S(1)} %get-tuple-element.45.a_ref, bf16[512,128]{1,0:T(8,128)(2,1)S(1)} %collective-permute-done.15.b_ref, bf16[512,128]{1,0:T(8,128)(2,1)S(1)} %collective-permute-done.16.c_ref, ...), custom_call_target="tpu_custom_call" | custom-call | flops 536870912 | tf_op jit(solution)/shard_map/pallas_call | solution.py:112
  65.5 0.0 collective-permute-done.12.c_ref
  65.5 0.1 collective-permute-done.13.d_ref
  65.6 2.9 %out_last.1 = bf16[512,1024]{1,0:T(8,128)(2,1)} custom-call(s32[4]{0:T(128)S(1)} %pad_add_fusion.sc_ref, bf16[512,128]{1,0:T(8,128)(2,1)S(1)} %get-tuple-element.43.a_ref, bf16[512,128]{1,0:T(8,128)(2,1)S(1)} %collective-permute-done.11.b_ref, bf16[512,128]{1,0:T(8,128)(2,1)S(1)} %collective-permute-done.12.c_ref, ...), custom_call_target="tpu_custom_call" | custom-call | flops 536870912 | tf_op jit(solution)/shard_map/out_last/pallas_call | solution.py:352
  (5 shorter events, 0.1 us)
Async XLA Ops:
  0.0 12.1 %collective-permute-start = (bf16[256,2048]{1,0:T(8,128)(2,1)}, bf16[256,2048]{1,0:T(8,128)(2,1)S(1)}, u32[]{:S(2)}, u32[]{:S(2)}) collective-permute-start(bf16[256,2048]{1,0:T(8,128)(2,1)} %xo_ref.1), channel_id=1, source_target_pairs={{0,1},{1,0},{2,3},{3,2},{4,5},{5,4},{6,7},{7,6},{8,9},{9,8},{10,11... | collective-permute-start | bytes 3145736 | tf_op jit(solution)/shard_map/ppermute | solution.py:365
  6.0 9.5 %collective-permute-start.2 = (bf16[2,2,256,128]{3,2,1,0:T(8,128)(2,1)S(1)}, bf16[2,2,256,128]{3,2,1,0:T(8,128)(2,1)S(1)}, u32[]{:S(2)}, u32[]{:S(2)}) collective-permute-start(bf16[2,2,256,128]{3,2,1,0:T(8,128)(2,1)S(1)} %get-tuple-element.34), channel_id=1, source_target_pairs={{0,2},{2,0},{4,6},{6,4},{8,10},{10,8},{12,14},{14,12},{1,3},{3,1},... | collective-permute-start | bytes 786440 | tf_op jit(solution)/shard_map/ppermute | solution.py:365
  8.6 10.7 %collective-permute-start.4 = (bf16[2,2,256,128]{3,2,1,0:T(8,128)(2,1)S(1)}, bf16[2,2,256,128]{3,2,1,0:T(8,128)(2,1)S(1)}, u32[]{:S(2)}, u32[]{:S(2)}) collective-permute-start(bf16[2,2,256,128]{3,2,1,0:T(8,128)(2,1)S(1)} %get-tuple-element.31.kva_ref), channel_id=1, source_target_pairs={{0,4},{2,6},{4,8},{6,10},{8,12},{10,14},{1,5},{3,7},{5,9},{7,11},{... | collective-permute-start | bytes 786440 | tf_op jit(solution)/shard_map/ppermute | solution.py:370
  12.1 17.3 %copy-start.1 = (bf16[256,2048]{1,0:T(8,128)(2,1)S(1)}, bf16[256,2048]{1,0:T(8,128)(2,1)}, u32[]{:S(2)}) copy-start(bf16[256,2048]{1,0:T(8,128)(2,1)} %xo_ref.1) | copy-start | bytes 3145732
  12.1 17.3 %copy-start.2 = (bf16[2048,512]{1,0:T(8,128)(2,1)S(1)}, bf16[2048,512]{1,0:T(8,128)(2,1)}, u32[]{:S(2)}) copy-start(bf16[2048,512]{1,0:T(8,128)(2,1)} %w_ref.3) | copy-start | bytes 6291460
  14.4 12.3 %collective-permute-start.3 = (bf16[2,2,256,128]{3,2,1,0:T(8,128)(2,1)S(1)}, bf16[2,2,256,128]{3,2,1,0:T(8,128)(2,1)S(1)}, u32[]{:S(2)}, u32[]{:S(2)}) collective-permute-start(bf16[2,2,256,128]{3,2,1,0:T(8,128)(2,1)S(1)} %get-tuple-element.35), channel_id=1, source_target_pairs={{0,2},{2,0},{4,6},{6,4},{8,10},{10,8},{12,14},{14,12},{1,3},{3,1},... | collective-permute-start | bytes 786440 | tf_op jit(solution)/shard_map/ppermute | solution.py:365
  15.5 13.8 %collective-permute-start.6 = (bf16[2,2,256,128]{3,2,1,0:T(8,128)(2,1)S(1)}, bf16[2,2,256,128]{3,2,1,0:T(8,128)(2,1)S(1)}, u32[]{:S(2)}, u32[]{:S(2)}) collective-permute-start(bf16[2,2,256,128]{3,2,1,0:T(8,128)(2,1)S(1)} %collective-permute-done.2.kvya_ref), channel_id=1, source_target_pairs={{0,4},{2,6},{4,8},{6,10},{8,12},{10,14},{1,5},{3,7},{5,9},{7,11},{... | collective-permute-start | bytes 786440 | tf_op jit(solution)/shard_map/ppermute | solution.py:370
  19.3 35.6 %collective-permute-start.8 = (bf16[2,2,256,128]{3,2,1,0:T(8,128)(2,1)S(1)}, bf16[2,2,256,128]{3,2,1,0:T(8,128)(2,1)S(1)}, u32[]{:S(2)}, u32[]{:S(2)}) collective-permute-start(bf16[2,2,256,128]{3,2,1,0:T(8,128)(2,1)S(1)} %collective-permute-done.4.kva_ref), channel_id=1, source_target_pairs={{0,4},{2,6},{4,8},{6,10},{8,12},{10,14},{1,5},{3,7},{5,9},{7,11},{... | collective-permute-start | bytes 786440 | tf_op jit(solution)/shard_map/ppermute | solution.py:370
  22.8 14.4 %collective-permute-start.5 = (bf16[2,2,256,128]{3,2,1,0:T(8,128)(2,1)S(1)}, bf16[2,2,256,128]{3,2,1,0:T(8,128)(2,1)S(1)}, u32[]{:S(2)}, u32[]{:S(2)}) collective-permute-start(bf16[2,2,256,128]{3,2,1,0:T(8,128)(2,1)S(1)} %get-tuple-element.33.kvb_ref), channel_id=1, source_target_pairs={{0,4},{2,6},{4,8},{6,10},{8,12},{10,14},{1,5},{3,7},{5,9},{7,11},{... | collective-permute-start | bytes 786440 | tf_op jit(solution)/shard_map/ppermute | solution.py:370
  26.7 16.0 %collective-permute-start.7 = (bf16[2,2,256,128]{3,2,1,0:T(8,128)(2,1)S(1)}, bf16[2,2,256,128]{3,2,1,0:T(8,128)(2,1)S(1)}, u32[]{:S(2)}, u32[]{:S(2)}) collective-permute-start(bf16[2,2,256,128]{3,2,1,0:T(8,128)(2,1)S(1)} %collective-permute-done.3.kvyb_ref), channel_id=1, source_target_pairs={{0,4},{2,6},{4,8},{6,10},{8,12},{10,14},{1,5},{3,7},{5,9},{7,11},{... | collective-permute-start | bytes 786440 | tf_op jit(solution)/shard_map/ppermute | solution.py:370
  29.4 21.3 %copy-start.4 = (f32[256,256]{1,0:T(8,128)S(1)}, f32[256,256]{1,0:T(8,128)}, u32[]{:S(2)}) copy-start(f32[256,256]{1,0:T(8,128)} %constant.49.clone.near1_ref.near_ref) | copy-start | bytes 786436
  29.4 21.3 %copy-start.6 = (f32[256,256]{1,0:T(8,128)S(1)}, f32[256,256]{1,0:T(8,128)}, u32[]{:S(2)}) copy-start(f32[256,256]{1,0:T(8,128)} %constant.47.clone.group_ref) | copy-start | bytes 786436
  29.5 21.3 %copy-start.7 = (f32[256,256]{1,0:T(8,128)S(1)}, f32[256,256]{1,0:T(8,128)}, u32[]{:S(2)}) copy-start(f32[256,256]{1,0:T(8,128)} %constant.48.clone.near0_ref) | copy-start | bytes 786436
  31.9 18.9 %collective-permute-start.1 = (bf16[2,512,128]{2,1,0:T(8,128)(2,1)S(1)}, bf16[2,512,128]{2,1,0:T(8,128)(2,1)S(1)}, u32[]{:S(2)}, u32[]{:S(2)}) collective-permute-start(bf16[2,512,128]{2,1,0:T(8,128)(2,1)S(1)} %get-tuple-element.30), channel_id=1, source_target_pairs={{0,2},{2,0},{4,6},{6,4},{8,10},{10,8},{12,14},{14,12},{1,3},{3,1},... | collective-permute-start | bytes 786440 | tf_op jit(solution)/shard_map/ppermute | solution.py:365
  37.2 17.8 %collective-permute-start.9 = (bf16[2,2,256,128]{3,2,1,0:T(8,128)(2,1)S(1)}, bf16[2,2,256,128]{3,2,1,0:T(8,128)(2,1)S(1)}, u32[]{:S(2)}, u32[]{:S(2)}) collective-permute-start(bf16[2,2,256,128]{3,2,1,0:T(8,128)(2,1)S(1)} %collective-permute-done.5.kvb_ref), channel_id=1, source_target_pairs={{0,4},{2,6},{4,8},{6,10},{8,12},{10,14},{1,5},{3,7},{5,9},{7,11},{... | collective-permute-start | bytes 786440 | tf_op jit(solution)/shard_map/ppermute | solution.py:370
  42.8 12.1 %collective-permute-start.14 = (bf16[2,2,256,128]{3,2,1,0:T(8,128)(2,1)S(1)}, bf16[2,2,256,128]{3,2,1,0:T(8,128)(2,1)S(1)}, u32[]{:S(2)}, u32[]{:S(2)}) collective-permute-start(bf16[2,2,256,128]{3,2,1,0:T(8,128)(2,1)S(1)} %pad_maximum_fusion.1), channel_id=1, source_target_pairs={{0,4},{2,6},{4,8},{6,10},{8,12},{10,14},{1,5},{3,7},{5,9},{7,11},{... | collective-permute-start | bytes 786440 | tf_op jit(solution)/shard_map/ppermute | solution.py:370
  47.3 11.0 %collective-permute-start.10 = (bf16[2,2,256,128]{3,2,1,0:T(8,128)(2,1)S(1)}, bf16[2,2,256,128]{3,2,1,0:T(8,128)(2,1)S(1)}, u32[]{:S(2)}, u32[]{:S(2)}) collective-permute-start(bf16[2,2,256,128]{3,2,1,0:T(8,128)(2,1)S(1)} %pad_maximum_fusion), channel_id=1, source_target_pairs={{0,4},{2,6},{4,8},{6,10},{8,12},{10,14},{1,5},{3,7},{5,9},{7,11},{... | collective-permute-start | bytes 786440 | tf_op jit(solution)/shard_map/ppermute | solution.py:370
  50.8 3.5 %copy-start.5 = (f32[256,256]{1,0:T(8,128)S(1)}, f32[256,256]{1,0:T(8,128)}, u32[]{:S(2)}) copy-start(f32[256,256]{1,0:T(8,128)} %constant.50.clone.group_ref) | copy-start | bytes 786436
  54.3 0.8 %copy-start.3 = (f32[128,128]{1,0:T(8,128)S(1)}, f32[128,128]{1,0:T(8,128)}, u32[]{:S(2)}) copy-start(f32[128,128]{1,0:T(8,128)} %constant.51.clone.pair_ref) | copy-start | bytes 196612
  56.0 8.2 %copy-start = (bf16[1024,1024]{1,0:T(8,128)(2,1)S(1)}, bf16[1024,1024]{1,0:T(8,128)(2,1)}, u32[]{:S(2)}) copy-start(bf16[1024,1024]{1,0:T(8,128)(2,1)} %w_ref.5) | copy-start | bytes 6291460
  56.0 5.5 %collective-permute-start.15 = (bf16[512,128]{1,0:T(8,128)(2,1)S(1)}, bf16[512,128]{1,0:T(8,128)(2,1)S(1)}, u32[]{:S(2)}, u32[]{:S(2)}) collective-permute-start(bf16[512,128]{1,0:T(8,128)(2,1)S(1)} %get-tuple-element.46), channel_id=1, source_target_pairs={{0,2},{2,0},{4,6},{6,4},{8,10},{10,8},{12,14},{14,12},{1,3},{3,1},... | collective-permute-start | bytes 393224 | tf_op jit(solution)/shard_map/ppermute | solution.py:365
  59.2 5.0 %collective-permute-start.11 = (bf16[512,128]{1,0:T(8,128)(2,1)S(1)}, bf16[512,128]{1,0:T(8,128)(2,1)S(1)}, u32[]{:S(2)}, u32[]{:S(2)}) collective-permute-start(bf16[512,128]{1,0:T(8,128)(2,1)S(1)} %get-tuple-element.44), channel_id=1, source_target_pairs={{0,2},{2,0},{4,6},{6,4},{8,10},{10,8},{12,14},{14,12},{1,3},{3,1},... | collective-permute-start | bytes 393224 | tf_op jit(solution)/shard_map/ppermute | solution.py:365
  60.8 3.5 %collective-permute-start.16 = (bf16[512,128]{1,0:T(8,128)(2,1)S(1)}, bf16[512,128]{1,0:T(8,128)(2,1)S(1)}, u32[]{:S(2)}, u32[]{:S(2)}) collective-permute-start(bf16[512,128]{1,0:T(8,128)(2,1)S(1)} %get-tuple-element.45.a_ref), channel_id=1, source_target_pairs={{0,1},{1,0},{2,3},{3,2},{4,5},{5,4},{6,7},{7,6},{8,9},{9,8},{10,11... | collective-permute-start | bytes 393224 | tf_op jit(solution)/shard_map/ppermute | solution.py:365
  61.5 2.7 %collective-permute-start.17 = (bf16[512,128]{1,0:T(8,128)(2,1)S(1)}, bf16[512,128]{1,0:T(8,128)(2,1)S(1)}, u32[]{:S(2)}, u32[]{:S(2)}) collective-permute-start(bf16[512,128]{1,0:T(8,128)(2,1)S(1)} %collective-permute-done.15.b_ref), channel_id=1, source_target_pairs={{0,1},{1,0},{2,3},{3,2},{4,5},{5,4},{6,7},{7,6},{8,9},{9,8},{10,11... | collective-permute-start | bytes 393224 | tf_op jit(solution)/shard_map/ppermute | solution.py:365
  61.5 4.0 %collective-permute-start.12 = (bf16[512,128]{1,0:T(8,128)(2,1)S(1)}, bf16[512,128]{1,0:T(8,128)(2,1)S(1)}, u32[]{:S(2)}, u32[]{:S(2)}) collective-permute-start(bf16[512,128]{1,0:T(8,128)(2,1)S(1)} %get-tuple-element.43.a_ref), channel_id=1, source_target_pairs={{0,1},{1,0},{2,3},{3,2},{4,5},{5,4},{6,7},{7,6},{8,9},{9,8},{10,11... | collective-permute-start | bytes 393224 | tf_op jit(solution)/shard_map/ppermute | solution.py:365
  64.2 1.3 %collective-permute-start.13 = (bf16[512,128]{1,0:T(8,128)(2,1)S(1)}, bf16[512,128]{1,0:T(8,128)(2,1)S(1)}, u32[]{:S(2)}, u32[]{:S(2)}) collective-permute-start(bf16[512,128]{1,0:T(8,128)(2,1)S(1)} %collective-permute-done.11.b_ref), channel_id=1, source_target_pairs={{0,1},{1,0},{2,3},{3,2},{4,5},{5,4},{6,7},{7,6},{8,9},{9,8},{10,11... | collective-permute-start | bytes 393224 | tf_op jit(solution)/shard_map/ppermute | solution.py:365
where the time goes:
time: 69.5 us; the launch traced here: 68.5 us
  starting transfers between devices  37.7 us (54%)
  Pallas kernels  19.9 us (29%)
  waiting for transfers between devices  9.95 us (14%)
    ppermute x8, starting transfers between devices, onward(): return lax.ppermute(x, 'sp', [(i, i + 2) for i in range(n - 2)])  29.5 us
    pallas_call x8, Pallas kernels, call(): pl.pallas_call(kernel, in_specs=[pl.BlockSpec(memory_space=pltpu.SMEM)] +...  17 us
    ppermute x10, starting transfers between devices, swap(): lax.ppermute(x, axis, [(i, i ^ 1) for i in range(lax.axis_size(axis))])  8.17 us
    ppermute x8, waiting for transfers between devices, onward(): return lax.ppermute(x, 'sp', [(i, i + 2) for i in range(n - 2)])  6.35 us
    ppermute x10, waiting for transfers between devices, swap(): lax.ppermute(x, axis, [(i, i ^ 1) for i in range(lax.axis_size(axis))])  3.6 us
    pallas_call x1, Pallas kernels, out_last(): pl.pallas_call(out_last_kernel, grid=(steps,), in_specs=[pl.BlockSpec(mem...  2.91 us
  transfers between devices with their start and end apart: 18, of which 7 were waited for; matrix products, arithmetic and copies ran while one was open for 0% of the time, Pallas kernels for 25%

commit v1 on v0

--- a/solution.py
+++ b/solution.py
@@ -37,37 +37,36 @@
         out_ref[lead + (pl.ds(at, nq_half), slice(None))] = piece.astype(BF16)
 
 
-def kv_half(x_ref, w_ref, keep_ref, send_ref, cos_ref, sin_ref, buf_ref, part, ready=None):
-    cos, sin = cos_ref.at[part], sin_ref.at[part]
+def kv_part(x_ref, w_ref, out_ref, cos_ref, sin_ref, buf_ref, ready=None):
     slot = 0
-    for side, out_ref in enumerate((keep_ref, send_ref)):
-        for which in (1, 0):
-            if ready is not None:
-                ready(side, which)
-            acc = jnp.dot(x_ref[...], w_ref[side, which], preferred_element_type=F32)
-            for h in range(acc.shape[1] // HEAD):
-                val = acc[:, h * HEAD:(h + 1) * HEAD]
-                if which == 0:
-                    val = rotated(val, cos[...], sin[...])
-                place(out_ref, (h, which), val, buf_ref, slot, None)
-                slot += 1
-
-
-def own_kernel(sc_ref, x_hbm, wk_hbm, wv_hbm, inv_ref,
-               keep_ref, send_ref, w_ref, cos_ref, sin_ref, x_ref, buf_ref, sems):
+    for which in (1, 0):
+        if ready is not None:
+            ready[which].wait()
+        acc = jnp.dot(x_ref[...], w_ref[which], preferred_element_type=F32)
+        for h in range(acc.shape[1] // HEAD):
+            val = acc[:, h * HEAD:(h + 1) * HEAD]
+            if which == 0:
+                val = rotated(val, cos_ref[...], sin_ref[...])
+            place(out_ref, (h, which), val, buf_ref, slot, None)
+            slot += 1
+
+
+def weight_copies(wk_hbm, wv_hbm, w_ref, side, sems):
+    width = w_ref.shape[2]
+    column = pl.multiple_of(side * width, width)
+    return [pltpu.make_async_copy(hbm.at[:, pl.ds(column, width)], w_ref.at[which], sems.at[which])
+            for which, hbm in enumerate((wk_hbm, wv_hbm))]
+
+
+def own_keep_kernel(sc_ref, x_hbm, wk_hbm, wv_hbm, inv_ref,
+                    out_ref, x_ref, w_ref, cos_ref, sin_ref, buf_ref, sems):
     tp, par, sp = sc_ref[0], sc_ref[1], sc_ref[3]
     half = x_ref.shape[0]
-    width = w_ref.shape[3]
-    copies = {}
-    copies["x"] = pltpu.make_async_copy(x_hbm, x_ref, sems.at[0])
-    copies["x"].start()
-    for side in range(2):
-        column = pl.multiple_of((par if side == 0 else 1 - par) * width, width)
-        for which, hbm in ((1, wv_hbm), (0, wk_hbm)):
-            copy = pltpu.make_async_copy(hbm.at[:, pl.ds(column, width)], w_ref.at[side, which],
-                                         sems.at[1 + 2 * side + which])
-            copy.start()
-            copies[side, which] = copy
+    x_copy = pltpu.make_async_copy(x_hbm, x_ref, sems.at[2])
+    copies = weight_copies(wk_hbm, wv_hbm, w_ref, par, sems)
+    x_copy.start()
+    copies[1].start()
+    copies[0].start()
     steps = half // FAR_DILATION
     lane = lax.broadcasted_iota(jnp.int32, (2 * steps, HEAD), 1)
     row = lax.broadcasted_iota(jnp.int32, (2 * steps, HEAD), 0)
@@ -80,13 +79,21 @@
     sign = jnp.where(lane[:1] < HEAD // 2, -1.0, 1.0)[None]
     cos_ref[...] = (cos_c * cos_f - sin_c * sin_f).reshape(2, half, HEAD)
     sin_ref[...] = ((sin_c * cos_f + cos_c * sin_f) * sign).reshape(2, half, HEAD)
-    copies["x"].wait()
-    kv_half(x_ref, w_ref, keep_ref, send_ref, cos_ref, sin_ref, buf_ref, 0,
-            lambda side, which: copies[side, which].wait())
-
-
-def rest_kernel(sc_ref, x_ref, w_ref, cos_ref, sin_ref, keep_ref, send_ref, buf_ref):
-    kv_half(x_ref, w_ref, keep_ref, send_ref, cos_ref, sin_ref, buf_ref, 1)
+    x_copy.wait()
+    kv_part(x_ref, w_ref, out_ref, cos_ref.at[0], sin_ref.at[0], buf_ref, copies)
+
+
+def rest_keep_kernel(sc_ref, x_ref, w_ref, cos_ref, sin_ref, wk_hbm, wv_hbm, out_ref, w_send_ref, buf_ref, sems):
+    copies = weight_copies(wk_hbm, wv_hbm, w_send_ref, 1 - sc_ref[1], sems)
+    for copy in copies:
+        copy.start()
+    kv_part(x_ref, w_ref, out_ref, cos_ref.at[1], sin_ref.at[1], buf_ref)
+    for copy in copies:
+        copy.wait()
+
+
+def send_kernel(sc_ref, x_ref, w_ref, cos_ref, sin_ref, out_ref, buf_ref, *, part):
+    kv_part(x_ref, w_ref, out_ref, cos_ref.at[part], sin_ref.at[part], buf_ref)
 
 
 def q_kernel(sc_ref, xo_ref, xp_ref, cos_ref, sin_ref, w_ref, keepa_ref, keepb_ref, send_ref, buf_ref):
@@ -348,7 +355,7 @@
 
 def out_last(scalars, parts, weight, total):
     rows, columns = total.shape
-    steps = columns // (2 * HEAD)
+    steps = 2
     return pl.pallas_call(
         out_last_kernel,
         grid=(steps,),
@@ -391,19 +398,24 @@
     buffers = pltpu.VMEM((4 * heads, half, HEAD), F32)
 
     partner = swap(tokens, "tp")
-    kv_a, send_a, weights, cosine, sine = call(
-        own_kernel, scalars, [tokens, key_weight, value_weight, inverse],
-        [kv, kv, shape((2, 2, depth, width), BF16), table, table],
-        [pltpu.VMEM((half, depth), BF16), buffers, pltpu.SemaphoreType.DMA((5,))],
-        2 * flops, hbm=(0, 1, 2))
+    weights = shape((2, depth, width), BF16)
+    kv_a, own, w_keep, cosine, sine = call(
+        own_keep_kernel, scalars, [tokens, key_weight, value_weight, inverse],
+        [kv, shape((half, depth), BF16), weights, table, table],
+        [buffers, pltpu.SemaphoreType.DMA((3,))], flops, hbm=(0, 1, 2))
     kv1_a = onward(kv_a)
+    kv_b, w_send = call(
+        rest_keep_kernel, scalars, [partner, w_keep, cosine, sine, key_weight, value_weight], [kv, weights],
+        [buffers, pltpu.SemaphoreType.DMA((2,))], flops, hbm=(4, 5))
+    kv1_b = onward(kv_b)
+    send_a, = call(functools.partial(send_kernel, part=0), scalars, [own, w_send, cosine, sine], [kv], [buffers],
+                   flops)
     kv_ya = swap(send_a, "sp")
-    kv_b, send_b = call(
-        rest_kernel, scalars, [partner, weights, cosine, sine], [kv, kv], [buffers], 2 * flops)
-    kv1_b = onward(kv_b)
+    send_b, = call(functools.partial(send_kernel, part=1), scalars, [partner, w_send, cosine, sine], [kv], [buffers],
+                   flops)
     kv_yb = swap(send_b, "sp")
     q_a, q_b, q_send = call(
-        q_kernel, scalars, [tokens, partner, cosine, sine, query_weight], [q_half, q_half, q_shape],
+        q_kernel, scalars, [own, partner, cosine, sine, query_weight], [q_half, q_half, q_shape],
         [buffers], 2 * flops)
     q_y = swap(q_send, "sp")
     kv1_ya = onward(kv_ya)

time: 69.5 us -> 73.1 us (1.052)
  waiting for transfers between devices: 9.95 us -> 16 us
  starting transfers between devices: 37.7 us -> 34.3 us
  Pallas kernels: 19.9 us -> 21 us
    ppermute x8, waiting for transfers between devices: 6.35 us -> 11.9 us  [onward(): return lax.ppermute(x, 'sp', [(i, i + 2) for i in range(n - 2)])]
    ppermute x8, starting transfers between devices: 29.5 us -> 26.3 us  [onward(): return lax.ppermute(x, 'sp', [(i, i + 2) for i in range(n - 2)])]
    pallas_call x8 -> x10, Pallas kernels: 17 us -> 18.7 us  [call(): pl.pallas_call(kernel, in_specs=[pl.BlockSpec(memory_space=pltpu.SMEM)] +...]
  transfers between devices with their start and end apart: 18 -> 18, of which waited for: 7 -> 5; matrix products, arithmetic and copies ran while one was open for 0% -> 0% of each run, Pallas kernels for 25% -> 20%
where the time goes in v1:
time: 73.1 us; the launch traced here: 71.9 us
  starting transfers between devices  34.3 us (47%)
  Pallas kernels  21 us (29%)
  waiting for transfers between devices  16 us (22%)
    ppermute x8, starting transfers between devices, onward(): return lax.ppermute(x, 'sp', [(i, i + 2) for i in range(n - 2)])  26.3 us
    pallas_call x10, Pallas kernels, call(): pl.pallas_call(kernel, in_specs=[pl.BlockSpec(memory_space=pltpu.SMEM)] +...  18.7 us
    ppermute x8, waiting for transfers between devices, onward(): return lax.ppermute(x, 'sp', [(i, i + 2) for i in range(n - 2)])  11.9 us
    ppermute x10, starting transfers between devices, swap(): lax.ppermute(x, axis, [(i, i ^ 1) for i in range(lax.axis_size(axis))])  8.02 us
    ppermute x10, waiting for transfers between devices, swap(): lax.ppermute(x, axis, [(i, i ^ 1) for i in range(lax.axis_size(axis))])  4.11 us
    pallas_call x1, Pallas kernels, out_last(): pl.pallas_call(out_last_kernel, grid=(steps,), in_specs=[pl.BlockSpec(mem...  2.25 us
  transfers between devices with their start and end apart: 18, of which 5 were waited for; matrix products, arithmetic and copies ran while one was open for 0% of the time, Pallas kernels for 20%

profile of v1, /device:TPU:0, one launch (start us, length us, event | category | flops | bytes accessed | tf_op | source)
XLA Modules:
  0.0 71.9 jit_solution(2191890722740465292)
XLA Ops:
  0.0 0.5 collective-permute-start
  0.5 0.1 maximum_bitcast_fusion.inv_ref
  0.6 0.1 pad_add_fusion.sc_ref
  0.7 3.7 %shard_map.100 = (bf16[2,2,256,128]{3,2,1,0:T(8,128)(2,1)S(1)}, bf16[256,2048]{1,0:T(8,128)(2,1)S(1)}, bf16[2,2048,256]{2,1,0:T(8,128)(2,1)S(1)}, f32[2,256,128]{2,1,0:T(8,128)S(1)}, f32[2,256,128]{2,1,0:T(8,128)S(1)}) custom-call(s32[4]{0:T(128)S(1)} %pad_add_fusion.sc_ref, bf16[256,2048]{1,0:T(8,128)(2,1)} %x_hbm.1, bf16[2048,512]{1,0:T(8,128)(2,1)} %wk_hbm.3, ...), custom_call_target="tpu_custom_call" | custom-call | flops 536870912 | tf_op jit(solution)/shard_map/pallas_call | solution.py:119
  4.4 0.0 collective-permute-done.xp_ref.x_ref
  4.4 2.6 %shard_map.102 = (bf16[2,2,256,128]{3,2,1,0:T(8,128)(2,1)S(1)}, bf16[2,2048,256]{2,1,0:T(8,128)(2,1)S(1)}) custom-call(s32[4]{0:T(128)S(1)} %pad_add_fusion.sc_ref, bf16[256,2048]{1,0:T(8,128)(2,1)S(1)} %collective-permute-done.xp_ref.x_ref, bf16[2,2048,256]{2,1,0:T(8,128)(2,1)S(1)} %get-tuple-element.33.w_ref, ...), custom_call_target="tpu_custom_call" | custom-call | flops 536870912 | tf_op jit(solution)/shard_map/pallas_call | solution.py:119
  7.0 1.5 %shard_map.104 = bf16[2,2,256,128]{3,2,1,0:T(8,128)(2,1)S(1)} custom-call(s32[4]{0:T(128)S(1)} %pad_add_fusion.sc_ref, bf16[256,2048]{1,0:T(8,128)(2,1)S(1)} %collective-permute-done.xp_ref.x_ref, bf16[2,2048,256]{2,1,0:T(8,128)(2,1)S(1)} %get-tuple-element.35.w_ref, f32[2,256,128]{2,1,0:T(8,128)S(1)} %get-tuple-element.27.cos_ref, ...), custom_call_target="tpu_custom_call" | custom-call | flops 536870912 | tf_op jit(solution)/shard_map/pallas_call | solution.py:119
  8.5 0.0 copy-start.1
  8.6 2.6 %collective-permute-start.3 = (bf16[2,2,256,128]{3,2,1,0:T(8,128)(2,1)S(1)}, bf16[2,2,256,128]{3,2,1,0:T(8,128)(2,1)S(1)}, u32[]{:S(2)}, u32[]{:S(2)}) collective-permute-start(bf16[2,2,256,128]{3,2,1,0:T(8,128)(2,1)S(1)} %shard_map.104), channel_id=1, source_target_pairs={{0,2},{2,0},{4,6},{6,4},{8,10},{10,8},{12,14},{14,12},{1,3},{3,1},... | collective-permute-start | bytes 786440 | tf_op jit(solution)/shard_map/ppermute | solution.py:372
  11.1 3.5 %collective-permute-start.4 = (bf16[2,2,256,128]{3,2,1,0:T(8,128)(2,1)S(1)}, bf16[2,2,256,128]{3,2,1,0:T(8,128)(2,1)S(1)}, u32[]{:S(2)}, u32[]{:S(2)}) collective-permute-start(bf16[2,2,256,128]{3,2,1,0:T(8,128)(2,1)S(1)} %get-tuple-element.32.kva_ref), channel_id=1, source_target_pairs={{0,4},{2,6},{4,8},{6,10},{8,12},{10,14},{1,5},{3,7},{5,9},{7,11},{... | collective-permute-start | bytes 786440 | tf_op jit(solution)/shard_map/ppermute | solution.py:377
  14.6 1.5 %shard_map.103 = bf16[2,2,256,128]{3,2,1,0:T(8,128)(2,1)S(1)} custom-call(s32[4]{0:T(128)S(1)} %pad_add_fusion.sc_ref, bf16[256,2048]{1,0:T(8,128)(2,1)S(1)} %get-tuple-element.26.xo_ref.x_ref, bf16[2,2048,256]{2,1,0:T(8,128)(2,1)S(1)} %get-tuple-element.35.w_ref, f32[2,256,128]{2,1,0:T(8,128)S(1)} %get-tuple-element.27.cos_ref, ...), custom_call_target="tpu_custom_call" | custom-call | flops 536870912 | tf_op jit(solution)/shard_map/pallas_call | solution.py:119
  16.1 0.7 collective-permute-start.2
  16.8 3.5 %collective-permute-start.5 = (bf16[2,2,256,128]{3,2,1,0:T(8,128)(2,1)S(1)}, bf16[2,2,256,128]{3,2,1,0:T(8,128)(2,1)S(1)}, u32[]{:S(2)}, u32[]{:S(2)}) collective-permute-start(bf16[2,2,256,128]{3,2,1,0:T(8,128)(2,1)S(1)} %get-tuple-element.34.kvb_ref), channel_id=1, source_target_pairs={{0,4},{2,6},{4,8},{6,10},{8,12},{10,14},{1,5},{3,7},{5,9},{7,11},{... | collective-permute-start | bytes 786440 | tf_op jit(solution)/shard_map/ppermute | solution.py:377
  20.3 0.0 collective-permute-done.3.kvyb_ref
  20.3 3.5 %collective-permute-start.7 = (bf16[2,2,256,128]{3,2,1,0:T(8,128)(2,1)S(1)}, bf16[2,2,256,128]{3,2,1,0:T(8,128)(2,1)S(1)}, u32[]{:S(2)}, u32[]{:S(2)}) collective-permute-start(bf16[2,2,256,128]{3,2,1,0:T(8,128)(2,1)S(1)} %collective-permute-done.3.kvyb_ref), channel_id=1, source_target_pairs={{0,4},{2,6},{4,8},{6,10},{8,12},{10,14},{1,5},{3,7},{5,9},{7,11},{... | collective-permute-start | bytes 786440 | tf_op jit(solution)/shard_map/ppermute | solution.py:377
  23.8 0.0 collective-permute-done.4.kva_ref
  23.8 1.9 %collective-permute-start.8 = (bf16[2,2,256,128]{3,2,1,0:T(8,128)(2,1)S(1)}, bf16[2,2,256,128]{3,2,1,0:T(8,128)(2,1)S(1)}, u32[]{:S(2)}, u32[]{:S(2)}) collective-permute-start(bf16[2,2,256,128]{3,2,1,0:T(8,128)(2,1)S(1)} %collective-permute-done.4.kva_ref), channel_id=1, source_target_pairs={{0,4},{2,6},{4,8},{6,10},{8,12},{10,14},{1,5},{3,7},{5,9},{7,11},{... | collective-permute-start | bytes 786440 | tf_op jit(solution)/shard_map/ppermute | solution.py:377
  25.7 0.0 collective-permute-done.2.kvya_ref
  25.7 3.5 %collective-permute-start.6 = (bf16[2,2,256,128]{3,2,1,0:T(8,128)(2,1)S(1)}, bf16[2,2,256,128]{3,2,1,0:T(8,128)(2,1)S(1)}, u32[]{:S(2)}, u32[]{:S(2)}) collective-permute-start(bf16[2,2,256,128]{3,2,1,0:T(8,128)(2,1)S(1)} %collective-permute-done.2.kvya_ref), channel_id=1, source_target_pairs={{0,4},{2,6},{4,8},{6,10},{8,12},{10,14},{1,5},{3,7},{5,9},{7,11},{... | collective-permute-start | bytes 786440 | tf_op jit(solution)/shard_map/ppermute | solution.py:377
  29.3 0.0 copy-done.1
  29.3 2.4 %shard_map.101 = (bf16[2,256,128]{2,1,0:T(8,128)(2,1)S(1)}, bf16[2,256,128]{2,1,0:T(8,128)(2,1)S(1)}, bf16[2,512,128]{2,1,0:T(8,128)(2,1)S(1)}) custom-call(s32[4]{0:T(128)S(1)} %pad_add_fusion.sc_ref, bf16[256,2048]{1,0:T(8,128)(2,1)S(1)} %get-tuple-element.26.xo_ref.x_ref, bf16[256,2048]{1,0:T(8,128)(2,1)S(1)} %collective-permute-done.xp_ref.x_ref, ...), custom_call_target="tpu_custom_call" | custom-call | flops 1073741824 | tf_op jit(solution)/shard_map/pallas_call | solution.py:119
  31.7 0.0 copy-start.3
  31.7 0.0 copy-start.5
  31.7 0.0 copy-start.6
  31.7 1.6 %collective-permute-start.1 = (bf16[2,512,128]{2,1,0:T(8,128)(2,1)S(1)}, bf16[2,512,128]{2,1,0:T(8,128)(2,1)S(1)}, u32[]{:S(2)}, u32[]{:S(2)}) collective-permute-start(bf16[2,512,128]{2,1,0:T(8,128)(2,1)S(1)} %get-tuple-element.31), channel_id=1, source_target_pairs={{0,2},{2,0},{4,6},{6,4},{8,10},{10,8},{12,14},{14,12},{1,3},{3,1},... | collective-permute-start | bytes 786440 | tf_op jit(solution)/shard_map/ppermute | solution.py:372
  33.3 0.0 collective-permute-done.5.kvb_ref
  33.3 2.5 %collective-permute-start.9 = (bf16[2,2,256,128]{3,2,1,0:T(8,128)(2,1)S(1)}, bf16[2,2,256,128]{3,2,1,0:T(8,128)(2,1)S(1)}, u32[]{:S(2)}, u32[]{:S(2)}) collective-permute-start(bf16[2,2,256,128]{3,2,1,0:T(8,128)(2,1)S(1)} %collective-permute-done.5.kvb_ref), channel_id=1, source_target_pairs={{0,4},{2,6},{4,8},{6,10},{8,12},{10,14},{1,5},{3,7},{5,9},{7,11},{... | collective-permute-start | bytes 786440 | tf_op jit(solution)/shard_map/ppermute | solution.py:377
  35.8 0.0 collective-permute-done.7.kvyb_ref
  35.8 8.0 %collective-permute-done.6.kvya_ref = bf16[2,2,256,128]{3,2,1,0:T(8,128)(2,1)S(1)} collective-permute-done((bf16[2,2,256,128]{3,2,1,0:T(8,128)(2,1)S(1)}, bf16[2,2,256,128]{3,2,1,0:T(8,128)(2,1)S(1)}, u32[]{:S(2)}, u32[]{:S(2)}) %collective-permute-start.6) | collective-permute-done | bytes 262176 | tf_op jit(solution)/shard_map/ppermute | solution.py:377
  43.9 4.4 %collective-permute-start.10 = (bf16[2,2,256,128]{3,2,1,0:T(8,128)(2,1)S(1)}, bf16[2,2,256,128]{3,2,1,0:T(8,128)(2,1)S(1)}, u32[]{:S(2)}, u32[]{:S(2)}) collective-permute-start(bf16[2,2,256,128]{3,2,1,0:T(8,128)(2,1)S(1)} %pad_maximum_fusion), channel_id=1, source_target_pairs={{0,4},{2,6},{4,8},{6,10},{8,12},{10,14},{1,5},{3,7},{5,9},{7,11},{... | collective-permute-start | bytes 786440 | tf_op jit(solution)/shard_map/ppermute | solution.py:377
  48.3 3.5 %collective-permute-start.14 = (bf16[2,2,256,128]{3,2,1,0:T(8,128)(2,1)S(1)}, bf16[2,2,256,128]{3,2,1,0:T(8,128)(2,1)S(1)}, u32[]{:S(2)}, u32[]{:S(2)}) collective-permute-start(bf16[2,2,256,128]{3,2,1,0:T(8,128)(2,1)S(1)} %pad_maximum_fusion.1), channel_id=1, source_target_pairs={{0,4},{2,6},{4,8},{6,10},{8,12},{10,14},{1,5},{3,7},{5,9},{7,11},{... | collective-permute-start | bytes 786440 | tf_op jit(solution)/shard_map/ppermute | solution.py:377
  51.8 0.0 collective-permute-done.1.qy_ref
  51.8 0.0 copy-done.3
  51.8 0.0 copy-done.5
  51.8 0.0 copy-done.6
  51.8 0.0 copy-start.4
  51.9 3.5 %shard_map.105 = (bf16[2,1024,128]{2,1,0:T(8,128)(2,1)S(1)}, f32[2,1024,128]{2,1,0:T(8,128)S(1)}, f32[2,1024,128]{2,1,0:T(8,128)S(1)}, f32[2,1024,128]{2,1,0:T(8,128)S(1)}) custom-call(s32[4]{0:T(128)S(1)} %pad_add_fusion.sc_ref, bf16[2,256,128]{2,1,0:T(8,128)(2,1)S(1)} %get-tuple-element.29.qa_ref, bf16[2,256,128]{2,1,0:T(8,128)(2,1)S(1)} %get-tuple-element.30.qb_ref, ...), custom_call_target="tpu_custom_call" | custom-call | flops 3000000000 | tf_op jit(solution)/shard_map/pallas_call | solution.py:119
  55.4 0.0 copy-done.4
  55.4 0.0 copy-start.2
  55.4 0.6 shard_map.106
  55.9 0.0 collective-permute-done.8.kva_ref
  56.0 0.0 collective-permute-done.9.kvb_ref
  56.0 3.9 %collective-permute-done.14.kvy_ref = bf16[2,2,256,128]{3,2,1,0:T(8,128)(2,1)S(1)} collective-permute-done((bf16[2,2,256,128]{3,2,1,0:T(8,128)(2,1)S(1)}, bf16[2,2,256,128]{3,2,1,0:T(8,128)(2,1)S(1)}, u32[]{:S(2)}, u32[]{:S(2)}) %collective-permute-start.14) | collective-permute-done | bytes 262176 | tf_op jit(solution)/shard_map/ppermute | solution.py:377
  59.9 0.0 copy-done.2
  59.9 0.9 %shard_map.108 = (bf16[512,128]{1,0:T(8,128)(2,1)S(1)}, bf16[512,128]{1,0:T(8,128)(2,1)S(1)}) custom-call(s32[4]{0:T(128)S(1)} %pad_add_fusion.sc_ref, bf16[2,1024,128]{2,1,0:T(8,128)(2,1)S(1)} %get-tuple-element.36.q_ref, f32[2,1024,128]{2,1,0:T(8,128)S(1)} %get-tuple-element.40.m_ref, f32[2,1024,128]{2,1,0:T(8,128)S(1)} %get-tuple-element.41.l_ref, ...), custom_call_target="tpu_custom_call" | custom-call | flops 1000000000 | tf_op jit(solution)/shard_map/pallas_call | solution.py:119
  60.7 0.0 copy-start
  60.7 1.0 %collective-permute-start.15 = (bf16[512,128]{1,0:T(8,128)(2,1)S(1)}, bf16[512,128]{1,0:T(8,128)(2,1)S(1)}, u32[]{:S(2)}, u32[]{:S(2)}) collective-permute-start(bf16[512,128]{1,0:T(8,128)(2,1)S(1)} %get-tuple-element.46), channel_id=1, source_target_pairs={{0,2},{2,0},{4,6},{6,4},{8,10},{10,8},{12,14},{14,12},{1,3},{3,1},... | collective-permute-start | bytes 393224 | tf_op jit(solution)/shard_map/ppermute | solution.py:372
  61.7 0.0 collective-permute-done.10.kvy_ref
  61.7 0.9 %shard_map.107 = (bf16[512,128]{1,0:T(8,128)(2,1)S(1)}, bf16[512,128]{1,0:T(8,128)(2,1)S(1)}) custom-call(s32[4]{0:T(128)S(1)} %pad_add_fusion.sc_ref, bf16[2,1024,128]{2,1,0:T(8,128)(2,1)S(1)} %get-tuple-element.36.q_ref, f32[2,1024,128]{2,1,0:T(8,128)S(1)} %get-tuple-element.40.m_ref, f32[2,1024,128]{2,1,0:T(8,128)S(1)} %get-tuple-element.41.l_ref, ...), custom_call_target="tpu_custom_call" | custom-call | flops 1000000000 | tf_op jit(solution)/shard_map/pallas_call | solution.py:119
  62.6 1.2 %collective-permute-start.11 = (bf16[512,128]{1,0:T(8,128)(2,1)S(1)}, bf16[512,128]{1,0:T(8,128)(2,1)S(1)}, u32[]{:S(2)}, u32[]{:S(2)}) collective-permute-start(bf16[512,128]{1,0:T(8,128)(2,1)S(1)} %get-tuple-element.44), channel_id=1, source_target_pairs={{0,2},{2,0},{4,6},{6,4},{8,10},{10,8},{12,14},{14,12},{1,3},{3,1},... | collective-permute-start | bytes 393224 | tf_op jit(solution)/shard_map/ppermute | solution.py:372
  63.8 0.0 collective-permute-start.16
  63.8 3.1 %collective-permute-done.15.b_ref = bf16[512,128]{1,0:T(8,128)(2,1)S(1)} collective-permute-done((bf16[512,128]{1,0:T(8,128)(2,1)S(1)}, bf16[512,128]{1,0:T(8,128)(2,1)S(1)}, u32[]{:S(2)}, u32[]{:S(2)}) %collective-permute-start.15) | collective-permute-done | bytes 131104 | tf_op jit(solution)/shard_map/ppermute | solution.py:372
  66.9 0.0 collective-permute-start.17
  66.9 0.5 collective-permute-start.12
  67.4 0.9 %collective-permute-done.11.b_ref = bf16[512,128]{1,0:T(8,128)(2,1)S(1)} collective-permute-done((bf16[512,128]{1,0:T(8,128)(2,1)S(1)}, bf16[512,128]{1,0:T(8,128)(2,1)S(1)}, u32[]{:S(2)}, u32[]{:S(2)}) %collective-permute-start.11) | collective-permute-done | bytes 131104 | tf_op jit(solution)/shard_map/ppermute | solution.py:372
  68.3 0.0 collective-permute-start.13
  68.3 0.0 collective-permute-done.16.c_ref
  68.3 0.0 collective-permute-done.17.d_ref
  68.3 0.0 copy-done
  68.3 1.3 %shard_map.109.t_ref = f32[512,1024]{1,0:T(8,128)S(1)} custom-call(s32[4]{0:T(128)S(1)} %pad_add_fusion.sc_ref, bf16[512,128]{1,0:T(8,128)(2,1)S(1)} %get-tuple-element.45.a_ref, bf16[512,128]{1,0:T(8,128)(2,1)S(1)} %collective-permute-done.15.b_ref, bf16[512,128]{1,0:T(8,128)(2,1)S(1)} %collective-permute-done.16.c_ref, ...), custom_call_target="tpu_custom_call" | custom-call | flops 536870912 | tf_op jit(solution)/shard_map/pallas_call | solution.py:119
  69.6 0.0 collective-permute-done.12.c_ref
  69.6 0.1 collective-permute-done.13.d_ref
  69.7 2.3 %out_last.1 = bf16[512,1024]{1,0:T(8,128)(2,1)} custom-call(s32[4]{0:T(128)S(1)} %pad_add_fusion.sc_ref, bf16[512,128]{1,0:T(8,128)(2,1)S(1)} %get-tuple-element.43.a_ref, bf16[512,128]{1,0:T(8,128)(2,1)S(1)} %collective-permute-done.11.b_ref, bf16[512,128]{1,0:T(8,128)(2,1)S(1)} %collective-permute-done.12.c_ref, ...), custom_call_target="tpu_custom_call" | custom-call | flops 536870912 | tf_op jit(solution)/shard_map/out_last/pallas_call | solution.py:359
  (5 shorter events, 0.1 us)
Async XLA Ops:
  0.0 4.4 %collective-permute-start = (bf16[256,2048]{1,0:T(8,128)(2,1)}, bf16[256,2048]{1,0:T(8,128)(2,1)S(1)}, u32[]{:S(2)}, u32[]{:S(2)}) collective-permute-start(bf16[256,2048]{1,0:T(8,128)(2,1)} %x_hbm.1), channel_id=1, source_target_pairs={{0,1},{1,0},{2,3},{3,2},{4,5},{5,4},{6,7},{7,6},{8,9},{9,8},{10,11... | collective-permute-start | bytes 3145736 | tf_op jit(solution)/shard_map/ppermute | solution.py:372
  8.5 20.7 %copy-start.1 = (bf16[2048,512]{1,0:T(8,128)(2,1)S(1)}, bf16[2048,512]{1,0:T(8,128)(2,1)}, u32[]{:S(2)}) copy-start(bf16[2048,512]{1,0:T(8,128)(2,1)} %w_ref.3) | copy-start | bytes 6291460
  8.6 11.8 %collective-permute-start.3 = (bf16[2,2,256,128]{3,2,1,0:T(8,128)(2,1)S(1)}, bf16[2,2,256,128]{3,2,1,0:T(8,128)(2,1)S(1)}, u32[]{:S(2)}, u32[]{:S(2)}) collective-permute-start(bf16[2,2,256,128]{3,2,1,0:T(8,128)(2,1)S(1)} %shard_map.104), channel_id=1, source_target_pairs={{0,2},{2,0},{4,6},{6,4},{8,10},{10,8},{12,14},{14,12},{1,3},{3,1},... | collective-permute-start | bytes 786440 | tf_op jit(solution)/shard_map/ppermute | solution.py:372
  11.1 12.7 %collective-permute-start.4 = (bf16[2,2,256,128]{3,2,1,0:T(8,128)(2,1)S(1)}, bf16[2,2,256,128]{3,2,1,0:T(8,128)(2,1)S(1)}, u32[]{:S(2)}, u32[]{:S(2)}) collective-permute-start(bf16[2,2,256,128]{3,2,1,0:T(8,128)(2,1)S(1)} %get-tuple-element.32.kva_ref), channel_id=1, source_target_pairs={{0,4},{2,6},{4,8},{6,10},{8,12},{10,14},{1,5},{3,7},{5,9},{7,11},{... | collective-permute-start | bytes 786440 | tf_op jit(solution)/shard_map/ppermute | solution.py:377
  16.1 9.6 %collective-permute-start.2 = (bf16[2,2,256,128]{3,2,1,0:T(8,128)(2,1)S(1)}, bf16[2,2,256,128]{3,2,1,0:T(8,128)(2,1)S(1)}, u32[]{:S(2)}, u32[]{:S(2)}) collective-permute-start(bf16[2,2,256,128]{3,2,1,0:T(8,128)(2,1)S(1)} %shard_map.103), channel_id=1, source_target_pairs={{0,2},{2,0},{4,6},{6,4},{8,10},{10,8},{12,14},{14,12},{1,3},{3,1},... | collective-permute-start | bytes 786440 | tf_op jit(solution)/shard_map/ppermute | solution.py:372
  16.8 16.5 %collective-permute-start.5 = (bf16[2,2,256,128]{3,2,1,0:T(8,128)(2,1)S(1)}, bf16[2,2,256,128]{3,2,1,0:T(8,128)(2,1)S(1)}, u32[]{:S(2)}, u32[]{:S(2)}) collective-permute-start(bf16[2,2,256,128]{3,2,1,0:T(8,128)(2,1)S(1)} %get-tuple-element.34.kvb_ref), channel_id=1, source_target_pairs={{0,4},{2,6},{4,8},{6,10},{8,12},{10,14},{1,5},{3,7},{5,9},{7,11},{... | collective-permute-start | bytes 786440 | tf_op jit(solution)/shard_map/ppermute | solution.py:377
  20.3 15.5 %collective-permute-start.7 = (bf16[2,2,256,128]{3,2,1,0:T(8,128)(2,1)S(1)}, bf16[2,2,256,128]{3,2,1,0:T(8,128)(2,1)S(1)}, u32[]{:S(2)}, u32[]{:S(2)}) collective-permute-start(bf16[2,2,256,128]{3,2,1,0:T(8,128)(2,1)S(1)} %collective-permute-done.3.kvyb_ref), channel_id=1, source_target_pairs={{0,4},{2,6},{4,8},{6,10},{8,12},{10,14},{1,5},{3,7},{5,9},{7,11},{... | collective-permute-start | bytes 786440 | tf_op jit(solution)/shard_map/ppermute | solution.py:377
  23.8 32.1 %collective-permute-start.8 = (bf16[2,2,256,128]{3,2,1,0:T(8,128)(2,1)S(1)}, bf16[2,2,256,128]{3,2,1,0:T(8,128)(2,1)S(1)}, u32[]{:S(2)}, u32[]{:S(2)}) collective-permute-start(bf16[2,2,256,128]{3,2,1,0:T(8,128)(2,1)S(1)} %collective-permute-done.4.kva_ref), channel_id=1, source_target_pairs={{0,4},{2,6},{4,8},{6,10},{8,12},{10,14},{1,5},{3,7},{5,9},{7,11},{... | collective-permute-start | bytes 786440 | tf_op jit(solution)/shard_map/ppermute | solution.py:377
  25.7 18.1 %collective-permute-start.6 = (bf16[2,2,256,128]{3,2,1,0:T(8,128)(2,1)S(1)}, bf16[2,2,256,128]{3,2,1,0:T(8,128)(2,1)S(1)}, u32[]{:S(2)}, u32[]{:S(2)}) collective-permute-start(bf16[2,2,256,128]{3,2,1,0:T(8,128)(2,1)S(1)} %collective-permute-done.2.kvya_ref), channel_id=1, source_target_pairs={{0,4},{2,6},{4,8},{6,10},{8,12},{10,14},{1,5},{3,7},{5,9},{7,11},{... | collective-permute-start | bytes 786440 | tf_op jit(solution)/shard_map/ppermute | solution.py:377
  31.7 20.1 %copy-start.3 = (f32[256,256]{1,0:T(8,128)S(1)}, f32[256,256]{1,0:T(8,128)}, u32[]{:S(2)}) copy-start(f32[256,256]{1,0:T(8,128)} %constant.49.clone.near1_ref.near_ref) | copy-start | bytes 786436
  31.7 20.1 %copy-start.5 = (f32[256,256]{1,0:T(8,128)S(1)}, f32[256,256]{1,0:T(8,128)}, u32[]{:S(2)}) copy-start(f32[256,256]{1,0:T(8,128)} %constant.47.clone.group_ref) | copy-start | bytes 786436
  31.7 20.1 %copy-start.6 = (f32[256,256]{1,0:T(8,128)S(1)}, f32[256,256]{1,0:T(8,128)}, u32[]{:S(2)}) copy-start(f32[256,256]{1,0:T(8,128)} %constant.48.clone.near0_ref) | copy-start | bytes 786436
  31.7 20.1 %collective-permute-start.1 = (bf16[2,512,128]{2,1,0:T(8,128)(2,1)S(1)}, bf16[2,512,128]{2,1,0:T(8,128)(2,1)S(1)}, u32[]{:S(2)}, u32[]{:S(2)}) collective-permute-start(bf16[2,512,128]{2,1,0:T(8,128)(2,1)S(1)} %get-tuple-element.31), channel_id=1, source_target_pairs={{0,2},{2,0},{4,6},{6,4},{8,10},{10,8},{12,14},{14,12},{1,3},{3,1},... | collective-permute-start | bytes 786440 | tf_op jit(solution)/shard_map/ppermute | solution.py:372
  33.3 22.7 %collective-permute-start.9 = (bf16[2,2,256,128]{3,2,1,0:T(8,128)(2,1)S(1)}, bf16[2,2,256,128]{3,2,1,0:T(8,128)(2,1)S(1)}, u32[]{:S(2)}, u32[]{:S(2)}) collective-permute-start(bf16[2,2,256,128]{3,2,1,0:T(8,128)(2,1)S(1)} %collective-permute-done.5.kvb_ref), channel_id=1, source_target_pairs={{0,4},{2,6},{4,8},{6,10},{8,12},{10,14},{1,5},{3,7},{5,9},{7,11},{... | collective-permute-start | bytes 786440 | tf_op jit(solution)/shard_map/ppermute | solution.py:377
  43.9 17.8 %collective-permute-start.10 = (bf16[2,2,256,128]{3,2,1,0:T(8,128)(2,1)S(1)}, bf16[2,2,256,128]{3,2,1,0:T(8,128)(2,1)S(1)}, u32[]{:S(2)}, u32[]{:S(2)}) collective-permute-start(bf16[2,2,256,128]{3,2,1,0:T(8,128)(2,1)S(1)} %pad_maximum_fusion), channel_id=1, source_target_pairs={{0,4},{2,6},{4,8},{6,10},{8,12},{10,14},{1,5},{3,7},{5,9},{7,11},{... | collective-permute-start | bytes 786440 | tf_op jit(solution)/shard_map/ppermute | solution.py:377
  48.3 11.5 %collective-permute-start.14 = (bf16[2,2,256,128]{3,2,1,0:T(8,128)(2,1)S(1)}, bf16[2,2,256,128]{3,2,1,0:T(8,128)(2,1)S(1)}, u32[]{:S(2)}, u32[]{:S(2)}) collective-permute-start(bf16[2,2,256,128]{3,2,1,0:T(8,128)(2,1)S(1)} %pad_maximum_fusion.1), channel_id=1, source_target_pairs={{0,4},{2,6},{4,8},{6,10},{8,12},{10,14},{1,5},{3,7},{5,9},{7,11},{... | collective-permute-start | bytes 786440 | tf_op jit(solution)/shard_map/ppermute | solution.py:377
  51.8 3.5 %copy-start.4 = (f32[256,256]{1,0:T(8,128)S(1)}, f32[256,256]{1,0:T(8,128)}, u32[]{:S(2)}) copy-start(f32[256,256]{1,0:T(8,128)} %constant.50.clone.group_ref) | copy-start | bytes 786436
  55.4 4.5 %copy-start.2 = (f32[128,128]{1,0:T(8,128)S(1)}, f32[128,128]{1,0:T(8,128)}, u32[]{:S(2)}) copy-start(f32[128,128]{1,0:T(8,128)} %constant.51.clone.pair_ref) | copy-start | bytes 196612
  60.7 7.6 %copy-start = (bf16[1024,1024]{1,0:T(8,128)(2,1)S(1)}, bf16[1024,1024]{1,0:T(8,128)(2,1)}, u32[]{:S(2)}) copy-start(bf16[1024,1024]{1,0:T(8,128)(2,1)} %w_ref.5) | copy-start | bytes 6291460
  60.7 6.2 %collective-permute-start.15 = (bf16[512,128]{1,0:T(8,128)(2,1)S(1)}, bf16[512,128]{1,0:T(8,128)(2,1)S(1)}, u32[]{:S(2)}, u32[]{:S(2)}) collective-permute-start(bf16[512,128]{1,0:T(8,128)(2,1)S(1)} %get-tuple-element.46), channel_id=1, source_target_pairs={{0,2},{2,0},{4,6},{6,4},{8,10},{10,8},{12,14},{14,12},{1,3},{3,1},... | collective-permute-start | bytes 393224 | tf_op jit(solution)/shard_map/ppermute | solution.py:372
  62.6 5.8 %collective-permute-start.11 = (bf16[512,128]{1,0:T(8,128)(2,1)S(1)}, bf16[512,128]{1,0:T(8,128)(2,1)S(1)}, u32[]{:S(2)}, u32[]{:S(2)}) collective-permute-start(bf16[512,128]{1,0:T(8,128)(2,1)S(1)} %get-tuple-element.44), channel_id=1, source_target_pairs={{0,2},{2,0},{4,6},{6,4},{8,10},{10,8},{12,14},{14,12},{1,3},{3,1},... | collective-permute-start | bytes 393224 | tf_op jit(solution)/shard_map/ppermute | solution.py:372
  63.8 4.6 %collective-permute-start.16 = (bf16[512,128]{1,0:T(8,128)(2,1)S(1)}, bf16[512,128]{1,0:T(8,128)(2,1)S(1)}, u32[]{:S(2)}, u32[]{:S(2)}) collective-permute-start(bf16[512,128]{1,0:T(8,128)(2,1)S(1)} %get-tuple-element.45.a_ref), channel_id=1, source_target_pairs={{0,1},{1,0},{2,3},{3,2},{4,5},{5,4},{6,7},{7,6},{8,9},{9,8},{10,11... | collective-permute-start | bytes 393224 | tf_op jit(solution)/shard_map/ppermute | solution.py:372
  66.9 1.4 %collective-permute-start.17 = (bf16[512,128]{1,0:T(8,128)(2,1)S(1)}, bf16[512,128]{1,0:T(8,128)(2,1)S(1)}, u32[]{:S(2)}, u32[]{:S(2)}) collective-permute-start(bf16[512,128]{1,0:T(8,128)(2,1)S(1)} %collective-permute-done.15.b_ref), channel_id=1, source_target_pairs={{0,1},{1,0},{2,3},{3,2},{4,5},{5,4},{6,7},{7,6},{8,9},{9,8},{10,11... | collective-permute-start | bytes 393224 | tf_op jit(solution)/shard_map/ppermute | solution.py:372
  66.9 2.7 %collective-permute-start.12 = (bf16[512,128]{1,0:T(8,128)(2,1)S(1)}, bf16[512,128]{1,0:T(8,128)(2,1)S(1)}, u32[]{:S(2)}, u32[]{:S(2)}) collective-permute-start(bf16[512,128]{1,0:T(8,128)(2,1)S(1)} %get-tuple-element.43.a_ref), channel_id=1, source_target_pairs={{0,1},{1,0},{2,3},{3,2},{4,5},{5,4},{6,7},{7,6},{8,9},{9,8},{10,11... | collective-permute-start | bytes 393224 | tf_op jit(solution)/shard_map/ppermute | solution.py:372
  68.3 1.3 %collective-permute-start.13 = (bf16[512,128]{1,0:T(8,128)(2,1)S(1)}, bf16[512,128]{1,0:T(8,128)(2,1)S(1)}, u32[]{:S(2)}, u32[]{:S(2)}) collective-permute-start(bf16[512,128]{1,0:T(8,128)(2,1)S(1)} %collective-permute-done.11.b_ref), channel_id=1, source_target_pairs={{0,1},{1,0},{2,3},{3,2},{4,5},{5,4},{6,7},{7,6},{8,9},{9,8},{10,11... | collective-permute-start | bytes 393224 | tf_op jit(solution)/shard_map/ppermute | solution.py:372

commit v2 on v1

--- a/solution.py
+++ b/solution.py
@@ -14,6 +14,7 @@
 FAR_DILATION = 16
 THETA_BASE = 500000.0
 TILE = 16
+RELAYED = 1
 MASKED = -1e30
 SCALE = HEAD ** -0.5 * 1.4426950408889634
 F32 = jnp.float32
@@ -37,12 +38,12 @@
         out_ref[lead + (pl.ds(at, nq_half), slice(None))] = piece.astype(BF16)
 
 
-def kv_part(x_ref, w_ref, out_ref, cos_ref, sin_ref, buf_ref, ready=None):
+def kv_part(x_ref, w_refs, out_ref, cos_ref, sin_ref, buf_ref, ready=None):
     slot = 0
     for which in (1, 0):
         if ready is not None:
             ready[which].wait()
-        acc = jnp.dot(x_ref[...], w_ref[which], preferred_element_type=F32)
+        acc = jnp.dot(x_ref[...], w_refs[which][...], preferred_element_type=F32)
         for h in range(acc.shape[1] // HEAD):
             val = acc[:, h * HEAD:(h + 1) * HEAD]
             if which == 0:
@@ -66,7 +67,6 @@
     copies = weight_copies(wk_hbm, wv_hbm, w_ref, par, sems)
     x_copy.start()
     copies[1].start()
-    copies[0].start()
     steps = half // FAR_DILATION
     lane = lax.broadcasted_iota(jnp.int32, (2 * steps, HEAD), 1)
     row = lax.broadcasted_iota(jnp.int32, (2 * steps, HEAD), 0)
@@ -80,23 +80,22 @@
     cos_ref[...] = (cos_c * cos_f - sin_c * sin_f).reshape(2, half, HEAD)
     sin_ref[...] = ((sin_c * cos_f + cos_c * sin_f) * sign).reshape(2, half, HEAD)
     x_copy.wait()
-    kv_part(x_ref, w_ref, out_ref, cos_ref.at[0], sin_ref.at[0], buf_ref, copies)
-
-
-def rest_keep_kernel(sc_ref, x_ref, w_ref, cos_ref, sin_ref, wk_hbm, wv_hbm, out_ref, w_send_ref, buf_ref, sems):
-    copies = weight_copies(wk_hbm, wv_hbm, w_send_ref, 1 - sc_ref[1], sems)
-    for copy in copies:
-        copy.start()
-    kv_part(x_ref, w_ref, out_ref, cos_ref.at[1], sin_ref.at[1], buf_ref)
-    for copy in copies:
-        copy.wait()
-
-
-def send_kernel(sc_ref, x_ref, w_ref, cos_ref, sin_ref, out_ref, buf_ref, *, part):
-    kv_part(x_ref, w_ref, out_ref, cos_ref.at[part], sin_ref.at[part], buf_ref)
-
-
-def q_kernel(sc_ref, xo_ref, xp_ref, cos_ref, sin_ref, w_ref, keepa_ref, keepb_ref, send_ref, buf_ref):
+    copies[0].start()
+    kv_part(x_ref, (w_ref.at[0], w_ref.at[1]), out_ref, cos_ref.at[0], sin_ref.at[0], buf_ref, copies)
+
+
+def rest_keep_kernel(sc_ref, x_ref, w_ref, cos_ref, sin_ref, out_ref, buf_ref):
+    kv_part(x_ref, (w_ref.at[0], w_ref.at[1]), out_ref, cos_ref.at[1], sin_ref.at[1], buf_ref)
+
+
+def send_kernel(sc_ref, x_ref, wk_ref, wv_ref, cos_ref, sin_ref, out_ref, buf_ref, *, part):
+    width = out_ref.shape[0] * HEAD
+    column = pl.ds(pl.multiple_of((1 - sc_ref[1]) * width, width), width)
+    kv_part(x_ref, (wk_ref.at[:, column], wv_ref.at[:, column]), out_ref, cos_ref.at[part], sin_ref.at[part], buf_ref)
+
+
+def q_kernel(sc_ref, xo_ref, xp_ref, cos_ref, sin_ref, w_ref, keepa_ref, keepb_ref, send_ref,
+             back_ref, buf_ref):
     tp, par = sc_ref[0], sc_ref[1]
     heads = send_ref.shape[0]
     width = heads * HEAD
@@ -111,6 +110,8 @@
                     place(send_ref, (h,), val, buf_ref, slot, tp if part == 0 else 1 - tp)
                 else:
                     place((keepa_ref, keepb_ref)[part], (h,), val, buf_ref, slot, None)
+                if h >= RELAYED and not side:
+                    place(back_ref, (h - RELAYED, part), val, buf_ref, slot, None)
                 slot += 1
 
 
@@ -262,7 +263,7 @@
 
 
 def one_kernel(sc_ref, q_ref, m_in, l_in, o_in, kva_ref, kvb_ref, kvya_ref, kvyb_ref, group_ref, near_ref,
-               m_ref, l_ref, o_ref, k_s, v_s, s_s, n_s):
+               m_ref, l_ref, o_ref, state_ref, k_s, v_s, s_s, n_s, piece_s, stat_s):
     tp, par = sc_ref[0], sc_ref[1]
     nq = kvya_ref.shape[2] // FAR_DILATION * 2
 
@@ -294,8 +295,14 @@
             put(o, near[0], take(o, near[0]) + ol[:, :HEAD])
             put(l, near[0], take(l, near[0]) + ol[:, HEAD:])
 
-
-def two_kernel(sc_ref, q_ref, m_ref, l_ref, o_ref, kva_ref, kvb_ref, kvy_ref, pair_ref,
+    for i in range(FAR_DILATION // 2):
+        rows = pair_rows(i, nq)
+        m, l, o = (take(x.at[RELAYED], rows) for x in (m_ref, l_ref, o_ref))
+        pack_rows(piece_s, stat_s, i, o / l, m, l)
+    pack_out(state_ref, piece_s, stat_s, 1 - par)
+
+
+def two_kernel(sc_ref, q_ref, m_ref, l_ref, o_ref, kvo_ref, kvy_ref, pair_ref,
                keep_ref, send_ref, k_s, v_s, s_s, n_s, mix_s, *, head):
     tp, par = sc_ref[0], sc_ref[1]
     nq = kvy_ref.shape[2] // FAR_DILATION * 2
@@ -309,7 +316,7 @@
 
     @pl.when(sc_ref[2] >= 2)
     def _():
-        gather_kv(k_s, v_s, [kva_ref.at[head], kvb_ref.at[head], kvy_ref.at[0], kvy_ref.at[1]], nq, tp, par)
+        gather_kv(k_s, v_s, [kvo_ref.at[0], kvo_ref.at[1], kvy_ref.at[0], kvy_ref.at[1]], nq, tp, par)
         items = [(rows, rows, pair_ref[...], i * length(rows)) for i, rows in enumerate(pairs)]
         for item in items:
             put(n_s, item[0], take(m, item[0]))
@@ -329,43 +336,122 @@
     send_ref[...] = mix_s[pl.ds(1 - par, 1)][0].astype(BF16)
 
 
-def out_terms(sc_ref, x_refs, w_ref, column, block, head):
+def diagonal(n):
+    return lax.broadcasted_iota(jnp.int32, (n, n), 0) == lax.broadcasted_iota(jnp.int32, (n, n), 1)
+
+
+def pack_rows(piece_s, stat_s, i, value, top, total):
+    nq = value.shape[0] // 4
+    eye = diagonal(HEAD)
+    for part in range(4):
+        r, block = 2 * i + part // 2, part % 2
+        piece_s[block, r * nq:(r + 1) * nq, :] = value[part * nq:(part + 1) * nq].astype(BF16)
+    for which, stat in enumerate((top, total)):
+        at = which * (FAR_DILATION // 2) + i
+        stat_s[at:at + 1, :] = jnp.sum(jnp.where(eye, stat, 0.0), axis=0, keepdims=True)
+
+
+def pack_out(out_ref, piece_s, stat_s, block):
+    rows, count = piece_s.shape[1], stat_s.shape[0]
+    out_ref[:rows, :] = piece_s[pl.ds(block, 1)][0]
+    rest = stat_s[...]
+    for term in range(3):
+        low = rest.astype(BF16)
+        out_ref[rows + term * count:rows + (term + 1) * count, :] = low
+        rest = rest - low.astype(F32)
+
+
+def unpacked_stats(ref, rows):
+    return sum(ref[rows + t * FAR_DILATION:rows + (t + 1) * FAR_DILATION, :].astype(F32) for t in range(3))
+
+
+def foreign_kernel(sc_ref, qn_ref, kva_ref, kvb_ref, kvya_ref, kvyb_ref, pair_ref,
+                   own_ref, diag_ref, q_s, k_s, v_s, s_s, n_s, piece_s, stat_s, *, head):
     tp, par = sc_ref[0], sc_ref[1]
+    nq = kvya_ref.shape[2] // FAR_DILATION * 2
+    half = kvya_ref.shape[2]
+    gather(q_s, nq, [(qn_ref.at[0, :half], par, tp), (qn_ref.at[0, half:], par, 1 - tp), (qn_ref.at[1], 1 - par, None)])
+    gather_kv(k_s, v_s, [x.at[head] for x in (kva_ref, kvb_ref, kvya_ref, kvyb_ref)], nq, tp, par)
+    pairs = [pair_rows(i, nq) for i in range(FAR_DILATION // 2)]
+    items = [(rows, rows, pair_ref[...], i * length(rows)) for i, rows in enumerate(pairs)]
+    for item in items:
+        scored(item, q_s, k_s, s_s, n_s, True)
+    for i, item in enumerate(items):
+        ol = weighed(item, v_s, s_s, n_s, length(item[0]))
+        total = ol[:, HEAD:]
+        pack_rows(piece_s, stat_s, i, ol[:, :HEAD] / total, take(n_s, item[0]), total)
+    pack_out(own_ref, piece_s, stat_s, par)
+    pack_out(diag_ref, piece_s, stat_s, 1 - par)
+
+
+def final_kernel(sc_ref, m_ref, l_ref, o_ref, state_ref, own_ref, diag_ref, out_ref, mix_s, *, head):
+    par = sc_ref[1]
+    m, l, o = (x.at[head] for x in (m_ref, l_ref, o_ref))
+    rows = out_ref.shape[1]
+    nq = rows // FAR_DILATION
+    count = FAR_DILATION // 2
+    far = sc_ref[2] >= 2
+    eye = diagonal(HEAD)
+
+    def columns(ref):
+        stats = unpacked_stats(ref, rows)
+        result = []
+        for i in range(2 * count):
+            spread = jnp.sum(jnp.where(eye, stats[i:i + 1, :], 0.0), axis=1, keepdims=True)
+            result.append(jnp.broadcast_to(spread, (HEAD, HEAD)))
+        return result
+
+    def rows_of(result, which, r):
+        column = result[which * count + r // 2]
+        at = (r % 2) * 2 * nq
+        return jnp.where(par == 0, column[at:at + nq], column[at + nq:at + 2 * nq])
+
+    def joined(top, total, numerator, ref, result, r):
+        top2, total2 = rows_of(result, 0, r), rows_of(result, 1, r)
+        top2 = jnp.where(far, top2, MASKED)
+        new = jnp.maximum(top, top2)
+        keep = jnp.exp2((top - new) * SCALE)
+        add = jnp.where(far, jnp.exp2((top2 - new) * SCALE) * total2, 0.0)
+        part = jnp.where(far, ref[r * nq:(r + 1) * nq, :].astype(F32), 0.0)
+        return (numerator * keep + part * add) / (total * keep + add)
+
+    own_stats, diag_stats, state_stats = columns(own_ref), columns(diag_ref), columns(state_ref)
+    for r in range(FAR_DILATION):
+        here = pl.ds(pl.multiple_of(r * 2 * nq + par * nq, TILE), nq)
+        mix_s[0, pl.ds(r, nq, stride=FAR_DILATION), :] = joined(
+            m[here, :], l[here, :], o[here, :], own_ref, own_stats, r)
+        top, total = rows_of(state_stats, 0, r), rows_of(state_stats, 1, r)
+        mix_s[1, pl.ds(r, nq, stride=FAR_DILATION), :] = joined(
+            top, total, state_ref[r * nq:(r + 1) * nq, :].astype(F32) * total, diag_ref, diag_stats, r)
+    out_ref[...] = mix_s[...].astype(BF16)
+
+
+def out_kernel(sc_ref, a_ref, b_ref, c_ref, d_ref, own_ref, tp_ref, w_ref, o_ref):
+    tp, par = sc_ref[0], sc_ref[1]
+    block = o_ref.shape[1]
     heads = w_ref.shape[0] // HEAD // 4
+    column = pl.multiple_of(pl.program_id(0) * block, block)
     order = (2 * tp + par, 2 * tp + 1 - par, 2 * (1 - tp) + par, 2 * (1 - tp) + 1 - par)
+    x_refs = (own_ref.at[0], own_ref.at[1], tp_ref.at[0], tp_ref.at[1], a_ref, b_ref, c_ref, d_ref)
     x = jnp.concatenate([x_ref[...] for x_ref in x_refs], axis=1)
     w = jnp.concatenate([w_ref[pl.ds(pl.multiple_of((i * heads + head) * HEAD, HEAD), HEAD), pl.ds(column, block)]
-                         for i in order], axis=0)
-    return jnp.dot(x, w, preferred_element_type=F32)
-
-
-def out_first_kernel(sc_ref, a_ref, b_ref, c_ref, d_ref, w_ref, o_ref):
-    block = 2 * HEAD
-    for j in range(o_ref.shape[1] // block):
-        o_ref[:, j * block:(j + 1) * block] = out_terms(
-            sc_ref, (a_ref, b_ref, c_ref, d_ref), w_ref, j * block, block, 0)
-
-
-def out_last_kernel(sc_ref, a_ref, b_ref, c_ref, d_ref, w_ref, t_ref, o_ref):
-    block = o_ref.shape[1]
-    column = pl.multiple_of(pl.program_id(0) * block, block)
-    total = out_terms(sc_ref, (a_ref, b_ref, c_ref, d_ref), w_ref, column, block, 1)
-    o_ref[...] = (t_ref[:, pl.ds(column, block)] + total).astype(BF16)
-
-
-def out_last(scalars, parts, weight, total):
-    rows, columns = total.shape
+                         for head in (1, 0) for i in order], axis=0)
+    o_ref[...] = jnp.dot(x, w, preferred_element_type=F32).astype(BF16)
+
+
+def out_project(scalars, first, last, weight):
+    rows, columns = first[0].shape[0], weight.shape[1]
     steps = 2
     return pl.pallas_call(
-        out_last_kernel,
+        out_kernel,
         grid=(steps,),
-        in_specs=[pl.BlockSpec(memory_space=pltpu.SMEM)] + in_vmem(6),
+        in_specs=[pl.BlockSpec(memory_space=pltpu.SMEM)] + in_vmem(7),
         out_specs=pl.BlockSpec((rows, columns // steps), lambda j: (0, j)),
         out_shape=jax.ShapeDtypeStruct((rows, columns), BF16),
         compiler_params=pltpu.CompilerParams(vmem_limit_bytes=16 * 2 ** 20),
-        cost_estimate=pl.CostEstimate(flops=rows * weight.size, transcendentals=0, bytes_accessed=0),
-        name="out_last",
-    )(scalars, *parts, weight, total)
+        cost_estimate=pl.CostEstimate(flops=2 * rows * weight.size, transcendentals=0, bytes_accessed=0),
+        name="out_project",
+    )(scalars, *first, *last, weight)
 
 
 def swap(x, axis):
@@ -404,50 +490,60 @@
         [kv, shape((half, depth), BF16), weights, table, table],
         [buffers, pltpu.SemaphoreType.DMA((3,))], flops, hbm=(0, 1, 2))
     kv1_a = onward(kv_a)
-    kv_b, w_send = call(
-        rest_keep_kernel, scalars, [partner, w_keep, cosine, sine, key_weight, value_weight], [kv, weights],
-        [buffers, pltpu.SemaphoreType.DMA((2,))], flops, hbm=(4, 5))
+    kv_b, = call(rest_keep_kernel, scalars, [partner, w_keep, cosine, sine], [kv], [buffers], flops)
     kv1_b = onward(kv_b)
-    send_a, = call(functools.partial(send_kernel, part=0), scalars, [own, w_send, cosine, sine], [kv], [buffers],
+    send_a, = call(functools.partial(send_kernel, part=0), scalars, [own, key_weight, value_weight, cosine, sine],
+                   [kv], [buffers],
                    flops)
     kv_ya = swap(send_a, "sp")
-    send_b, = call(functools.partial(send_kernel, part=1), scalars, [partner, w_send, cosine, sine], [kv], [buffers],
+    send_b, = call(functools.partial(send_kernel, part=1), scalars, [partner, key_weight, value_weight, cosine, sine],
+                   [kv], [buffers],
                    flops)
     kv_yb = swap(send_b, "sp")
-    q_a, q_b, q_send = call(
-        q_kernel, scalars, [own, partner, cosine, sine, query_weight], [q_half, q_half, q_shape],
+    back = shape((heads - RELAYED, 2, half, HEAD), BF16)
+    q_a, q_b, q_send, back_own = call(
+        q_kernel, scalars, [own, partner, cosine, sine, query_weight], [q_half, q_half, q_shape, back],
         [buffers], 2 * flops)
     q_y = swap(q_send, "sp")
+    behind = jnp.stack([back_own.reshape(rows, HEAD), q_y[RELAYED]])
+    n = lax.axis_size("sp")
+    q_next = lax.ppermute(behind, "sp", [(i, i - 2) for i in range(2, n)])
     kv1_ya = onward(kv_ya)
     kv1_yb = onward(kv_yb)
-    kv2_a = onward(kv1_a)
-    kv2_b = onward(kv1_b)
-    kv2_y = []
-    for h in range(heads):
-        kv2_y.append(onward(jnp.stack([kv1_ya[h], kv1_yb[h]])))
+    kv2_ab = onward(jnp.stack([kv1_a[0], kv1_b[0]]))
+    kv2_y = onward(jnp.stack([kv1_ya[0], kv1_yb[0]]))
+    packed = shape((rows + 3 * FAR_DILATION, HEAD), BF16)
+    packing = [pltpu.VMEM((2, rows, HEAD), BF16), pltpu.VMEM((FAR_DILATION, HEAD), F32)]
+    piece_own, piece_diag = call(
+        functools.partial(foreign_kernel, head=1), scalars,
+        [q_next, kv1_a, kv1_b, kv1_ya, kv1_yb, pair2], [packed, packed],
+        [pltpu.VMEM((group, HEAD), BF16)] * 3 + [pltpu.VMEM((group, HEAD), F32)] * 2 + packing, 10 ** 9)
+    n = lax.axis_size("sp")
+    piece_diag = lax.ppermute(piece_diag, "sp", [(i, (i ^ 1) + 2) for i in range(n - 2)])
+    piece_own = onward(piece_own)
     state = shape((heads, group, HEAD), F32)
     kv_scratch = [pltpu.VMEM((heads, group, HEAD), BF16)] * 2
     q, m, l, o = call(
         local_kernel, scalars, [q_a, q_b, q_y, kv_a, kv_b, kv_ya, kv_yb, group0, near0, near1],
         [shape((heads, group, HEAD), BF16), state, state, state],
         kv_scratch + [pltpu.VMEM((heads, 2 * group, 4 * HEAD), F32)], 3 * 10 ** 9)
-    m, l, o = call(
-        one_kernel, scalars, [q, m, l, o, kv1_a, kv1_b, kv1_ya, kv1_yb, group1, near1], [state, state, state],
-        kv_scratch + [pltpu.VMEM((heads, 2 * group, 2 * HEAD), F32), pltpu.VMEM((heads, group, HEAD), F32)],
-        10 ** 9, {2: 0, 3: 1, 4: 2})
+    m, l, o, state_y = call(
+        one_kernel, scalars, [q, m, l, o, kv1_a, kv1_b, kv1_ya, kv1_yb, group1, near1], [state, state, state, packed],
+        kv_scratch + [pltpu.VMEM((heads, 2 * group, 2 * HEAD), F32), pltpu.VMEM((heads, group, HEAD), F32)]
+        + packing, 10 ** 9, {2: 0, 3: 1, 4: 2})
+    state_y = swap(state_y, "sp")
     mixed = shape((rows, HEAD), BF16)
-    parts = []
-    for h in range(heads):
-        keep, send = call(
-            functools.partial(two_kernel, head=h), scalars, [q, m, l, o, kv2_a, kv2_b, kv2_y[h], pair2], [mixed, mixed],
-            [pltpu.VMEM((group, HEAD), BF16)] * 2 + [pltpu.VMEM((group, HEAD), F32)] * 2
-            + [pltpu.VMEM((2, rows, HEAD), F32)], 10 ** 9)
-        keep_tp = swap(keep, "tp")
-        from_y = swap(send, "sp")
-        parts.append([keep, from_y, keep_tp, swap(from_y, "tp")])
-    total = call(out_first_kernel, scalars, parts[0] + [output_weight],
-                 [shape((rows, output_weight.shape[1]), F32)], [], rows * output_weight.size, limit=16)[0]
-    return out_last(scalars, parts[1], output_weight, total)
+    keep, send = call(
+        functools.partial(two_kernel, head=0), scalars, [q, m, l, o, kv2_ab, kv2_y, pair2],
+        [mixed, mixed], [pltpu.VMEM((group, HEAD), BF16)] * 2 + [pltpu.VMEM((group, HEAD), F32)] * 2
+        + [pltpu.VMEM((2, rows, HEAD), F32)], 10 ** 9)
+    keep_tp = swap(keep, "tp")
+    from_y = swap(send, "sp")
+    first = [keep, from_y, keep_tp, swap(from_y, "tp")]
+    last, = call(functools.partial(final_kernel, head=1), scalars, [m, l, o, state_y, piece_own, piece_diag],
+                 [shape((2, rows, HEAD), BF16)], [pltpu.VMEM((2, rows, HEAD), F32)], 10 ** 9)
+    last_tp = swap(last, "tp")
+    return out_project(scalars, first, [last, last_tp], output_weight)
 
 
 def solution(mesh):

time: 73.1 us -> 78.3 us (1.071); the launches traced: 71.9 us -> 77.9 us
  starting transfers between devices: 34.3 us -> 38.8 us
  Pallas kernels: 21 us -> 22 us
    ppermute x10 -> x9, waiting for transfers between devices: 4.11 us -> 12.6 us  [swap(): lax.ppermute(x, axis, [(i, i ^ 1) for i in range(lax.axis_size(axis))])]
    ppermute x8 -> x7, waiting for transfers between devices: 11.9 us -> 3.78 us  [onward(): return lax.ppermute(x, 'sp', [(i, i + 2) for i in range(n - 2)])]
    ppermute x0 -> x2, starting transfers between devices: none -> 4.74 us  [the longest x1 3.45 us: body(): lax.ppermute(piece_diag, 'sp', [(i, (i ^ 1) + 2) for i in range(n - 2)])]
    ppermute x8 -> x7, starting transfers between devices: 26.3 us -> 25.5 us  [onward(): return lax.ppermute(x, 'sp', [(i, i + 2) for i in range(n - 2)])]
    ppermute x10 -> x9, starting transfers between devices: 8.02 us -> 8.61 us  [swap(): lax.ppermute(x, axis, [(i, i ^ 1) for i in range(lax.axis_size(axis))])]
  transfers between devices with their start and end apart: 18 -> 18, of which waited for: 5 -> 6; matrix products, arithmetic and copies ran while one was open for 0% -> 0% of each run, Pallas kernels for 20% -> 25%
where the time goes in v2:
time: 78.3 us; the launch traced here: 77.9 us
  starting transfers between devices  38.8 us (50%)
  Pallas kernels  22 us (28%)
  waiting for transfers between devices  16.4 us (21%)
    ppermute x7, starting transfers between devices, onward(): return lax.ppermute(x, 'sp', [(i, i + 2) for i in range(n - 2)])  25.5 us
    pallas_call x10, Pallas kernels, call(): pl.pallas_call(kernel, in_specs=[pl.BlockSpec(memory_space=pltpu.SMEM)] +...  19.2 us
    ppermute x9, waiting for transfers between devices, swap(): lax.ppermute(x, axis, [(i, i ^ 1) for i in range(lax.axis_size(axis))])  12.6 us
    ppermute x9, starting transfers between devices, swap(): lax.ppermute(x, axis, [(i, i ^ 1) for i in range(lax.axis_size(axis))])  8.61 us
    ppermute x7, waiting for transfers between devices, onward(): return lax.ppermute(x, 'sp', [(i, i + 2) for i in range(n - 2)])  3.78 us
    ppermute x1, starting transfers between devices, body(): lax.ppermute(piece_diag, 'sp', [(i, (i ^ 1) + 2) for i in range(n - 2)])  3.45 us
    pallas_call x1, Pallas kernels, out_project(): pl.pallas_call(out_kernel, grid=(steps,), in_specs=[pl.BlockSpec(memory_s...  2.79 us
  transfers between devices with their start and end apart: 18, of which 6 were waited for; matrix products, arithmetic and copies ran while one was open for 0% of the time, Pallas kernels for 25%

profile of v2, /device:TPU:0, one launch (start us, length us, event | category | flops | bytes accessed | tf_op | source)
XLA Modules:
  0.0 77.9 jit_solution(15983133629316588496)
XLA Ops:
  0.0 0.5 collective-permute-start
  0.5 0.1 maximum_bitcast_fusion.inv_ref
  0.6 0.1 pad_add_fusion.sc_ref
  0.7 4.2 %shard_map.100 = (bf16[2,2,256,128]{3,2,1,0:T(8,128)(2,1)S(1)}, bf16[256,2048]{1,0:T(8,128)(2,1)S(1)}, bf16[2,2048,256]{2,1,0:T(8,128)(2,1)S(1)}, f32[2,256,128]{2,1,0:T(8,128)S(1)}, f32[2,256,128]{2,1,0:T(8,128)S(1)}) custom-call(s32[4]{0:T(128)S(1)} %pad_add_fusion.sc_ref, bf16[256,2048]{1,0:T(8,128)(2,1)} %x_hbm.1, bf16[2048,512]{1,0:T(8,128)(2,1)} %wk_ref.3, ...), custom_call_target="tpu_custom_call" | custom-call | flops 536870912 | tf_op jit(solution)/shard_map/pallas_call | solution.py:120
  4.9 0.0 copy-done
  4.9 0.0 copy-done.1
  4.9 0.0 copy-start.2
  4.9 1.5 %shard_map.103 = bf16[2,2,256,128]{3,2,1,0:T(8,128)(2,1)S(1)} custom-call(s32[4]{0:T(128)S(1)} %pad_add_fusion.sc_ref, bf16[256,2048]{1,0:T(8,128)(2,1)S(1)} %get-tuple-element.26.xo_ref.x_ref, bf16[2048,512]{1,0:T(8,128)(2,1)S(1)} %copy-done, bf16[2048,512]{1,0:T(8,128)(2,1)S(1)} %copy-done.1, f32[2,256,128]{2,1,0:T(8,128)S(1)} %get-tuple-element.27.cos_ref, ...), custom_call_target="tpu_custom_call" | custom-call | flops 536870912 | tf_op jit(solution)/shard_map/pallas_call | solution.py:120
  6.4 2.6 %collective-permute-start.2 = (bf16[2,2,256,128]{3,2,1,0:T(8,128)(2,1)S(1)}, bf16[2,2,256,128]{3,2,1,0:T(8,128)(2,1)S(1)}, u32[]{:S(2)}, u32[]{:S(2)}) collective-permute-start(bf16[2,2,256,128]{3,2,1,0:T(8,128)(2,1)S(1)} %shard_map.103), channel_id=1, source_target_pairs={{0,2},{2,0},{4,6},{6,4},{8,10},{10,8},{12,14},{14,12},{1,3},{3,1},... | collective-permute-start | bytes 786440 | tf_op jit(solution)/shard_map/ppermute | solution.py:458
  9.0 3.5 %collective-permute-start.4 = (bf16[2,2,256,128]{3,2,1,0:T(8,128)(2,1)S(1)}, bf16[2,2,256,128]{3,2,1,0:T(8,128)(2,1)S(1)}, u32[]{:S(2)}, u32[]{:S(2)}) collective-permute-start(bf16[2,2,256,128]{3,2,1,0:T(8,128)(2,1)S(1)} %get-tuple-element.32.kva_ref), channel_id=1, source_target_pairs={{0,4},{2,6},{4,8},{6,10},{8,12},{10,14},{1,5},{3,7},{5,9},{7,11},{... | collective-permute-start | bytes 786440 | tf_op jit(solution)/shard_map/ppermute | solution.py:463
  12.5 3.5 %collective-permute-done.2.kvya_ref = bf16[2,2,256,128]{3,2,1,0:T(8,128)(2,1)S(1)} collective-permute-done((bf16[2,2,256,128]{3,2,1,0:T(8,128)(2,1)S(1)}, bf16[2,2,256,128]{3,2,1,0:T(8,128)(2,1)S(1)}, u32[]{:S(2)}, u32[]{:S(2)}) %collective-permute-start.2) | collective-permute-done | bytes 262176 | tf_op jit(solution)/shard_map/ppermute | solution.py:458
  16.0 3.7 %collective-permute-start.6 = (bf16[2,2,256,128]{3,2,1,0:T(8,128)(2,1)S(1)}, bf16[2,2,256,128]{3,2,1,0:T(8,128)(2,1)S(1)}, u32[]{:S(2)}, u32[]{:S(2)}) collective-permute-start(bf16[2,2,256,128]{3,2,1,0:T(8,128)(2,1)S(1)} %collective-permute-done.2.kvya_ref), channel_id=1, source_target_pairs={{0,4},{2,6},{4,8},{6,10},{8,12},{10,14},{1,5},{3,7},{5,9},{7,11},{... | collective-permute-start | bytes 786440 | tf_op jit(solution)/shard_map/ppermute | solution.py:463
  19.7 0.0 collective-permute-done.xp_ref.x_ref
  19.7 0.0 copy-done.2
  19.7 2.5 %shard_map.101 = (bf16[2,256,128]{2,1,0:T(8,128)(2,1)S(1)}, bf16[2,256,128]{2,1,0:T(8,128)(2,1)S(1)}, bf16[2,512,128]{2,1,0:T(8,128)(2,1)S(1)}, bf16[1,2,256,128]{3,2,1,0:T(8,128)(2,1)S(1)}) custom-call(s32[4]{0:T(128)S(1)} %pad_add_fusion.sc_ref, bf16[256,2048]{1,0:T(8,128)(2,1)S(1)} %get-tuple-element.26.xo_ref.x_ref, ...), custom_call_target="tpu_custom_call" | custom-call | flops 1073741824 | tf_op jit(solution)/shard_map/pallas_call | solution.py:120
  22.2 1.6 %collective-permute-start.1 = (bf16[2,512,128]{2,1,0:T(8,128)(2,1)S(1)}, bf16[2,512,128]{2,1,0:T(8,128)(2,1)S(1)}, u32[]{:S(2)}, u32[]{:S(2)}) collective-permute-start(bf16[2,512,128]{2,1,0:T(8,128)(2,1)S(1)} %get-tuple-element.31), channel_id=1, source_target_pairs={{0,2},{2,0},{4,6},{6,4},{8,10},{10,8},{12,14},{14,12},{1,3},{3,1},... | collective-permute-start | bytes 786440 | tf_op jit(solution)/shard_map/ppermute | solution.py:458
  23.8 1.5 %shard_map.102.kvb_ref = bf16[2,2,256,128]{3,2,1,0:T(8,128)(2,1)S(1)} custom-call(s32[4]{0:T(128)S(1)} %pad_add_fusion.sc_ref, bf16[256,2048]{1,0:T(8,128)(2,1)S(1)} %collective-permute-done.xp_ref.x_ref, bf16[2,2048,256]{2,1,0:T(8,128)(2,1)S(1)} %get-tuple-element.33.w_ref, f32[2,256,128]{2,1,0:T(8,128)S(1)} %get-tuple-element.27.cos_ref, ...), custom_call_target="tpu_custom_call" | custom-call | flops 536870912 | tf_op jit(solution)/shard_map/pallas_call | solution.py:120
  25.3 3.5 %collective-permute-start.5 = (bf16[2,2,256,128]{3,2,1,0:T(8,128)(2,1)S(1)}, bf16[2,2,256,128]{3,2,1,0:T(8,128)(2,1)S(1)}, u32[]{:S(2)}, u32[]{:S(2)}) collective-permute-start(bf16[2,2,256,128]{3,2,1,0:T(8,128)(2,1)S(1)} %shard_map.102.kvb_ref), channel_id=1, source_target_pairs={{0,4},{2,6},{4,8},{6,10},{8,12},{10,14},{1,5},{3,7},{5,9},{7,11},{... | collective-permute-start | bytes 786440 | tf_op jit(solution)/shard_map/ppermute | solution.py:463
  28.8 1.5 %shard_map.104 = bf16[2,2,256,128]{3,2,1,0:T(8,128)(2,1)S(1)} custom-call(s32[4]{0:T(128)S(1)} %pad_add_fusion.sc_ref, bf16[256,2048]{1,0:T(8,128)(2,1)S(1)} %collective-permute-done.xp_ref.x_ref, bf16[2048,512]{1,0:T(8,128)(2,1)S(1)} %copy-done, bf16[2048,512]{1,0:T(8,128)(2,1)S(1)} %copy-done.1, f32[2,256,128]{2,1,0:T(8,128)S(1)} %get-tuple-element.27.cos_ref, ...), custom_call_target="tpu_custom_call" | custom-call | flops 536870912 | tf_op jit(solution)/shard_map/pallas_call | solution.py:120
  30.3 0.0 copy-start.4
  30.3 0.0 copy-start.7
  30.3 0.0 copy-start.8
  30.3 0.6 collective-permute-start.3
  30.9 0.0 collective-permute-done.4.kva_ref
  30.9 0.0 collective-permute-done.6.kvya_ref
  31.0 0.0 collective-permute-done.1.qy_ref
  31.0 1.3 %collective-permute-start.14 = (bf16[2,512,128]{2,1,0:T(8,128)(2,1)S(1)}, bf16[2,512,128]{2,1,0:T(8,128)(2,1)S(1)}, u32[]{:S(2)}, u32[]{:S(2)}) collective-permute-start(bf16[2,512,128]{2,1,0:T(8,128)(2,1)S(1)} %pad_maximum_fusion.2), channel_id=1, source_target_pairs={{4,0},{6,2},{8,4},{10,6},{12,8},{14,10},{5,1},{7,3},{9,5},{11,7},{... | collective-permute-start | bytes 786440 | tf_op jit(solution)/shard_map/ppermute | solution.py:510
  32.3 1.2 %collective-permute-done.5.kvb_ref = bf16[2,2,256,128]{3,2,1,0:T(8,128)(2,1)S(1)} collective-permute-done((bf16[2,2,256,128]{3,2,1,0:T(8,128)(2,1)S(1)}, bf16[2,2,256,128]{3,2,1,0:T(8,128)(2,1)S(1)}, u32[]{:S(2)}, u32[]{:S(2)}) %collective-permute-start.5) | collective-permute-done | bytes 262176 | tf_op jit(solution)/shard_map/ppermute | solution.py:463
  33.6 4.4 %collective-permute-start.8 = (bf16[2,2,256,128]{3,2,1,0:T(8,128)(2,1)S(1)}, bf16[2,2,256,128]{3,2,1,0:T(8,128)(2,1)S(1)}, u32[]{:S(2)}, u32[]{:S(2)}) collective-permute-start(bf16[2,2,256,128]{3,2,1,0:T(8,128)(2,1)S(1)} %pad_maximum_fusion), channel_id=1, source_target_pairs={{0,4},{2,6},{4,8},{6,10},{8,12},{10,14},{1,5},{3,7},{5,9},{7,11},{... | collective-permute-start | bytes 786440 | tf_op jit(solution)/shard_map/ppermute | solution.py:463
  38.0 0.0 collective-permute-done.3.kvyb_ref
  38.0 3.5 %collective-permute-start.7 = (bf16[2,2,256,128]{3,2,1,0:T(8,128)(2,1)S(1)}, bf16[2,2,256,128]{3,2,1,0:T(8,128)(2,1)S(1)}, u32[]{:S(2)}, u32[]{:S(2)}) collective-permute-start(bf16[2,2,256,128]{3,2,1,0:T(8,128)(2,1)S(1)} %collective-permute-done.3.kvyb_ref), channel_id=1, source_target_pairs={{0,4},{2,6},{4,8},{6,10},{8,12},{10,14},{1,5},{3,7},{5,9},{7,11},{... | collective-permute-start | bytes 786440 | tf_op jit(solution)/shard_map/ppermute | solution.py:463
  41.5 0.0 copy-done.4
  41.5 0.0 copy-done.7
  41.5 0.0 copy-done.8
  41.5 0.0 copy-start.6
  41.6 3.4 %shard_map.105 = (bf16[2,1024,128]{2,1,0:T(8,128)(2,1)S(1)}, f32[2,1024,128]{2,1,0:T(8,128)S(1)}, f32[2,1024,128]{2,1,0:T(8,128)S(1)}, f32[2,1024,128]{2,1,0:T(8,128)S(1)}) custom-call(s32[4]{0:T(128)S(1)} %pad_add_fusion.sc_ref, bf16[2,256,128]{2,1,0:T(8,128)(2,1)S(1)} %get-tuple-element.29.qa_ref, bf16[2,256,128]{2,1,0:T(8,128)(2,1)S(1)} %get-tuple-element.30.qb_ref, ...), custom_call_target="tpu_custom_call" | custom-call | flops 3000000000 | tf_op jit(solution)/shard_map/pallas_call | solution.py:120
  45.0 0.0 copy-start.5
  45.0 0.0 collective-permute-done.14.qn_ref
  45.0 2.5 %collective-permute-done.7.kvyb_ref = bf16[2,2,256,128]{3,2,1,0:T(8,128)(2,1)S(1)} collective-permute-done((bf16[2,2,256,128]{3,2,1,0:T(8,128)(2,1)S(1)}, bf16[2,2,256,128]{3,2,1,0:T(8,128)(2,1)S(1)}, u32[]{:S(2)}, u32[]{:S(2)}) %collective-permute-start.7) | collective-permute-done | bytes 262176 | tf_op jit(solution)/shard_map/ppermute | solution.py:463
  47.5 0.0 copy-done.6
  47.5 1.2 %shard_map.108 = (bf16[560,128]{1,0:T(8,128)(2,1)S(1)}, bf16[560,128]{1,0:T(8,128)(2,1)S(1)}) custom-call(s32[4]{0:T(128)S(1)} %pad_add_fusion.sc_ref, bf16[2,512,128]{2,1,0:T(8,128)(2,1)S(1)} %collective-permute-done.14.qn_ref, bf16[2,2,256,128]{3,2,1,0:T(8,128)(2,1)S(1)} %collective-permute-done.4.kva_ref, ...), custom_call_target="tpu_custom_call" | custom-call | flops 1000000000 | tf_op jit(solution)/shard_map/pallas_call | solution.py:120
  48.8 4.4 %collective-permute-start.15 = (bf16[560,128]{1,0:T(8,128)(2,1)S(1)}, bf16[560,128]{1,0:T(8,128)(2,1)S(1)}, u32[]{:S(2)}, u32[]{:S(2)}) collective-permute-start(bf16[560,128]{1,0:T(8,128)(2,1)S(1)} %get-tuple-element.45), channel_id=1, source_target_pairs={{0,4},{2,6},{4,8},{6,10},{8,12},{10,14},{1,5},{3,7},{5,9},{7,11},{... | collective-permute-start | bytes 430088 | tf_op jit(solution)/shard_map/ppermute | solution.py:463
  53.2 3.4 %collective-permute-start.16 = (bf16[560,128]{1,0:T(8,128)(2,1)S(1)}, bf16[560,128]{1,0:T(8,128)(2,1)S(1)}, u32[]{:S(2)}, u32[]{:S(2)}) collective-permute-start(bf16[560,128]{1,0:T(8,128)(2,1)S(1)} %get-tuple-element.46), channel_id=1, source_target_pairs={{0,6},{2,4},{4,10},{6,8},{8,14},{10,12},{1,7},{3,5},{5,11},{7,9},{... | collective-permute-start | bytes 430088 | tf_op jit(solution)/shard_map/ppermute | solution.py:522
  56.7 2.5 %collective-permute-start.9 = (bf16[2,2,256,128]{3,2,1,0:T(8,128)(2,1)S(1)}, bf16[2,2,256,128]{3,2,1,0:T(8,128)(2,1)S(1)}, u32[]{:S(2)}, u32[]{:S(2)}) collective-permute-start(bf16[2,2,256,128]{3,2,1,0:T(8,128)(2,1)S(1)} %pad_maximum_fusion.1), channel_id=1, source_target_pairs={{0,4},{2,6},{4,8},{6,10},{8,12},{10,14},{1,5},{3,7},{5,9},{7,11},{... | collective-permute-start | bytes 786440 | tf_op jit(solution)/shard_map/ppermute | solution.py:463
  59.2 0.0 copy-done.5
  59.2 0.9 %shard_map.106 = (f32[2,1024,128]{2,1,0:T(8,128)S(1)}, f32[2,1024,128]{2,1,0:T(8,128)S(1)}, f32[2,1024,128]{2,1,0:T(8,128)S(1)}, bf16[560,128]{1,0:T(8,128)(2,1)S(1)}) custom-call(s32[4]{0:T(128)S(1)} %pad_add_fusion.sc_ref, bf16[2,1024,128]{2,1,0:T(8,128)(2,1)S(1)} %get-tuple-element.34.q_ref, ...), custom_call_target="tpu_custom_call", output_to_operand_aliasing={{0}: (2, {}), {1}: (3, {}), {2}: (4, {})} | custom-call | flops 1000000000 | tf_op jit(solution)/shard_map/pallas_call | solution.py:120
  60.1 1.6 %collective-permute-start.13 = (bf16[560,128]{1,0:T(8,128)(2,1)S(1)}, bf16[560,128]{1,0:T(8,128)(2,1)S(1)}, u32[]{:S(2)}, u32[]{:S(2)}) collective-permute-start(bf16[560,128]{1,0:T(8,128)(2,1)S(1)} %get-tuple-element.43), channel_id=1, source_target_pairs={{0,2},{2,0},{4,6},{6,4},{8,10},{10,8},{12,14},{14,12},{1,3},{3,1},... | collective-permute-start | bytes 430088 | tf_op jit(solution)/shard_map/ppermute | solution.py:458
  61.7 0.0 collective-permute-done.15.own_ref
  61.7 0.0 collective-permute-done.16.diag_ref
  61.7 3.6 %collective-permute-done.13.state_ref = bf16[560,128]{1,0:T(8,128)(2,1)S(1)} collective-permute-done((bf16[560,128]{1,0:T(8,128)(2,1)S(1)}, bf16[560,128]{1,0:T(8,128)(2,1)S(1)}, u32[]{:S(2)}, u32[]{:S(2)}) %collective-permute-start.13) | collective-permute-done | bytes 143392 | tf_op jit(solution)/shard_map/ppermute | solution.py:458
  65.3 1.6 %shard_map.109.own_ref = bf16[2,512,128]{2,1,0:T(8,128)(2,1)S(1)} custom-call(s32[4]{0:T(128)S(1)} %pad_add_fusion.sc_ref, f32[2,1024,128]{2,1,0:T(8,128)S(1)} %get-tuple-element.38.m_ref, f32[2,1024,128]{2,1,0:T(8,128)S(1)} %get-tuple-element.39.l_ref, f32[2,1024,128]{2,1,0:T(8,128)S(1)} %get-tuple-element.40.o_ref, ...), custom_call_target="tpu_custom_call" | custom-call | flops 1000000000 | tf_op jit(solution)/shard_map/pallas_call | solution.py:120
  66.9 0.0 copy-start.3
  66.9 0.1 collective-permute-start.17
  67.0 0.0 collective-permute-done.8.kvo_ref
  67.0 0.0 collective-permute-done.9.kvy_ref
  67.0 0.9 %shard_map.107 = (bf16[512,128]{1,0:T(8,128)(2,1)S(1)}, bf16[512,128]{1,0:T(8,128)(2,1)S(1)}) custom-call(s32[4]{0:T(128)S(1)} %pad_add_fusion.sc_ref, bf16[2,1024,128]{2,1,0:T(8,128)(2,1)S(1)} %get-tuple-element.34.q_ref, f32[2,1024,128]{2,1,0:T(8,128)S(1)} %get-tuple-element.38.m_ref, f32[2,1024,128]{2,1,0:T(8,128)S(1)} %get-tuple-element.39.l_ref, ...), custom_call_target="tpu_custom_call" | custom-call | flops 1000000000 | tf_op jit(solution)/shard_map/pallas_call | solution.py:120
  67.9 1.6 %collective-permute-start.10 = (bf16[512,128]{1,0:T(8,128)(2,1)S(1)}, bf16[512,128]{1,0:T(8,128)(2,1)S(1)}, u32[]{:S(2)}, u32[]{:S(2)}) collective-permute-start(bf16[512,128]{1,0:T(8,128)(2,1)S(1)} %get-tuple-element.42), channel_id=1, source_target_pairs={{0,2},{2,0},{4,6},{6,4},{8,10},{10,8},{12,14},{14,12},{1,3},{3,1},... | collective-permute-start | bytes 393224 | tf_op jit(solution)/shard_map/ppermute | solution.py:458
  69.4 0.2 collective-permute-start.11
  69.6 4.2 %collective-permute-done.10.b_ref = bf16[512,128]{1,0:T(8,128)(2,1)S(1)} collective-permute-done((bf16[512,128]{1,0:T(8,128)(2,1)S(1)}, bf16[512,128]{1,0:T(8,128)(2,1)S(1)}, u32[]{:S(2)}, u32[]{:S(2)}) %collective-permute-start.10) | collective-permute-done | bytes 131104 | tf_op jit(solution)/shard_map/ppermute | solution.py:458
  73.8 0.0 collective-permute-start.12
  73.8 0.0 collective-permute-done.11.c_ref
  73.8 0.0 collective-permute-done.17.tp_ref
  73.8 1.3 %collective-permute-done.12.d_ref = bf16[512,128]{1,0:T(8,128)(2,1)S(1)} collective-permute-done((bf16[512,128]{1,0:T(8,128)(2,1)S(1)}, bf16[512,128]{1,0:T(8,128)(2,1)S(1)}, u32[]{:S(2)}, u32[]{:S(2)}) %collective-permute-start.12) | collective-permute-done | bytes 131104 | tf_op jit(solution)/shard_map/ppermute | solution.py:458
  75.1 2.8 %out_project.1 = bf16[512,1024]{1,0:T(8,128)(2,1)} custom-call(s32[4]{0:T(128)S(1)} %pad_add_fusion.sc_ref, bf16[512,128]{1,0:T(8,128)(2,1)S(1)} %get-tuple-element.41.a_ref, bf16[512,128]{1,0:T(8,128)(2,1)S(1)} %collective-permute-done.10.b_ref, bf16[512,128]{1,0:T(8,128)(2,1)S(1)} %collective-permute-done.11.c_ref, ...), custom_call_target="tpu_custom_call" | custom-call | flops 1073741824 | tf_op jit(solution)/shard_map/out_project/pallas_call | solution.py:445
  (12 shorter events, 0.1 us)
Async XLA Ops:
  0.0 19.7 %collective-permute-start = (bf16[256,2048]{1,0:T(8,128)(2,1)}, bf16[256,2048]{1,0:T(8,128)(2,1)S(1)}, u32[]{:S(2)}, u32[]{:S(2)}) collective-permute-start(bf16[256,2048]{1,0:T(8,128)(2,1)} %x_hbm.1), channel_id=1, source_target_pairs={{0,1},{1,0},{2,3},{3,2},{4,5},{5,4},{6,7},{7,6},{8,9},{9,8},{10,11... | collective-permute-start | bytes 3145736 | tf_op jit(solution)/shard_map/ppermute | solution.py:458
  0.7 4.2 %copy-start = (bf16[2048,512]{1,0:T(8,128)(2,1)S(1)}, bf16[2048,512]{1,0:T(8,128)(2,1)}, u32[]{:S(2)}) copy-start(bf16[2048,512]{1,0:T(8,128)(2,1)} %wk_ref.3) | copy-start | bytes 6291460
  0.7 4.2 %copy-start.1 = (bf16[2048,512]{1,0:T(8,128)(2,1)S(1)}, bf16[2048,512]{1,0:T(8,128)(2,1)}, u32[]{:S(2)}) copy-start(bf16[2048,512]{1,0:T(8,128)(2,1)} %wv_ref.3) | copy-start | bytes 6291460
  4.9 14.8 %copy-start.2 = (bf16[2048,512]{1,0:T(8,128)(2,1)S(1)}, bf16[2048,512]{1,0:T(8,128)(2,1)}, u32[]{:S(2)}) copy-start(bf16[2048,512]{1,0:T(8,128)(2,1)} %w_ref.2) | copy-start | bytes 6291460
  6.4 9.5 %collective-permute-start.2 = (bf16[2,2,256,128]{3,2,1,0:T(8,128)(2,1)S(1)}, bf16[2,2,256,128]{3,2,1,0:T(8,128)(2,1)S(1)}, u32[]{:S(2)}, u32[]{:S(2)}) collective-permute-start(bf16[2,2,256,128]{3,2,1,0:T(8,128)(2,1)S(1)} %shard_map.103), channel_id=1, source_target_pairs={{0,2},{2,0},{4,6},{6,4},{8,10},{10,8},{12,14},{14,12},{1,3},{3,1},... | collective-permute-start | bytes 786440 | tf_op jit(solution)/shard_map/ppermute | solution.py:458
  9.0 21.9 %collective-permute-start.4 = (bf16[2,2,256,128]{3,2,1,0:T(8,128)(2,1)S(1)}, bf16[2,2,256,128]{3,2,1,0:T(8,128)(2,1)S(1)}, u32[]{:S(2)}, u32[]{:S(2)}) collective-permute-start(bf16[2,2,256,128]{3,2,1,0:T(8,128)(2,1)S(1)} %get-tuple-element.32.kva_ref), channel_id=1, source_target_pairs={{0,4},{2,6},{4,8},{6,10},{8,12},{10,14},{1,5},{3,7},{5,9},{7,11},{... | collective-permute-start | bytes 786440 | tf_op jit(solution)/shard_map/ppermute | solution.py:463
  16.0 15.0 %collective-permute-start.6 = (bf16[2,2,256,128]{3,2,1,0:T(8,128)(2,1)S(1)}, bf16[2,2,256,128]{3,2,1,0:T(8,128)(2,1)S(1)}, u32[]{:S(2)}, u32[]{:S(2)}) collective-permute-start(bf16[2,2,256,128]{3,2,1,0:T(8,128)(2,1)S(1)} %collective-permute-done.2.kvya_ref), channel_id=1, source_target_pairs={{0,4},{2,6},{4,8},{6,10},{8,12},{10,14},{1,5},{3,7},{5,9},{7,11},{... | collective-permute-start | bytes 786440 | tf_op jit(solution)/shard_map/ppermute | solution.py:463
  22.2 8.8 %collective-permute-start.1 = (bf16[2,512,128]{2,1,0:T(8,128)(2,1)S(1)}, bf16[2,512,128]{2,1,0:T(8,128)(2,1)S(1)}, u32[]{:S(2)}, u32[]{:S(2)}) collective-permute-start(bf16[2,512,128]{2,1,0:T(8,128)(2,1)S(1)} %get-tuple-element.31), channel_id=1, source_target_pairs={{0,2},{2,0},{4,6},{6,4},{8,10},{10,8},{12,14},{14,12},{1,3},{3,1},... | collective-permute-start | bytes 786440 | tf_op jit(solution)/shard_map/ppermute | solution.py:458
  25.3 8.3 %collective-permute-start.5 = (bf16[2,2,256,128]{3,2,1,0:T(8,128)(2,1)S(1)}, bf16[2,2,256,128]{3,2,1,0:T(8,128)(2,1)S(1)}, u32[]{:S(2)}, u32[]{:S(2)}) collective-permute-start(bf16[2,2,256,128]{3,2,1,0:T(8,128)(2,1)S(1)} %shard_map.102.kvb_ref), channel_id=1, source_target_pairs={{0,4},{2,6},{4,8},{6,10},{8,12},{10,14},{1,5},{3,7},{5,9},{7,11},{... | collective-permute-start | bytes 786440 | tf_op jit(solution)/shard_map/ppermute | solution.py:463
  30.3 11.2 %copy-start.4 = (f32[256,256]{1,0:T(8,128)S(1)}, f32[256,256]{1,0:T(8,128)}, u32[]{:S(2)}) copy-start(f32[256,256]{1,0:T(8,128)} %constant.50.clone.near1_ref.near_ref) | copy-start | bytes 786436
  30.3 11.2 %copy-start.7 = (f32[256,256]{1,0:T(8,128)S(1)}, f32[256,256]{1,0:T(8,128)}, u32[]{:S(2)}) copy-start(f32[256,256]{1,0:T(8,128)} %constant.48.clone.group_ref) | copy-start | bytes 786436
  30.3 11.2 %copy-start.8 = (f32[256,256]{1,0:T(8,128)S(1)}, f32[256,256]{1,0:T(8,128)}, u32[]{:S(2)}) copy-start(f32[256,256]{1,0:T(8,128)} %constant.49.clone.near0_ref) | copy-start | bytes 786436
  30.3 7.7 %collective-permute-start.3 = (bf16[2,2,256,128]{3,2,1,0:T(8,128)(2,1)S(1)}, bf16[2,2,256,128]{3,2,1,0:T(8,128)(2,1)S(1)}, u32[]{:S(2)}, u32[]{:S(2)}) collective-permute-start(bf16[2,2,256,128]{3,2,1,0:T(8,128)(2,1)S(1)} %shard_map.104), channel_id=1, source_target_pairs={{0,2},{2,0},{4,6},{6,4},{8,10},{10,8},{12,14},{14,12},{1,3},{3,1},... | collective-permute-start | bytes 786440 | tf_op jit(solution)/shard_map/ppermute | solution.py:458
  31.0 14.0 %collective-permute-start.14 = (bf16[2,512,128]{2,1,0:T(8,128)(2,1)S(1)}, bf16[2,512,128]{2,1,0:T(8,128)(2,1)S(1)}, u32[]{:S(2)}, u32[]{:S(2)}) collective-permute-start(bf16[2,512,128]{2,1,0:T(8,128)(2,1)S(1)} %pad_maximum_fusion.2), channel_id=1, source_target_pairs={{4,0},{6,2},{8,4},{10,6},{12,8},{14,10},{5,1},{7,3},{9,5},{11,7},{... | collective-permute-start | bytes 786440 | tf_op jit(solution)/shard_map/ppermute | solution.py:510
  33.6 33.4 %collective-permute-start.8 = (bf16[2,2,256,128]{3,2,1,0:T(8,128)(2,1)S(1)}, bf16[2,2,256,128]{3,2,1,0:T(8,128)(2,1)S(1)}, u32[]{:S(2)}, u32[]{:S(2)}) collective-permute-start(bf16[2,2,256,128]{3,2,1,0:T(8,128)(2,1)S(1)} %pad_maximum_fusion), channel_id=1, source_target_pairs={{0,4},{2,6},{4,8},{6,10},{8,12},{10,14},{1,5},{3,7},{5,9},{7,11},{... | collective-permute-start | bytes 786440 | tf_op jit(solution)/shard_map/ppermute | solution.py:463
  38.0 9.5 %collective-permute-start.7 = (bf16[2,2,256,128]{3,2,1,0:T(8,128)(2,1)S(1)}, bf16[2,2,256,128]{3,2,1,0:T(8,128)(2,1)S(1)}, u32[]{:S(2)}, u32[]{:S(2)}) collective-permute-start(bf16[2,2,256,128]{3,2,1,0:T(8,128)(2,1)S(1)} %collective-permute-done.3.kvyb_ref), channel_id=1, source_target_pairs={{0,4},{2,6},{4,8},{6,10},{8,12},{10,14},{1,5},{3,7},{5,9},{7,11},{... | collective-permute-start | bytes 786440 | tf_op jit(solution)/shard_map/ppermute | solution.py:463
  41.5 6.0 %copy-start.6 = (f32[128,128]{1,0:T(8,128)S(1)}, f32[128,128]{1,0:T(8,128)}, u32[]{:S(2)}) copy-start(f32[128,128]{1,0:T(8,128)} %constant.47.clone.pair_ref) | copy-start | bytes 196612
  45.0 14.2 %copy-start.5 = (f32[256,256]{1,0:T(8,128)S(1)}, f32[256,256]{1,0:T(8,128)}, u32[]{:S(2)}) copy-start(f32[256,256]{1,0:T(8,128)} %constant.51.clone.group_ref) | copy-start | bytes 786436
  48.8 12.9 %collective-permute-start.15 = (bf16[560,128]{1,0:T(8,128)(2,1)S(1)}, bf16[560,128]{1,0:T(8,128)(2,1)S(1)}, u32[]{:S(2)}, u32[]{:S(2)}) collective-permute-start(bf16[560,128]{1,0:T(8,128)(2,1)S(1)} %get-tuple-element.45), channel_id=1, source_target_pairs={{0,4},{2,6},{4,8},{6,10},{8,12},{10,14},{1,5},{3,7},{5,9},{7,11},{... | collective-permute-start | bytes 430088 | tf_op jit(solution)/shard_map/ppermute | solution.py:463
  53.2 8.5 %collective-permute-start.16 = (bf16[560,128]{1,0:T(8,128)(2,1)S(1)}, bf16[560,128]{1,0:T(8,128)(2,1)S(1)}, u32[]{:S(2)}, u32[]{:S(2)}) collective-permute-start(bf16[560,128]{1,0:T(8,128)(2,1)S(1)} %get-tuple-element.46), channel_id=1, source_target_pairs={{0,6},{2,4},{4,10},{6,8},{8,14},{10,12},{1,7},{3,5},{5,11},{7,9},{... | collective-permute-start | bytes 430088 | tf_op jit(solution)/shard_map/ppermute | solution.py:522
  56.7 10.3 %collective-permute-start.9 = (bf16[2,2,256,128]{3,2,1,0:T(8,128)(2,1)S(1)}, bf16[2,2,256,128]{3,2,1,0:T(8,128)(2,1)S(1)}, u32[]{:S(2)}, u32[]{:S(2)}) collective-permute-start(bf16[2,2,256,128]{3,2,1,0:T(8,128)(2,1)S(1)} %pad_maximum_fusion.1), channel_id=1, source_target_pairs={{0,4},{2,6},{4,8},{6,10},{8,12},{10,14},{1,5},{3,7},{5,9},{7,11},{... | collective-permute-start | bytes 786440 | tf_op jit(solution)/shard_map/ppermute | solution.py:463
  60.1 5.2 %collective-permute-start.13 = (bf16[560,128]{1,0:T(8,128)(2,1)S(1)}, bf16[560,128]{1,0:T(8,128)(2,1)S(1)}, u32[]{:S(2)}, u32[]{:S(2)}) collective-permute-start(bf16[560,128]{1,0:T(8,128)(2,1)S(1)} %get-tuple-element.43), channel_id=1, source_target_pairs={{0,2},{2,0},{4,6},{6,4},{8,10},{10,8},{12,14},{14,12},{1,3},{3,1},... | collective-permute-start | bytes 430088 | tf_op jit(solution)/shard_map/ppermute | solution.py:458
  66.9 8.3 %copy-start.3 = (bf16[1024,1024]{1,0:T(8,128)(2,1)S(1)}, bf16[1024,1024]{1,0:T(8,128)(2,1)}, u32[]{:S(2)}) copy-start(bf16[1024,1024]{1,0:T(8,128)(2,1)} %w_ref.3) | copy-start | bytes 6291460
  66.9 6.9 %collective-permute-start.17 = (bf16[2,512,128]{2,1,0:T(8,128)(2,1)S(1)}, bf16[2,512,128]{2,1,0:T(8,128)(2,1)S(1)}, u32[]{:S(2)}, u32[]{:S(2)}) collective-permute-start(bf16[2,512,128]{2,1,0:T(8,128)(2,1)S(1)} %shard_map.109.own_ref), channel_id=1, source_target_pairs={{0,1},{1,0},{2,3},{3,2},{4,5},{5,4},{6,7},{7,6},{8,9},{9,8},{10,11... | collective-permute-start | bytes 786440 | tf_op jit(solution)/shard_map/ppermute | solution.py:458
  67.9 5.9 %collective-permute-start.10 = (bf16[512,128]{1,0:T(8,128)(2,1)S(1)}, bf16[512,128]{1,0:T(8,128)(2,1)S(1)}, u32[]{:S(2)}, u32[]{:S(2)}) collective-permute-start(bf16[512,128]{1,0:T(8,128)(2,1)S(1)} %get-tuple-element.42), channel_id=1, source_target_pairs={{0,2},{2,0},{4,6},{6,4},{8,10},{10,8},{12,14},{14,12},{1,3},{3,1},... | collective-permute-start | bytes 393224 | tf_op jit(solution)/shard_map/ppermute | solution.py:458
  69.4 4.4 %collective-permute-start.11 = (bf16[512,128]{1,0:T(8,128)(2,1)S(1)}, bf16[512,128]{1,0:T(8,128)(2,1)S(1)}, u32[]{:S(2)}, u32[]{:S(2)}) collective-permute-start(bf16[512,128]{1,0:T(8,128)(2,1)S(1)} %get-tuple-element.41.a_ref), channel_id=1, source_target_pairs={{0,1},{1,0},{2,3},{3,2},{4,5},{5,4},{6,7},{7,6},{8,9},{9,8},{10,11... | collective-permute-start | bytes 393224 | tf_op jit(solution)/shard_map/ppermute | solution.py:458
  73.8 1.3 %collective-permute-start.12 = (bf16[512,128]{1,0:T(8,128)(2,1)S(1)}, bf16[512,128]{1,0:T(8,128)(2,1)S(1)}, u32[]{:S(2)}, u32[]{:S(2)}) collective-permute-start(bf16[512,128]{1,0:T(8,128)(2,1)S(1)} %collective-permute-done.10.b_ref), channel_id=1, source_target_pairs={{0,1},{1,0},{2,3},{3,2},{4,5},{5,4},{6,7},{7,6},{8,9},{9,8},{10,11... | collective-permute-start | bytes 393224 | tf_op jit(solution)/shard_map/ppermute | solution.py:458

commit v3 on v2

--- a/solution.py
+++ b/solution.py
@@ -67,6 +67,7 @@
     copies = weight_copies(wk_hbm, wv_hbm, w_ref, par, sems)
     x_copy.start()
     copies[1].start()
+    copies[0].start()
     steps = half // FAR_DILATION
     lane = lax.broadcasted_iota(jnp.int32, (2 * steps, HEAD), 1)
     row = lax.broadcasted_iota(jnp.int32, (2 * steps, HEAD), 0)
@@ -80,12 +81,13 @@
     cos_ref[...] = (cos_c * cos_f - sin_c * sin_f).reshape(2, half, HEAD)
     sin_ref[...] = ((sin_c * cos_f + cos_c * sin_f) * sign).reshape(2, half, HEAD)
     x_copy.wait()
-    copies[0].start()
     kv_part(x_ref, (w_ref.at[0], w_ref.at[1]), out_ref, cos_ref.at[0], sin_ref.at[0], buf_ref, copies)
 
 
-def rest_keep_kernel(sc_ref, x_ref, w_ref, cos_ref, sin_ref, out_ref, buf_ref):
-    kv_part(x_ref, (w_ref.at[0], w_ref.at[1]), out_ref, cos_ref.at[1], sin_ref.at[1], buf_ref)
+def middle_kernel(sc_ref, xo_ref, xp_ref, wk_ref, wv_ref, w_ref, cos_ref, sin_ref, send_ref, keep_ref, buf_ref):
+    send_kernel(sc_ref, xo_ref, wk_ref, wv_ref, cos_ref, sin_ref, send_ref, buf_ref, part=0)
+    half = buf_ref.shape[0] // 2
+    kv_part(xp_ref, (w_ref.at[0], w_ref.at[1]), keep_ref, cos_ref.at[1], sin_ref.at[1], buf_ref.at[half:])
 
 
 def send_kernel(sc_ref, x_ref, wk_ref, wv_ref, cos_ref, sin_ref, out_ref, buf_ref, *, part):
@@ -166,7 +168,11 @@
 
 def scored(item, q_ref, k_ref, s_ref, m_ref, fresh):
     rows, keys, bias, at = item
-    s = scores_of(take(q_ref, rows), take(k_ref, keys))
+    if rows[0][1] < TILE:
+        s = scores_of(take(q_ref, [(a, TILE) for a, _ in rows]), take(k_ref, keys))
+        s = s.reshape(len(rows), TILE, s.shape[1])[:, :rows[0][1]].reshape(length(rows), s.shape[1])
+    else:
+        s = scores_of(take(q_ref, rows), take(k_ref, keys))
     if bias is not None:
         s = s + bias
     n, columns = s.shape
@@ -193,6 +199,10 @@
 
 def near_rows(c, nq):
     return [(r * 2 * nq + c * TILE, TILE) for r in range(FAR_DILATION)]
+
+
+def upper_rows(c, nq):
+    return [(a, REACH_STEPS // FAR_DILATION) for a, _ in near_rows(c, nq)]
 
 
 def pair_rows(i, nq):
@@ -222,10 +232,11 @@
     t = (np.arange(TILE)[None, :] * FAR_DILATION + r).reshape(-1)
     tq, tk = t[:, None], t[None, :]
     near0, near1 = near_of(tq, tk), near_of(tq + TILE * FAR_DILATION, tk)
+    upper = near1.reshape(FAR_DILATION, TILE, -1)[:, :REACH_STEPS // FAR_DILATION].reshape(-1, near1.shape[1])
     r = np.arange(2)[:, None]
     t = (np.arange(2 * nq)[None, :] * FAR_DILATION + r).reshape(-1)
     pair2 = every(t[:, None] + 2 * group, t[None, :], FAR_DILATION)
-    return [bias_of(np.asarray(x, int)) for x in (group0, group1, near0, near1, pair2)]
+    return [bias_of(np.asarray(x, int)) for x in (group0, group1, near0, near1, upper, pair2)]
 
 
 def local_kernel(sc_ref, qa_ref, qb_ref, qy_ref, kva_ref, kvb_ref, kvya_ref, kvyb_ref, group_ref, near0_ref, near1_ref,
@@ -245,13 +256,13 @@
             at += length(rows)
         for c in range(2 * nq // TILE):
             rows = near_rows(c, nq)
-            keys, bias = rows, near0_ref[...]
-            if c:
-                keys = near_rows(c - 1, nq) + rows
-                bias = jnp.concatenate([near1_ref[...], bias], axis=1)
-            items.append((rows, keys, bias, at))
+            items.append((rows, rows, near0_ref[...], at))
             scored(items[-1], q, k, sh, m, False)
             at += length(rows)
+            if c:
+                items.append((upper_rows(c, nq), near_rows(c - 1, nq), near1_ref[...], at))
+                scored(items[-1], q, k, sh, m, False)
+                at += length(items[-1][0])
         for i, item in enumerate(items):
             ol = weighed(item, v, sh, m, length(item[1]))
             if i < MIDDLE_DILATION:
@@ -476,7 +487,7 @@
     scalars = jnp.stack([tp, sp % 2, sp // 2, sp]).astype(jnp.int32)
     inverse = THETA_BASE ** (-jnp.arange(HEAD // 2, dtype=F32) / (HEAD // 2))
     inverse = jnp.concatenate([inverse, inverse])[None]
-    group0, group1, near0, near1, pair2 = biases(nq)
+    group0, group1, near0, near1, upper, pair2 = biases(nq)
     shape = jax.ShapeDtypeStruct
     kv = shape((heads, 2, half, HEAD), BF16)
     q_shape, q_half = shape((heads, rows, HEAD), BF16), shape((heads, half, HEAD), BF16)
@@ -490,11 +501,11 @@
         [kv, shape((half, depth), BF16), weights, table, table],
         [buffers, pltpu.SemaphoreType.DMA((3,))], flops, hbm=(0, 1, 2))
     kv1_a = onward(kv_a)
-    kv_b, = call(rest_keep_kernel, scalars, [partner, w_keep, cosine, sine], [kv], [buffers], flops)
+    key_weight, value_weight, own = lax.optimization_barrier((key_weight, value_weight, own))
+    send_a, kv_b = call(
+        middle_kernel, scalars, [own, partner, key_weight, value_weight, w_keep, cosine, sine], [kv, kv], [buffers],
+        2 * flops)
     kv1_b = onward(kv_b)
-    send_a, = call(functools.partial(send_kernel, part=0), scalars, [own, key_weight, value_weight, cosine, sine],
-                   [kv], [buffers],
-                   flops)
     kv_ya = swap(send_a, "sp")
     send_b, = call(functools.partial(send_kernel, part=1), scalars, [partner, key_weight, value_weight, cosine, sine],
                    [kv], [buffers],
@@ -524,9 +535,9 @@
     state = shape((heads, group, HEAD), F32)
     kv_scratch = [pltpu.VMEM((heads, group, HEAD), BF16)] * 2
     q, m, l, o = call(
-        local_kernel, scalars, [q_a, q_b, q_y, kv_a, kv_b, kv_ya, kv_yb, group0, near0, near1],
+        local_kernel, scalars, [q_a, q_b, q_y, kv_a, kv_b, kv_ya, kv_yb, group0, near0, upper],
         [shape((heads, group, HEAD), BF16), state, state, state],
-        kv_scratch + [pltpu.VMEM((heads, 2 * group, 4 * HEAD), F32)], 3 * 10 ** 9)
+        kv_scratch + [pltpu.VMEM((heads, 3 * group, 2 * HEAD), F32)], 3 * 10 ** 9)
     m, l, o, state_y = call(
         one_kernel, scalars, [q, m, l, o, kv1_a, kv1_b, kv1_ya, kv1_yb, group1, near1], [state, state, state, packed],
         kv_scratch + [pltpu.VMEM((heads, 2 * group, 2 * HEAD), F32), pltpu.VMEM((heads, group, HEAD), F32)]

time: 78.3 us -> 75.8 us (0.968)
  Pallas kernels: 22 us -> 20.4 us
  waiting for transfers between devices: 16.4 us -> 15.6 us
    ppermute x9, waiting for transfers between devices: 12.6 us -> 10.5 us  [swap(): lax.ppermute(x, axis, [(i, i ^ 1) for i in range(lax.axis_size(axis))])]
    pallas_call x10 -> x9, Pallas kernels: 19.2 us -> 17.6 us  [call(): pl.pallas_call(kernel, in_specs=[pl.BlockSpec(memory_space=pltpu.SMEM)] +...]
    ppermute x7, waiting for transfers between devices: 3.78 us -> 5.1 us  [onward(): return lax.ppermute(x, 'sp', [(i, i + 2) for i in range(n - 2)])]
    ppermute x9, starting transfers between devices: 8.61 us -> 7.69 us  [swap(): lax.ppermute(x, axis, [(i, i ^ 1) for i in range(lax.axis_size(axis))])]
    ppermute x7, starting transfers between devices: 25.5 us -> 26.3 us  [onward(): return lax.ppermute(x, 'sp', [(i, i + 2) for i in range(n - 2)])]
  transfers between devices with their start and end apart: 18 -> 18, of which waited for: 6 -> 8; matrix products, arithmetic and copies ran while one was open for 0% -> 0% of each run, Pallas kernels for 25% -> 23%
where the time goes in v3:
time: 75.8 us; the launch traced here: 75.5 us
  starting transfers between devices  38.7 us (51%)
  Pallas kernels  20.4 us (27%)
  waiting for transfers between devices  15.6 us (21%)
    ppermute x7, starting transfers between devices, onward(): return lax.ppermute(x, 'sp', [(i, i + 2) for i in range(n - 2)])  26.3 us
    pallas_call x9, Pallas kernels, call(): pl.pallas_call(kernel, in_specs=[pl.BlockSpec(memory_space=pltpu.SMEM)] +...  17.6 us
    ppermute x9, waiting for transfers between devices, swap(): lax.ppermute(x, axis, [(i, i ^ 1) for i in range(lax.axis_size(axis))])  10.5 us
    ppermute x9, starting transfers between devices, swap(): lax.ppermute(x, axis, [(i, i ^ 1) for i in range(lax.axis_size(axis))])  7.69 us
    ppermute x7, waiting for transfers between devices, onward(): return lax.ppermute(x, 'sp', [(i, i + 2) for i in range(n - 2)])  5.1 us
    ppermute x1, starting transfers between devices, body(): lax.ppermute(piece_diag, 'sp', [(i, (i ^ 1) + 2) for i in range(n - 2)])  3.41 us
    pallas_call x1, Pallas kernels, out_project(): pl.pallas_call(out_kernel, grid=(steps,), in_specs=[pl.BlockSpec(memory_s...  2.79 us
  transfers between devices with their start and end apart: 18, of which 8 were waited for; matrix products, arithmetic and copies ran while one was open for 0% of the time, Pallas kernels for 23%

profile of v3, /device:TPU:0, one launch (start us, length us, event | category | flops | bytes accessed | tf_op | source)
XLA Modules:
  0.0 75.5 jit_solution(8799701584599263819)
XLA Ops:
  0.0 0.5 collective-permute-start
  0.5 0.1 maximum_bitcast_fusion.inv_ref
  0.6 0.1 pad_add_fusion.sc_ref
  0.7 3.8 %shard_map.109 = (bf16[2,2,256,128]{3,2,1,0:T(8,128)(2,1)S(1)}, bf16[256,2048]{1,0:T(8,128)(2,1)S(1)}, bf16[2,2048,256]{2,1,0:T(8,128)(2,1)S(1)}, f32[2,256,128]{2,1,0:T(8,128)S(1)}, f32[2,256,128]{2,1,0:T(8,128)S(1)}) custom-call(s32[4]{0:T(128)S(1)} %pad_add_fusion.sc_ref, bf16[256,2048]{1,0:T(8,128)(2,1)} %x_hbm.1, bf16[2048,512]{1,0:T(8,128)(2,1)} %wk_ref.1, ...), custom_call_target="tpu_custom_call" | custom-call | flops 536870912 | tf_op jit(solution)/shard_map/pallas_call | solution.py:122
  4.5 4.5 %collective-permute-start.4 = (bf16[2,2,256,128]{3,2,1,0:T(8,128)(2,1)S(1)}, bf16[2,2,256,128]{3,2,1,0:T(8,128)(2,1)S(1)}, u32[]{:S(2)}, u32[]{:S(2)}) collective-permute-start(bf16[2,2,256,128]{3,2,1,0:T(8,128)(2,1)S(1)} %get-tuple-element.38.kva_ref), channel_id=1, source_target_pairs={{0,4},{2,6},{4,8},{6,10},{8,12},{10,14},{1,5},{3,7},{5,9},{7,11},{... | collective-permute-start | bytes 786440 | tf_op jit(solution)/shard_map/ppermute | solution.py:474
  9.0 0.0 collective-permute-done.xp_ref.x_ref
  9.0 0.0 copy-done.2
  9.0 0.0 copy-start
  9.0 0.0 copy-start.1
  9.0 2.5 %shard_map.110 = (bf16[2,256,128]{2,1,0:T(8,128)(2,1)S(1)}, bf16[2,256,128]{2,1,0:T(8,128)(2,1)S(1)}, bf16[2,512,128]{2,1,0:T(8,128)(2,1)S(1)}, bf16[1,2,256,128]{3,2,1,0:T(8,128)(2,1)S(1)}) custom-call(s32[4]{0:T(128)S(1)} %pad_add_fusion.sc_ref, bf16[256,2048]{1,0:T(8,128)(2,1)S(1)} %get-tuple-element.32.xo_ref, ...), custom_call_target="tpu_custom_call" | custom-call | flops 1073741824 | tf_op jit(solution)/shard_map/pallas_call | solution.py:122
  11.5 1.6 %collective-permute-start.1 = (bf16[2,512,128]{2,1,0:T(8,128)(2,1)S(1)}, bf16[2,512,128]{2,1,0:T(8,128)(2,1)S(1)}, u32[]{:S(2)}, u32[]{:S(2)}) collective-permute-start(bf16[2,512,128]{2,1,0:T(8,128)(2,1)S(1)} %get-tuple-element.37), channel_id=1, source_target_pairs={{0,2},{2,0},{4,6},{6,4},{8,10},{10,8},{12,14},{14,12},{1,3},{3,1},... | collective-permute-start | bytes 786440 | tf_op jit(solution)/shard_map/ppermute | solution.py:469
  13.1 0.0 copy-done
  13.1 0.0 copy-done.1
  13.1 2.3 %shard_map.111 = (bf16[2,2,256,128]{3,2,1,0:T(8,128)(2,1)S(1)}, bf16[2,2,256,128]{3,2,1,0:T(8,128)(2,1)S(1)}) custom-call(s32[4]{0:T(128)S(1)} %pad_add_fusion.sc_ref, bf16[256,2048]{1,0:T(8,128)(2,1)S(1)} %get-tuple-element.32.xo_ref, bf16[256,2048]{1,0:T(8,128)(2,1)S(1)} %collective-permute-done.xp_ref.x_ref, bf16[2048,512]{1,0:T(8,128)(2,1)S(1)} %copy-done, ...), custom_call_target="tpu_custom_call" | custom-call | flops 1073741824 | tf_op jit(solution)/shard_map/pallas_call | solution.py:122
  15.3 0.0 copy-start.7
  15.4 0.0 copy-start.8
  15.4 0.0 copy-start.9
  15.4 3.6 %collective-permute-start.5 = (bf16[2,2,256,128]{3,2,1,0:T(8,128)(2,1)S(1)}, bf16[2,2,256,128]{3,2,1,0:T(8,128)(2,1)S(1)}, u32[]{:S(2)}, u32[]{:S(2)}) collective-permute-start(bf16[2,2,256,128]{3,2,1,0:T(8,128)(2,1)S(1)} %get-tuple-element.42.kvb_ref), channel_id=1, source_target_pairs={{0,4},{2,6},{4,8},{6,10},{8,12},{10,14},{1,5},{3,7},{5,9},{7,11},{... | collective-permute-start | bytes 786440 | tf_op jit(solution)/shard_map/ppermute | solution.py:474
  19.0 1.5 %shard_map.112 = bf16[2,2,256,128]{3,2,1,0:T(8,128)(2,1)S(1)} custom-call(s32[4]{0:T(128)S(1)} %pad_add_fusion.sc_ref, bf16[256,2048]{1,0:T(8,128)(2,1)S(1)} %collective-permute-done.xp_ref.x_ref, bf16[2048,512]{1,0:T(8,128)(2,1)S(1)} %copy-done, bf16[2048,512]{1,0:T(8,128)(2,1)S(1)} %copy-done.1, f32[2,256,128]{2,1,0:T(8,128)S(1)} %get-tuple-element.33.cos_ref, ...), custom_call_target="tpu_custom_call" | custom-call | flops 536870912 | tf_op jit(solution)/shard_map/pallas_call | solution.py:122
  20.5 0.6 collective-permute-start.3
  21.1 1.5 %collective-permute-start.2 = (bf16[2,2,256,128]{3,2,1,0:T(8,128)(2,1)S(1)}, bf16[2,2,256,128]{3,2,1,0:T(8,128)(2,1)S(1)}, u32[]{:S(2)}, u32[]{:S(2)}) collective-permute-start(bf16[2,2,256,128]{3,2,1,0:T(8,128)(2,1)S(1)} %get-tuple-element.43), channel_id=1, source_target_pairs={{0,2},{2,0},{4,6},{6,4},{8,10},{10,8},{12,14},{14,12},{1,3},{3,1},... | collective-permute-start | bytes 786440 | tf_op jit(solution)/shard_map/ppermute | solution.py:469
  22.6 0.0 collective-permute-done.4.kva_ref
  22.6 0.0 collective-permute-done.1.qy_ref
  22.7 1.3 %collective-permute-start.14 = (bf16[2,512,128]{2,1,0:T(8,128)(2,1)S(1)}, bf16[2,512,128]{2,1,0:T(8,128)(2,1)S(1)}, u32[]{:S(2)}, u32[]{:S(2)}) collective-permute-start(bf16[2,512,128]{2,1,0:T(8,128)(2,1)S(1)} %pad_maximum_fusion.2), channel_id=1, source_target_pairs={{4,0},{6,2},{8,4},{10,6},{12,8},{14,10},{5,1},{7,3},{9,5},{11,7},{... | collective-permute-start | bytes 786440 | tf_op jit(solution)/shard_map/ppermute | solution.py:521
  24.0 0.7 collective-permute-done.5.kvb_ref
  24.7 4.4 %collective-permute-start.8 = (bf16[2,2,256,128]{3,2,1,0:T(8,128)(2,1)S(1)}, bf16[2,2,256,128]{3,2,1,0:T(8,128)(2,1)S(1)}, u32[]{:S(2)}, u32[]{:S(2)}) collective-permute-start(bf16[2,2,256,128]{3,2,1,0:T(8,128)(2,1)S(1)} %pad_maximum_fusion), channel_id=1, source_target_pairs={{0,4},{2,6},{4,8},{6,10},{8,12},{10,14},{1,5},{3,7},{5,9},{7,11},{... | collective-permute-start | bytes 786440 | tf_op jit(solution)/shard_map/ppermute | solution.py:474
  29.1 0.7 collective-permute-done.3.kvyb_ref
  29.8 3.5 %collective-permute-start.7 = (bf16[2,2,256,128]{3,2,1,0:T(8,128)(2,1)S(1)}, bf16[2,2,256,128]{3,2,1,0:T(8,128)(2,1)S(1)}, u32[]{:S(2)}, u32[]{:S(2)}) collective-permute-start(bf16[2,2,256,128]{3,2,1,0:T(8,128)(2,1)S(1)} %collective-permute-done.3.kvyb_ref), channel_id=1, source_target_pairs={{0,4},{2,6},{4,8},{6,10},{8,12},{10,14},{1,5},{3,7},{5,9},{7,11},{... | collective-permute-start | bytes 786440 | tf_op jit(solution)/shard_map/ppermute | solution.py:474
  33.2 0.8 %collective-permute-done.2.kvya_ref = bf16[2,2,256,128]{3,2,1,0:T(8,128)(2,1)S(1)} collective-permute-done((bf16[2,2,256,128]{3,2,1,0:T(8,128)(2,1)S(1)}, bf16[2,2,256,128]{3,2,1,0:T(8,128)(2,1)S(1)}, u32[]{:S(2)}, u32[]{:S(2)}) %collective-permute-start.2) | collective-permute-done | bytes 262176 | tf_op jit(solution)/shard_map/ppermute | solution.py:469
  34.1 3.5 %collective-permute-start.6 = (bf16[2,2,256,128]{3,2,1,0:T(8,128)(2,1)S(1)}, bf16[2,2,256,128]{3,2,1,0:T(8,128)(2,1)S(1)}, u32[]{:S(2)}, u32[]{:S(2)}) collective-permute-start(bf16[2,2,256,128]{3,2,1,0:T(8,128)(2,1)S(1)} %collective-permute-done.2.kvya_ref), channel_id=1, source_target_pairs={{0,4},{2,6},{4,8},{6,10},{8,12},{10,14},{1,5},{3,7},{5,9},{7,11},{... | collective-permute-start | bytes 786440 | tf_op jit(solution)/shard_map/ppermute | solution.py:474
  37.6 0.0 copy-done.7
  37.6 0.0 copy-start.6
  37.6 3.0 %shard_map.113 = (bf16[2,1024,128]{2,1,0:T(8,128)(2,1)S(1)}, f32[2,1024,128]{2,1,0:T(8,128)S(1)}, f32[2,1024,128]{2,1,0:T(8,128)S(1)}, f32[2,1024,128]{2,1,0:T(8,128)S(1)}) custom-call(s32[4]{0:T(128)S(1)} %pad_add_fusion.sc_ref, bf16[2,256,128]{2,1,0:T(8,128)(2,1)S(1)} %get-tuple-element.35.qa_ref, bf16[2,256,128]{2,1,0:T(8,128)(2,1)S(1)} %get-tuple-element.36.qb_ref, ...), custom_call_target="tpu_custom_call" | custom-call | flops 3000000000 | tf_op jit(solution)/shard_map/pallas_call | solution.py:122
  40.6 0.0 copy-start.4
  40.7 0.0 copy-start.5
  40.7 0.0 collective-permute-done.14.qn_ref
  40.7 0.7 collective-permute-done.7.kvyb_ref
  41.4 3.7 %collective-permute-done.6.kvya_ref = bf16[2,2,256,128]{3,2,1,0:T(8,128)(2,1)S(1)} collective-permute-done((bf16[2,2,256,128]{3,2,1,0:T(8,128)(2,1)S(1)}, bf16[2,2,256,128]{3,2,1,0:T(8,128)(2,1)S(1)}, u32[]{:S(2)}, u32[]{:S(2)}) %collective-permute-start.6) | collective-permute-done | bytes 262176 | tf_op jit(solution)/shard_map/ppermute | solution.py:474
  45.1 0.0 copy-done.6
  45.1 1.2 %shard_map.116 = (bf16[560,128]{1,0:T(8,128)(2,1)S(1)}, bf16[560,128]{1,0:T(8,128)(2,1)S(1)}) custom-call(s32[4]{0:T(128)S(1)} %pad_add_fusion.sc_ref, bf16[2,512,128]{2,1,0:T(8,128)(2,1)S(1)} %collective-permute-done.14.qn_ref, bf16[2,2,256,128]{3,2,1,0:T(8,128)(2,1)S(1)} %collective-permute-done.4.kva_ref, ...), custom_call_target="tpu_custom_call" | custom-call | flops 1000000000 | tf_op jit(solution)/shard_map/pallas_call | solution.py:122
  46.4 4.4 %collective-permute-start.15 = (bf16[560,128]{1,0:T(8,128)(2,1)S(1)}, bf16[560,128]{1,0:T(8,128)(2,1)S(1)}, u32[]{:S(2)}, u32[]{:S(2)}) collective-permute-start(bf16[560,128]{1,0:T(8,128)(2,1)S(1)} %get-tuple-element.55), channel_id=1, source_target_pairs={{0,4},{2,6},{4,8},{6,10},{8,12},{10,14},{1,5},{3,7},{5,9},{7,11},{... | collective-permute-start | bytes 430088 | tf_op jit(solution)/shard_map/ppermute | solution.py:474
  50.8 3.4 %collective-permute-start.16 = (bf16[560,128]{1,0:T(8,128)(2,1)S(1)}, bf16[560,128]{1,0:T(8,128)(2,1)S(1)}, u32[]{:S(2)}, u32[]{:S(2)}) collective-permute-start(bf16[560,128]{1,0:T(8,128)(2,1)S(1)} %get-tuple-element.56), channel_id=1, source_target_pairs={{0,6},{2,4},{4,10},{6,8},{8,14},{10,12},{1,7},{3,5},{5,11},{7,9},{... | collective-permute-start | bytes 430088 | tf_op jit(solution)/shard_map/ppermute | solution.py:533
  54.3 2.5 %collective-permute-start.9 = (bf16[2,2,256,128]{3,2,1,0:T(8,128)(2,1)S(1)}, bf16[2,2,256,128]{3,2,1,0:T(8,128)(2,1)S(1)}, u32[]{:S(2)}, u32[]{:S(2)}) collective-permute-start(bf16[2,2,256,128]{3,2,1,0:T(8,128)(2,1)S(1)} %pad_maximum_fusion.1), channel_id=1, source_target_pairs={{0,4},{2,6},{4,8},{6,10},{8,12},{10,14},{1,5},{3,7},{5,9},{7,11},{... | collective-permute-start | bytes 786440 | tf_op jit(solution)/shard_map/ppermute | solution.py:474
  56.8 0.0 copy-done.4
  56.8 0.0 copy-done.5
  56.8 0.9 %shard_map.114 = (f32[2,1024,128]{2,1,0:T(8,128)S(1)}, f32[2,1024,128]{2,1,0:T(8,128)S(1)}, f32[2,1024,128]{2,1,0:T(8,128)S(1)}, bf16[560,128]{1,0:T(8,128)(2,1)S(1)}) custom-call(s32[4]{0:T(128)S(1)} %pad_add_fusion.sc_ref, bf16[2,1024,128]{2,1,0:T(8,128)(2,1)S(1)} %get-tuple-element.44.q_ref, ...), custom_call_target="tpu_custom_call", output_to_operand_aliasing={{0}: (2, {}), {1}: (3, {}), {2}: (4, {})} | custom-call | flops 1000000000 | tf_op jit(solution)/shard_map/pallas_call | solution.py:122
  57.7 1.6 %collective-permute-start.13 = (bf16[560,128]{1,0:T(8,128)(2,1)S(1)}, bf16[560,128]{1,0:T(8,128)(2,1)S(1)}, u32[]{:S(2)}, u32[]{:S(2)}) collective-permute-start(bf16[560,128]{1,0:T(8,128)(2,1)S(1)} %get-tuple-element.53), channel_id=1, source_target_pairs={{0,2},{2,0},{4,6},{6,4},{8,10},{10,8},{12,14},{14,12},{1,3},{3,1},... | collective-permute-start | bytes 430088 | tf_op jit(solution)/shard_map/ppermute | solution.py:469
  59.3 0.0 collective-permute-done.15.own_ref
  59.3 0.0 collective-permute-done.16.diag_ref
  59.3 3.5 %collective-permute-done.13.state_ref = bf16[560,128]{1,0:T(8,128)(2,1)S(1)} collective-permute-done((bf16[560,128]{1,0:T(8,128)(2,1)S(1)}, bf16[560,128]{1,0:T(8,128)(2,1)S(1)}, u32[]{:S(2)}, u32[]{:S(2)}) %collective-permute-start.13) | collective-permute-done | bytes 143392 | tf_op jit(solution)/shard_map/ppermute | solution.py:469
  62.8 1.6 %shard_map.117.own_ref = bf16[2,512,128]{2,1,0:T(8,128)(2,1)S(1)} custom-call(s32[4]{0:T(128)S(1)} %pad_add_fusion.sc_ref, f32[2,1024,128]{2,1,0:T(8,128)S(1)} %get-tuple-element.48.m_ref, f32[2,1024,128]{2,1,0:T(8,128)S(1)} %get-tuple-element.49.l_ref, f32[2,1024,128]{2,1,0:T(8,128)S(1)} %get-tuple-element.50.o_ref, ...), custom_call_target="tpu_custom_call" | custom-call | flops 1000000000 | tf_op jit(solution)/shard_map/pallas_call | solution.py:122
  64.4 0.0 copy-start.3
  64.4 0.1 collective-permute-start.17
  64.5 0.0 collective-permute-done.8.kvo_ref
  64.5 0.0 collective-permute-done.9.kvy_ref
  64.5 0.9 %shard_map.115 = (bf16[512,128]{1,0:T(8,128)(2,1)S(1)}, bf16[512,128]{1,0:T(8,128)(2,1)S(1)}) custom-call(s32[4]{0:T(128)S(1)} %pad_add_fusion.sc_ref, bf16[2,1024,128]{2,1,0:T(8,128)(2,1)S(1)} %get-tuple-element.44.q_ref, f32[2,1024,128]{2,1,0:T(8,128)S(1)} %get-tuple-element.48.m_ref, f32[2,1024,128]{2,1,0:T(8,128)S(1)} %get-tuple-element.49.l_ref, ...), custom_call_target="tpu_custom_call" | custom-call | flops 1000000000 | tf_op jit(solution)/shard_map/pallas_call | solution.py:122
  65.4 1.6 %collective-permute-start.10 = (bf16[512,128]{1,0:T(8,128)(2,1)S(1)}, bf16[512,128]{1,0:T(8,128)(2,1)S(1)}, u32[]{:S(2)}, u32[]{:S(2)}) collective-permute-start(bf16[512,128]{1,0:T(8,128)(2,1)S(1)} %get-tuple-element.52), channel_id=1, source_target_pairs={{0,2},{2,0},{4,6},{6,4},{8,10},{10,8},{12,14},{14,12},{1,3},{3,1},... | collective-permute-start | bytes 393224 | tf_op jit(solution)/shard_map/ppermute | solution.py:469
  67.0 0.2 collective-permute-start.11
  67.2 4.1 %collective-permute-done.10.b_ref = bf16[512,128]{1,0:T(8,128)(2,1)S(1)} collective-permute-done((bf16[512,128]{1,0:T(8,128)(2,1)S(1)}, bf16[512,128]{1,0:T(8,128)(2,1)S(1)}, u32[]{:S(2)}, u32[]{:S(2)}) %collective-permute-start.10) | collective-permute-done | bytes 131104 | tf_op jit(solution)/shard_map/ppermute | solution.py:469
  71.4 0.0 collective-permute-start.12
  71.4 0.0 collective-permute-done.11.c_ref
  71.4 0.0 collective-permute-done.17.tp_ref
  71.4 1.3 %collective-permute-done.12.d_ref = bf16[512,128]{1,0:T(8,128)(2,1)S(1)} collective-permute-done((bf16[512,128]{1,0:T(8,128)(2,1)S(1)}, bf16[512,128]{1,0:T(8,128)(2,1)S(1)}, u32[]{:S(2)}, u32[]{:S(2)}) %collective-permute-start.12) | collective-permute-done | bytes 131104 | tf_op jit(solution)/shard_map/ppermute | solution.py:469
  72.7 2.8 %out_project.1 = bf16[512,1024]{1,0:T(8,128)(2,1)} custom-call(s32[4]{0:T(128)S(1)} %pad_add_fusion.sc_ref, bf16[512,128]{1,0:T(8,128)(2,1)S(1)} %get-tuple-element.51.a_ref, bf16[512,128]{1,0:T(8,128)(2,1)S(1)} %collective-permute-done.10.b_ref, bf16[512,128]{1,0:T(8,128)(2,1)S(1)} %collective-permute-done.11.c_ref, ...), custom_call_target="tpu_custom_call" | custom-call | flops 1073741824 | tf_op jit(solution)/shard_map/out_project/pallas_call | solution.py:456
  (13 shorter events, 0.2 us)
Async XLA Ops:
  0.0 9.0 %collective-permute-start = (bf16[256,2048]{1,0:T(8,128)(2,1)}, bf16[256,2048]{1,0:T(8,128)(2,1)S(1)}, u32[]{:S(2)}, u32[]{:S(2)}) collective-permute-start(bf16[256,2048]{1,0:T(8,128)(2,1)} %x_hbm.1), channel_id=1, source_target_pairs={{0,1},{1,0},{2,3},{3,2},{4,5},{5,4},{6,7},{7,6},{8,9},{9,8},{10,11... | collective-permute-start | bytes 3145736 | tf_op jit(solution)/shard_map/ppermute | solution.py:469
  0.7 8.3 %copy-start.2 = (bf16[2048,512]{1,0:T(8,128)(2,1)S(1)}, bf16[2048,512]{1,0:T(8,128)(2,1)}, u32[]{:S(2)}) copy-start(bf16[2048,512]{1,0:T(8,128)(2,1)} %w_ref.2) | copy-start | bytes 6291460
  4.5 18.2 %collective-permute-start.4 = (bf16[2,2,256,128]{3,2,1,0:T(8,128)(2,1)S(1)}, bf16[2,2,256,128]{3,2,1,0:T(8,128)(2,1)S(1)}, u32[]{:S(2)}, u32[]{:S(2)}) collective-permute-start(bf16[2,2,256,128]{3,2,1,0:T(8,128)(2,1)S(1)} %get-tuple-element.38.kva_ref), channel_id=1, source_target_pairs={{0,4},{2,6},{4,8},{6,10},{8,12},{10,14},{1,5},{3,7},{5,9},{7,11},{... | collective-permute-start | bytes 786440 | tf_op jit(solution)/shard_map/ppermute | solution.py:474
  9.0 4.1 %copy-start = (bf16[2048,512]{1,0:T(8,128)(2,1)S(1)}, bf16[2048,512]{1,0:T(8,128)(2,1)}, u32[]{:S(2)}) copy-start(bf16[2048,512]{1,0:T(8,128)(2,1)} %wk_ref.1) | copy-start | bytes 6291460
  9.0 4.1 %copy-start.1 = (bf16[2048,512]{1,0:T(8,128)(2,1)S(1)}, bf16[2048,512]{1,0:T(8,128)(2,1)}, u32[]{:S(2)}) copy-start(bf16[2048,512]{1,0:T(8,128)(2,1)} %wv_ref.1) | copy-start | bytes 6291460
  11.5 11.2 %collective-permute-start.1 = (bf16[2,512,128]{2,1,0:T(8,128)(2,1)S(1)}, bf16[2,512,128]{2,1,0:T(8,128)(2,1)S(1)}, u32[]{:S(2)}, u32[]{:S(2)}) collective-permute-start(bf16[2,512,128]{2,1,0:T(8,128)(2,1)S(1)} %get-tuple-element.37), channel_id=1, source_target_pairs={{0,2},{2,0},{4,6},{6,4},{8,10},{10,8},{12,14},{14,12},{1,3},{3,1},... | collective-permute-start | bytes 786440 | tf_op jit(solution)/shard_map/ppermute | solution.py:469
  15.3 22.2 %copy-start.7 = (f32[256,256]{1,0:T(8,128)S(1)}, f32[256,256]{1,0:T(8,128)}, u32[]{:S(2)}) copy-start(f32[256,256]{1,0:T(8,128)} %constant.50.clone.group_ref) | copy-start | bytes 786436
  15.4 22.2 %copy-start.8 = (f32[256,256]{1,0:T(8,128)S(1)}, f32[256,256]{1,0:T(8,128)}, u32[]{:S(2)}) copy-start(f32[256,256]{1,0:T(8,128)} %constant.51.clone.near0_ref) | copy-start | bytes 786436
  15.4 22.2 %copy-start.9 = (f32[128,256]{1,0:T(8,128)S(1)}, f32[128,256]{1,0:T(8,128)}, u32[]{:S(2)}) copy-start(f32[128,256]{1,0:T(8,128)} %constant.52.clone.near1_ref) | copy-start | bytes 393220
  15.4 9.3 %collective-permute-start.5 = (bf16[2,2,256,128]{3,2,1,0:T(8,128)(2,1)S(1)}, bf16[2,2,256,128]{3,2,1,0:T(8,128)(2,1)S(1)}, u32[]{:S(2)}, u32[]{:S(2)}) collective-permute-start(bf16[2,2,256,128]{3,2,1,0:T(8,128)(2,1)S(1)} %get-tuple-element.42.kvb_ref), channel_id=1, source_target_pairs={{0,4},{2,6},{4,8},{6,10},{8,12},{10,14},{1,5},{3,7},{5,9},{7,11},{... | collective-permute-start | bytes 786440 | tf_op jit(solution)/shard_map/ppermute | solution.py:474
  20.5 9.2 %collective-permute-start.3 = (bf16[2,2,256,128]{3,2,1,0:T(8,128)(2,1)S(1)}, bf16[2,2,256,128]{3,2,1,0:T(8,128)(2,1)S(1)}, u32[]{:S(2)}, u32[]{:S(2)}) collective-permute-start(bf16[2,2,256,128]{3,2,1,0:T(8,128)(2,1)S(1)} %shard_map.112), channel_id=1, source_target_pairs={{0,2},{2,0},{4,6},{6,4},{8,10},{10,8},{12,14},{14,12},{1,3},{3,1},... | collective-permute-start | bytes 786440 | tf_op jit(solution)/shard_map/ppermute | solution.py:469
  21.1 13.0 %collective-permute-start.2 = (bf16[2,2,256,128]{3,2,1,0:T(8,128)(2,1)S(1)}, bf16[2,2,256,128]{3,2,1,0:T(8,128)(2,1)S(1)}, u32[]{:S(2)}, u32[]{:S(2)}) collective-permute-start(bf16[2,2,256,128]{3,2,1,0:T(8,128)(2,1)S(1)} %get-tuple-element.43), channel_id=1, source_target_pairs={{0,2},{2,0},{4,6},{6,4},{8,10},{10,8},{12,14},{14,12},{1,3},{3,1},... | collective-permute-start | bytes 786440 | tf_op jit(solution)/shard_map/ppermute | solution.py:469
  22.7 18.0 %collective-permute-start.14 = (bf16[2,512,128]{2,1,0:T(8,128)(2,1)S(1)}, bf16[2,512,128]{2,1,0:T(8,128)(2,1)S(1)}, u32[]{:S(2)}, u32[]{:S(2)}) collective-permute-start(bf16[2,512,128]{2,1,0:T(8,128)(2,1)S(1)} %pad_maximum_fusion.2), channel_id=1, source_target_pairs={{4,0},{6,2},{8,4},{10,6},{12,8},{14,10},{5,1},{7,3},{9,5},{11,7},{... | collective-permute-start | bytes 786440 | tf_op jit(solution)/shard_map/ppermute | solution.py:521
  24.7 39.8 %collective-permute-start.8 = (bf16[2,2,256,128]{3,2,1,0:T(8,128)(2,1)S(1)}, bf16[2,2,256,128]{3,2,1,0:T(8,128)(2,1)S(1)}, u32[]{:S(2)}, u32[]{:S(2)}) collective-permute-start(bf16[2,2,256,128]{3,2,1,0:T(8,128)(2,1)S(1)} %pad_maximum_fusion), channel_id=1, source_target_pairs={{0,4},{2,6},{4,8},{6,10},{8,12},{10,14},{1,5},{3,7},{5,9},{7,11},{... | collective-permute-start | bytes 786440 | tf_op jit(solution)/shard_map/ppermute | solution.py:474
  29.8 11.6 %collective-permute-start.7 = (bf16[2,2,256,128]{3,2,1,0:T(8,128)(2,1)S(1)}, bf16[2,2,256,128]{3,2,1,0:T(8,128)(2,1)S(1)}, u32[]{:S(2)}, u32[]{:S(2)}) collective-permute-start(bf16[2,2,256,128]{3,2,1,0:T(8,128)(2,1)S(1)} %collective-permute-done.3.kvyb_ref), channel_id=1, source_target_pairs={{0,4},{2,6},{4,8},{6,10},{8,12},{10,14},{1,5},{3,7},{5,9},{7,11},{... | collective-permute-start | bytes 786440 | tf_op jit(solution)/shard_map/ppermute | solution.py:474
  34.1 11.0 %collective-permute-start.6 = (bf16[2,2,256,128]{3,2,1,0:T(8,128)(2,1)S(1)}, bf16[2,2,256,128]{3,2,1,0:T(8,128)(2,1)S(1)}, u32[]{:S(2)}, u32[]{:S(2)}) collective-permute-start(bf16[2,2,256,128]{3,2,1,0:T(8,128)(2,1)S(1)} %collective-permute-done.2.kvya_ref), channel_id=1, source_target_pairs={{0,4},{2,6},{4,8},{6,10},{8,12},{10,14},{1,5},{3,7},{5,9},{7,11},{... | collective-permute-start | bytes 786440 | tf_op jit(solution)/shard_map/ppermute | solution.py:474
  37.6 7.5 %copy-start.6 = (f32[128,128]{1,0:T(8,128)S(1)}, f32[128,128]{1,0:T(8,128)}, u32[]{:S(2)}) copy-start(f32[128,128]{1,0:T(8,128)} %constant.49.clone.pair_ref) | copy-start | bytes 196612
  40.6 16.1 %copy-start.4 = (f32[256,256]{1,0:T(8,128)S(1)}, f32[256,256]{1,0:T(8,128)}, u32[]{:S(2)}) copy-start(f32[256,256]{1,0:T(8,128)} %constant.53.clone.group_ref) | copy-start | bytes 786436
  40.7 16.1 %copy-start.5 = (f32[256,256]{1,0:T(8,128)S(1)}, f32[256,256]{1,0:T(8,128)}, u32[]{:S(2)}) copy-start(f32[256,256]{1,0:T(8,128)} %constant.54.clone.near_ref) | copy-start | bytes 786436
  46.4 12.9 %collective-permute-start.15 = (bf16[560,128]{1,0:T(8,128)(2,1)S(1)}, bf16[560,128]{1,0:T(8,128)(2,1)S(1)}, u32[]{:S(2)}, u32[]{:S(2)}) collective-permute-start(bf16[560,128]{1,0:T(8,128)(2,1)S(1)} %get-tuple-element.55), channel_id=1, source_target_pairs={{0,4},{2,6},{4,8},{6,10},{8,12},{10,14},{1,5},{3,7},{5,9},{7,11},{... | collective-permute-start | bytes 430088 | tf_op jit(solution)/shard_map/ppermute | solution.py:474
  50.8 8.5 %collective-permute-start.16 = (bf16[560,128]{1,0:T(8,128)(2,1)S(1)}, bf16[560,128]{1,0:T(8,128)(2,1)S(1)}, u32[]{:S(2)}, u32[]{:S(2)}) collective-permute-start(bf16[560,128]{1,0:T(8,128)(2,1)S(1)} %get-tuple-element.56), channel_id=1, source_target_pairs={{0,6},{2,4},{4,10},{6,8},{8,14},{10,12},{1,7},{3,5},{5,11},{7,9},{... | collective-permute-start | bytes 430088 | tf_op jit(solution)/shard_map/ppermute | solution.py:533
  54.3 10.3 %collective-permute-start.9 = (bf16[2,2,256,128]{3,2,1,0:T(8,128)(2,1)S(1)}, bf16[2,2,256,128]{3,2,1,0:T(8,128)(2,1)S(1)}, u32[]{:S(2)}, u32[]{:S(2)}) collective-permute-start(bf16[2,2,256,128]{3,2,1,0:T(8,128)(2,1)S(1)} %pad_maximum_fusion.1), channel_id=1, source_target_pairs={{0,4},{2,6},{4,8},{6,10},{8,12},{10,14},{1,5},{3,7},{5,9},{7,11},{... | collective-permute-start | bytes 786440 | tf_op jit(solution)/shard_map/ppermute | solution.py:474
  57.7 5.2 %collective-permute-start.13 = (bf16[560,128]{1,0:T(8,128)(2,1)S(1)}, bf16[560,128]{1,0:T(8,128)(2,1)S(1)}, u32[]{:S(2)}, u32[]{:S(2)}) collective-permute-start(bf16[560,128]{1,0:T(8,128)(2,1)S(1)} %get-tuple-element.53), channel_id=1, source_target_pairs={{0,2},{2,0},{4,6},{6,4},{8,10},{10,8},{12,14},{14,12},{1,3},{3,1},... | collective-permute-start | bytes 430088 | tf_op jit(solution)/shard_map/ppermute | solution.py:469
  64.4 8.3 %copy-start.3 = (bf16[1024,1024]{1,0:T(8,128)(2,1)S(1)}, bf16[1024,1024]{1,0:T(8,128)(2,1)}, u32[]{:S(2)}) copy-start(bf16[1024,1024]{1,0:T(8,128)(2,1)} %w_ref.3) | copy-start | bytes 6291460
  64.4 6.9 %collective-permute-start.17 = (bf16[2,512,128]{2,1,0:T(8,128)(2,1)S(1)}, bf16[2,512,128]{2,1,0:T(8,128)(2,1)S(1)}, u32[]{:S(2)}, u32[]{:S(2)}) collective-permute-start(bf16[2,512,128]{2,1,0:T(8,128)(2,1)S(1)} %shard_map.117.own_ref), channel_id=1, source_target_pairs={{0,1},{1,0},{2,3},{3,2},{4,5},{5,4},{6,7},{7,6},{8,9},{9,8},{10,11... | collective-permute-start | bytes 786440 | tf_op jit(solution)/shard_map/ppermute | solution.py:469
  65.4 5.9 %collective-permute-start.10 = (bf16[512,128]{1,0:T(8,128)(2,1)S(1)}, bf16[512,128]{1,0:T(8,128)(2,1)S(1)}, u32[]{:S(2)}, u32[]{:S(2)}) collective-permute-start(bf16[512,128]{1,0:T(8,128)(2,1)S(1)} %get-tuple-element.52), channel_id=1, source_target_pairs={{0,2},{2,0},{4,6},{6,4},{8,10},{10,8},{12,14},{14,12},{1,3},{3,1},... | collective-permute-start | bytes 393224 | tf_op jit(solution)/shard_map/ppermute | solution.py:469
  67.0 4.3 %collective-permute-start.11 = (bf16[512,128]{1,0:T(8,128)(2,1)S(1)}, bf16[512,128]{1,0:T(8,128)(2,1)S(1)}, u32[]{:S(2)}, u32[]{:S(2)}) collective-permute-start(bf16[512,128]{1,0:T(8,128)(2,1)S(1)} %get-tuple-element.51.a_ref), channel_id=1, source_target_pairs={{0,1},{1,0},{2,3},{3,2},{4,5},{5,4},{6,7},{7,6},{8,9},{9,8},{10,11... | collective-permute-start | bytes 393224 | tf_op jit(solution)/shard_map/ppermute | solution.py:469
  71.4 1.3 %collective-permute-start.12 = (bf16[512,128]{1,0:T(8,128)(2,1)S(1)}, bf16[512,128]{1,0:T(8,128)(2,1)S(1)}, u32[]{:S(2)}, u32[]{:S(2)}) collective-permute-start(bf16[512,128]{1,0:T(8,128)(2,1)S(1)} %collective-permute-done.10.b_ref), channel_id=1, source_target_pairs={{0,1},{1,0},{2,3},{3,2},{4,5},{5,4},{6,7},{7,6},{8,9},{9,8},{10,11... | collective-permute-start | bytes 393224 | tf_op jit(solution)/shard_map/ppermute | solution.py:469

commit v4 on v3

--- a/solution.py
+++ b/solution.py
@@ -38,36 +38,37 @@
         out_ref[lead + (pl.ds(at, nq_half), slice(None))] = piece.astype(BF16)
 
 
-def kv_part(x_ref, w_refs, out_ref, cos_ref, sin_ref, buf_ref, ready=None):
-    slot = 0
+def kv_finish(acc, which, out_ref, cos_ref, sin_ref, buf_ref):
+    heads = acc.shape[1] // HEAD
+    for h in range(heads):
+        val = acc[:, h * HEAD:(h + 1) * HEAD]
+        if which == 0:
+            val = rotated(val, cos_ref[...], sin_ref[...])
+        place(out_ref, (h, which), val, buf_ref, (1 - which) * heads + h, None)
+
+
+def kv_part(x_ref, w_refs, out_ref, cos_ref, sin_ref, buf_ref):
     for which in (1, 0):
-        if ready is not None:
-            ready[which].wait()
         acc = jnp.dot(x_ref[...], w_refs[which][...], preferred_element_type=F32)
-        for h in range(acc.shape[1] // HEAD):
-            val = acc[:, h * HEAD:(h + 1) * HEAD]
-            if which == 0:
-                val = rotated(val, cos_ref[...], sin_ref[...])
-            place(out_ref, (h, which), val, buf_ref, slot, None)
-            slot += 1
-
-
-def weight_copies(wk_hbm, wv_hbm, w_ref, side, sems):
-    width = w_ref.shape[2]
-    column = pl.multiple_of(side * width, width)
-    return [pltpu.make_async_copy(hbm.at[:, pl.ds(column, width)], w_ref.at[which], sems.at[which])
-            for which, hbm in enumerate((wk_hbm, wv_hbm))]
+        kv_finish(acc, which, out_ref, cos_ref, sin_ref, buf_ref)
 
 
 def own_keep_kernel(sc_ref, x_hbm, wk_hbm, wv_hbm, inv_ref,
-                    out_ref, x_ref, w_ref, cos_ref, sin_ref, buf_ref, sems):
+                    out_ref, x_ref, w_ref, cos_ref, sin_ref, buf_ref, acc_ref, sems):
     tp, par, sp = sc_ref[0], sc_ref[1], sc_ref[3]
     half = x_ref.shape[0]
-    x_copy = pltpu.make_async_copy(x_hbm, x_ref, sems.at[2])
-    copies = weight_copies(wk_hbm, wv_hbm, w_ref, par, sems)
-    x_copy.start()
-    copies[1].start()
-    copies[0].start()
+    depth, width = w_ref.shape[1:]
+    column = pl.ds(pl.multiple_of(par * width, width), width)
+    cuts = [pl.ds(i * depth // 2, depth // 2) for i in range(2)]
+    copies = []
+    for i, cut in enumerate(cuts):
+        copies.append([
+            pltpu.make_async_copy(wk_hbm.at[cut, column], w_ref.at[0, cut], sems.at[i, 0]),
+            pltpu.make_async_copy(wv_hbm.at[cut, column], w_ref.at[1, cut], sems.at[i, 1]),
+            pltpu.make_async_copy(x_hbm.at[:, cut], x_ref.at[:, cut], sems.at[i, 2])])
+    for part in copies:
+        for i in (2, 1, 0):
+            part[i].start()
     steps = half // FAR_DILATION
     lane = lax.broadcasted_iota(jnp.int32, (2 * steps, HEAD), 1)
     row = lax.broadcasted_iota(jnp.int32, (2 * steps, HEAD), 0)
@@ -80,8 +81,15 @@
     sign = jnp.where(lane[:1] < HEAD // 2, -1.0, 1.0)[None]
     cos_ref[...] = (cos_c * cos_f - sin_c * sin_f).reshape(2, half, HEAD)
     sin_ref[...] = ((sin_c * cos_f + cos_c * sin_f) * sign).reshape(2, half, HEAD)
-    x_copy.wait()
-    kv_part(x_ref, (w_ref.at[0], w_ref.at[1]), out_ref, cos_ref.at[0], sin_ref.at[0], buf_ref, copies)
+    for i, cut in enumerate(cuts):
+        copies[i][2].wait()
+        for which in (1, 0):
+            copies[i][which].wait()
+            acc = jnp.dot(x_ref[:, cut], w_ref[which, cut], preferred_element_type=F32)
+            if i == 0:
+                acc_ref[which] = acc
+            else:
+                kv_finish(acc_ref[which] + acc, which, out_ref, cos_ref.at[0], sin_ref.at[0], buf_ref)
 
 
 def middle_kernel(sc_ref, xo_ref, xp_ref, wk_ref, wv_ref, w_ref, cos_ref, sin_ref, send_ref, keep_ref, buf_ref):
@@ -499,7 +507,7 @@
     kv_a, own, w_keep, cosine, sine = call(
         own_keep_kernel, scalars, [tokens, key_weight, value_weight, inverse],
         [kv, shape((half, depth), BF16), weights, table, table],
-        [buffers, pltpu.SemaphoreType.DMA((3,))], flops, hbm=(0, 1, 2))
+        [buffers, pltpu.VMEM((2, half, width), F32), pltpu.SemaphoreType.DMA((2, 3))], flops, hbm=(0, 1, 2))
     kv1_a = onward(kv_a)
     key_weight, value_weight, own = lax.optimization_barrier((key_weight, value_weight, own))
     send_a, kv_b = call(

time: 75.8 us -> 75.6 us (level)
  no operation moved by 1% of the time
where the time goes in v4:
time: 75.6 us; the launch traced here: 75.3 us
  starting transfers between devices  38.7 us (51%)
  Pallas kernels  20.2 us (27%)
  waiting for transfers between devices  15.7 us (21%)
    ppermute x7, starting transfers between devices, onward(): return lax.ppermute(x, 'sp', [(i, i + 2) for i in range(n - 2)])  26.3 us
    pallas_call x9, Pallas kernels, call(): pl.pallas_call(kernel, in_specs=[pl.BlockSpec(memory_space=pltpu.SMEM)] +...  17.4 us
    ppermute x9, waiting for transfers between devices, swap(): lax.ppermute(x, axis, [(i, i ^ 1) for i in range(lax.axis_size(axis))])  10.5 us
    ppermute x9, starting transfers between devices, swap(): lax.ppermute(x, axis, [(i, i ^ 1) for i in range(lax.axis_size(axis))])  7.67 us
    ppermute x7, waiting for transfers between devices, onward(): return lax.ppermute(x, 'sp', [(i, i + 2) for i in range(n - 2)])  5.17 us
    ppermute x1, starting transfers between devices, body(): lax.ppermute(piece_diag, 'sp', [(i, (i ^ 1) + 2) for i in range(n - 2)])  3.38 us
    pallas_call x1, Pallas kernels, out_project(): pl.pallas_call(out_kernel, grid=(steps,), in_specs=[pl.BlockSpec(memory_s...  2.79 us
  transfers between devices with their start and end apart: 18, of which 8 were waited for; matrix products, arithmetic and copies ran while one was open for 0% of the time, Pallas kernels for 23%

profile of v4, /device:TPU:0, one launch (start us, length us, event | category | flops | bytes accessed | tf_op | source)
XLA Modules:
  0.0 75.3 jit_solution(6813138751015902)
XLA Ops:
  0.0 0.5 collective-permute-start
  0.5 0.1 maximum_bitcast_fusion.inv_ref
  0.6 0.1 pad_add_fusion.sc_ref
  0.7 3.5 %shard_map.109 = (bf16[2,2,256,128]{3,2,1,0:T(8,128)(2,1)S(1)}, bf16[256,2048]{1,0:T(8,128)(2,1)S(1)}, bf16[2,2048,256]{2,1,0:T(8,128)(2,1)S(1)}, f32[2,256,128]{2,1,0:T(8,128)S(1)}, f32[2,256,128]{2,1,0:T(8,128)S(1)}) custom-call(s32[4]{0:T(128)S(1)} %pad_add_fusion.sc_ref, bf16[256,2048]{1,0:T(8,128)(2,1)} %x_hbm.1, bf16[2048,512]{1,0:T(8,128)(2,1)} %wk_ref.1, ...), custom_call_target="tpu_custom_call" | custom-call | flops 536870912 | tf_op jit(solution)/shard_map/pallas_call | solution.py:130
  4.2 4.5 %collective-permute-start.4 = (bf16[2,2,256,128]{3,2,1,0:T(8,128)(2,1)S(1)}, bf16[2,2,256,128]{3,2,1,0:T(8,128)(2,1)S(1)}, u32[]{:S(2)}, u32[]{:S(2)}) collective-permute-start(bf16[2,2,256,128]{3,2,1,0:T(8,128)(2,1)S(1)} %get-tuple-element.38.kva_ref), channel_id=1, source_target_pairs={{0,4},{2,6},{4,8},{6,10},{8,12},{10,14},{1,5},{3,7},{5,9},{7,11},{... | collective-permute-start | bytes 786440 | tf_op jit(solution)/shard_map/ppermute | solution.py:482
  8.7 0.0 collective-permute-done.xp_ref.x_ref
  8.7 0.0 copy-done.2
  8.7 0.0 copy-start
  8.7 0.0 copy-start.1
  8.8 2.5 %shard_map.110 = (bf16[2,256,128]{2,1,0:T(8,128)(2,1)S(1)}, bf16[2,256,128]{2,1,0:T(8,128)(2,1)S(1)}, bf16[2,512,128]{2,1,0:T(8,128)(2,1)S(1)}, bf16[1,2,256,128]{3,2,1,0:T(8,128)(2,1)S(1)}) custom-call(s32[4]{0:T(128)S(1)} %pad_add_fusion.sc_ref, bf16[256,2048]{1,0:T(8,128)(2,1)S(1)} %get-tuple-element.32.xo_ref, ...), custom_call_target="tpu_custom_call" | custom-call | flops 1073741824 | tf_op jit(solution)/shard_map/pallas_call | solution.py:130
  11.2 1.6 %collective-permute-start.1 = (bf16[2,512,128]{2,1,0:T(8,128)(2,1)S(1)}, bf16[2,512,128]{2,1,0:T(8,128)(2,1)S(1)}, u32[]{:S(2)}, u32[]{:S(2)}) collective-permute-start(bf16[2,512,128]{2,1,0:T(8,128)(2,1)S(1)} %get-tuple-element.37), channel_id=1, source_target_pairs={{0,2},{2,0},{4,6},{6,4},{8,10},{10,8},{12,14},{14,12},{1,3},{3,1},... | collective-permute-start | bytes 786440 | tf_op jit(solution)/shard_map/ppermute | solution.py:477
  12.8 0.0 copy-done
  12.8 0.0 copy-done.1
  12.8 2.3 %shard_map.111 = (bf16[2,2,256,128]{3,2,1,0:T(8,128)(2,1)S(1)}, bf16[2,2,256,128]{3,2,1,0:T(8,128)(2,1)S(1)}) custom-call(s32[4]{0:T(128)S(1)} %pad_add_fusion.sc_ref, bf16[256,2048]{1,0:T(8,128)(2,1)S(1)} %get-tuple-element.32.xo_ref, bf16[256,2048]{1,0:T(8,128)(2,1)S(1)} %collective-permute-done.xp_ref.x_ref, bf16[2048,512]{1,0:T(8,128)(2,1)S(1)} %copy-done, ...), custom_call_target="tpu_custom_call" | custom-call | flops 1073741824 | tf_op jit(solution)/shard_map/pallas_call | solution.py:130
  15.1 0.0 copy-start.7
  15.1 0.0 copy-start.8
  15.1 0.0 copy-start.9
  15.1 3.6 %collective-permute-start.5 = (bf16[2,2,256,128]{3,2,1,0:T(8,128)(2,1)S(1)}, bf16[2,2,256,128]{3,2,1,0:T(8,128)(2,1)S(1)}, u32[]{:S(2)}, u32[]{:S(2)}) collective-permute-start(bf16[2,2,256,128]{3,2,1,0:T(8,128)(2,1)S(1)} %get-tuple-element.42.kvb_ref), channel_id=1, source_target_pairs={{0,4},{2,6},{4,8},{6,10},{8,12},{10,14},{1,5},{3,7},{5,9},{7,11},{... | collective-permute-start | bytes 786440 | tf_op jit(solution)/shard_map/ppermute | solution.py:482
  18.8 1.5 %shard_map.112 = bf16[2,2,256,128]{3,2,1,0:T(8,128)(2,1)S(1)} custom-call(s32[4]{0:T(128)S(1)} %pad_add_fusion.sc_ref, bf16[256,2048]{1,0:T(8,128)(2,1)S(1)} %collective-permute-done.xp_ref.x_ref, bf16[2048,512]{1,0:T(8,128)(2,1)S(1)} %copy-done, bf16[2048,512]{1,0:T(8,128)(2,1)S(1)} %copy-done.1, f32[2,256,128]{2,1,0:T(8,128)S(1)} %get-tuple-element.33.cos_ref, ...), custom_call_target="tpu_custom_call" | custom-call | flops 536870912 | tf_op jit(solution)/shard_map/pallas_call | solution.py:130
  20.3 0.6 collective-permute-start.3
  20.8 1.5 %collective-permute-start.2 = (bf16[2,2,256,128]{3,2,1,0:T(8,128)(2,1)S(1)}, bf16[2,2,256,128]{3,2,1,0:T(8,128)(2,1)S(1)}, u32[]{:S(2)}, u32[]{:S(2)}) collective-permute-start(bf16[2,2,256,128]{3,2,1,0:T(8,128)(2,1)S(1)} %get-tuple-element.43), channel_id=1, source_target_pairs={{0,2},{2,0},{4,6},{6,4},{8,10},{10,8},{12,14},{14,12},{1,3},{3,1},... | collective-permute-start | bytes 786440 | tf_op jit(solution)/shard_map/ppermute | solution.py:477
  22.4 0.0 collective-permute-done.4.kva_ref
  22.4 0.0 collective-permute-done.1.qy_ref
  22.4 1.3 %collective-permute-start.14 = (bf16[2,512,128]{2,1,0:T(8,128)(2,1)S(1)}, bf16[2,512,128]{2,1,0:T(8,128)(2,1)S(1)}, u32[]{:S(2)}, u32[]{:S(2)}) collective-permute-start(bf16[2,512,128]{2,1,0:T(8,128)(2,1)S(1)} %pad_maximum_fusion.2), channel_id=1, source_target_pairs={{4,0},{6,2},{8,4},{10,6},{12,8},{14,10},{5,1},{7,3},{9,5},{11,7},{... | collective-permute-start | bytes 786440 | tf_op jit(solution)/shard_map/ppermute | solution.py:529
  23.7 0.7 collective-permute-done.5.kvb_ref
  24.5 4.4 %collective-permute-start.8 = (bf16[2,2,256,128]{3,2,1,0:T(8,128)(2,1)S(1)}, bf16[2,2,256,128]{3,2,1,0:T(8,128)(2,1)S(1)}, u32[]{:S(2)}, u32[]{:S(2)}) collective-permute-start(bf16[2,2,256,128]{3,2,1,0:T(8,128)(2,1)S(1)} %pad_maximum_fusion), channel_id=1, source_target_pairs={{0,4},{2,6},{4,8},{6,10},{8,12},{10,14},{1,5},{3,7},{5,9},{7,11},{... | collective-permute-start | bytes 786440 | tf_op jit(solution)/shard_map/ppermute | solution.py:482
  28.9 0.6 collective-permute-done.3.kvyb_ref
  29.5 3.5 %collective-permute-start.7 = (bf16[2,2,256,128]{3,2,1,0:T(8,128)(2,1)S(1)}, bf16[2,2,256,128]{3,2,1,0:T(8,128)(2,1)S(1)}, u32[]{:S(2)}, u32[]{:S(2)}) collective-permute-start(bf16[2,2,256,128]{3,2,1,0:T(8,128)(2,1)S(1)} %collective-permute-done.3.kvyb_ref), channel_id=1, source_target_pairs={{0,4},{2,6},{4,8},{6,10},{8,12},{10,14},{1,5},{3,7},{5,9},{7,11},{... | collective-permute-start | bytes 786440 | tf_op jit(solution)/shard_map/ppermute | solution.py:482
  33.0 0.8 %collective-permute-done.2.kvya_ref = bf16[2,2,256,128]{3,2,1,0:T(8,128)(2,1)S(1)} collective-permute-done((bf16[2,2,256,128]{3,2,1,0:T(8,128)(2,1)S(1)}, bf16[2,2,256,128]{3,2,1,0:T(8,128)(2,1)S(1)}, u32[]{:S(2)}, u32[]{:S(2)}) %collective-permute-start.2) | collective-permute-done | bytes 262176 | tf_op jit(solution)/shard_map/ppermute | solution.py:477
  33.8 3.5 %collective-permute-start.6 = (bf16[2,2,256,128]{3,2,1,0:T(8,128)(2,1)S(1)}, bf16[2,2,256,128]{3,2,1,0:T(8,128)(2,1)S(1)}, u32[]{:S(2)}, u32[]{:S(2)}) collective-permute-start(bf16[2,2,256,128]{3,2,1,0:T(8,128)(2,1)S(1)} %collective-permute-done.2.kvya_ref), channel_id=1, source_target_pairs={{0,4},{2,6},{4,8},{6,10},{8,12},{10,14},{1,5},{3,7},{5,9},{7,11},{... | collective-permute-start | bytes 786440 | tf_op jit(solution)/shard_map/ppermute | solution.py:482
  37.3 0.0 copy-done.7
  37.3 0.0 copy-done.8
  37.3 0.0 copy-done.9
  37.3 0.0 copy-start.6
  37.4 3.0 %shard_map.113 = (bf16[2,1024,128]{2,1,0:T(8,128)(2,1)S(1)}, f32[2,1024,128]{2,1,0:T(8,128)S(1)}, f32[2,1024,128]{2,1,0:T(8,128)S(1)}, f32[2,1024,128]{2,1,0:T(8,128)S(1)}) custom-call(s32[4]{0:T(128)S(1)} %pad_add_fusion.sc_ref, bf16[2,256,128]{2,1,0:T(8,128)(2,1)S(1)} %get-tuple-element.35.qa_ref, bf16[2,256,128]{2,1,0:T(8,128)(2,1)S(1)} %get-tuple-element.36.qb_ref, ...), custom_call_target="tpu_custom_call" | custom-call | flops 3000000000 | tf_op jit(solution)/shard_map/pallas_call | solution.py:130
  40.4 0.0 copy-start.4
  40.4 0.0 copy-start.5
  40.4 0.0 collective-permute-done.14.qn_ref
  40.4 0.7 collective-permute-done.7.kvyb_ref
  41.2 3.8 %collective-permute-done.6.kvya_ref = bf16[2,2,256,128]{3,2,1,0:T(8,128)(2,1)S(1)} collective-permute-done((bf16[2,2,256,128]{3,2,1,0:T(8,128)(2,1)S(1)}, bf16[2,2,256,128]{3,2,1,0:T(8,128)(2,1)S(1)}, u32[]{:S(2)}, u32[]{:S(2)}) %collective-permute-start.6) | collective-permute-done | bytes 262176 | tf_op jit(solution)/shard_map/ppermute | solution.py:482
  44.9 0.0 copy-done.6
  44.9 1.2 %shard_map.116 = (bf16[560,128]{1,0:T(8,128)(2,1)S(1)}, bf16[560,128]{1,0:T(8,128)(2,1)S(1)}) custom-call(s32[4]{0:T(128)S(1)} %pad_add_fusion.sc_ref, bf16[2,512,128]{2,1,0:T(8,128)(2,1)S(1)} %collective-permute-done.14.qn_ref, bf16[2,2,256,128]{3,2,1,0:T(8,128)(2,1)S(1)} %collective-permute-done.4.kva_ref, ...), custom_call_target="tpu_custom_call" | custom-call | flops 1000000000 | tf_op jit(solution)/shard_map/pallas_call | solution.py:130
  46.2 4.4 %collective-permute-start.15 = (bf16[560,128]{1,0:T(8,128)(2,1)S(1)}, bf16[560,128]{1,0:T(8,128)(2,1)S(1)}, u32[]{:S(2)}, u32[]{:S(2)}) collective-permute-start(bf16[560,128]{1,0:T(8,128)(2,1)S(1)} %get-tuple-element.55), channel_id=1, source_target_pairs={{0,4},{2,6},{4,8},{6,10},{8,12},{10,14},{1,5},{3,7},{5,9},{7,11},{... | collective-permute-start | bytes 430088 | tf_op jit(solution)/shard_map/ppermute | solution.py:482
  50.6 3.4 %collective-permute-start.16 = (bf16[560,128]{1,0:T(8,128)(2,1)S(1)}, bf16[560,128]{1,0:T(8,128)(2,1)S(1)}, u32[]{:S(2)}, u32[]{:S(2)}) collective-permute-start(bf16[560,128]{1,0:T(8,128)(2,1)S(1)} %get-tuple-element.56), channel_id=1, source_target_pairs={{0,6},{2,4},{4,10},{6,8},{8,14},{10,12},{1,7},{3,5},{5,11},{7,9},{... | collective-permute-start | bytes 430088 | tf_op jit(solution)/shard_map/ppermute | solution.py:541
  54.0 2.5 %collective-permute-start.9 = (bf16[2,2,256,128]{3,2,1,0:T(8,128)(2,1)S(1)}, bf16[2,2,256,128]{3,2,1,0:T(8,128)(2,1)S(1)}, u32[]{:S(2)}, u32[]{:S(2)}) collective-permute-start(bf16[2,2,256,128]{3,2,1,0:T(8,128)(2,1)S(1)} %pad_maximum_fusion.1), channel_id=1, source_target_pairs={{0,4},{2,6},{4,8},{6,10},{8,12},{10,14},{1,5},{3,7},{5,9},{7,11},{... | collective-permute-start | bytes 786440 | tf_op jit(solution)/shard_map/ppermute | solution.py:482
  56.5 0.9 %shard_map.114 = (f32[2,1024,128]{2,1,0:T(8,128)S(1)}, f32[2,1024,128]{2,1,0:T(8,128)S(1)}, f32[2,1024,128]{2,1,0:T(8,128)S(1)}, bf16[560,128]{1,0:T(8,128)(2,1)S(1)}) custom-call(s32[4]{0:T(128)S(1)} %pad_add_fusion.sc_ref, bf16[2,1024,128]{2,1,0:T(8,128)(2,1)S(1)} %get-tuple-element.44.q_ref, ...), custom_call_target="tpu_custom_call", output_to_operand_aliasing={{0}: (2, {}), {1}: (3, {}), {2}: (4, {})} | custom-call | flops 1000000000 | tf_op jit(solution)/shard_map/pallas_call | solution.py:130
  57.4 1.6 %collective-permute-start.13 = (bf16[560,128]{1,0:T(8,128)(2,1)S(1)}, bf16[560,128]{1,0:T(8,128)(2,1)S(1)}, u32[]{:S(2)}, u32[]{:S(2)}) collective-permute-start(bf16[560,128]{1,0:T(8,128)(2,1)S(1)} %get-tuple-element.53), channel_id=1, source_target_pairs={{0,2},{2,0},{4,6},{6,4},{8,10},{10,8},{12,14},{14,12},{1,3},{3,1},... | collective-permute-start | bytes 430088 | tf_op jit(solution)/shard_map/ppermute | solution.py:477
  59.0 0.0 collective-permute-done.15.own_ref
  59.0 0.0 collective-permute-done.16.diag_ref
  59.1 3.5 %collective-permute-done.13.state_ref = bf16[560,128]{1,0:T(8,128)(2,1)S(1)} collective-permute-done((bf16[560,128]{1,0:T(8,128)(2,1)S(1)}, bf16[560,128]{1,0:T(8,128)(2,1)S(1)}, u32[]{:S(2)}, u32[]{:S(2)}) %collective-permute-start.13) | collective-permute-done | bytes 143392 | tf_op jit(solution)/shard_map/ppermute | solution.py:477
  62.6 1.6 %shard_map.117.own_ref = bf16[2,512,128]{2,1,0:T(8,128)(2,1)S(1)} custom-call(s32[4]{0:T(128)S(1)} %pad_add_fusion.sc_ref, f32[2,1024,128]{2,1,0:T(8,128)S(1)} %get-tuple-element.48.m_ref, f32[2,1024,128]{2,1,0:T(8,128)S(1)} %get-tuple-element.49.l_ref, f32[2,1024,128]{2,1,0:T(8,128)S(1)} %get-tuple-element.50.o_ref, ...), custom_call_target="tpu_custom_call" | custom-call | flops 1000000000 | tf_op jit(solution)/shard_map/pallas_call | solution.py:130
  64.2 0.0 copy-start.3
  64.2 0.1 collective-permute-start.17
  64.3 0.0 collective-permute-done.8.kvo_ref
  64.3 0.0 collective-permute-done.9.kvy_ref
  64.3 0.9 %shard_map.115 = (bf16[512,128]{1,0:T(8,128)(2,1)S(1)}, bf16[512,128]{1,0:T(8,128)(2,1)S(1)}) custom-call(s32[4]{0:T(128)S(1)} %pad_add_fusion.sc_ref, bf16[2,1024,128]{2,1,0:T(8,128)(2,1)S(1)} %get-tuple-element.44.q_ref, f32[2,1024,128]{2,1,0:T(8,128)S(1)} %get-tuple-element.48.m_ref, f32[2,1024,128]{2,1,0:T(8,128)S(1)} %get-tuple-element.49.l_ref, ...), custom_call_target="tpu_custom_call" | custom-call | flops 1000000000 | tf_op jit(solution)/shard_map/pallas_call | solution.py:130
  65.2 1.6 %collective-permute-start.10 = (bf16[512,128]{1,0:T(8,128)(2,1)S(1)}, bf16[512,128]{1,0:T(8,128)(2,1)S(1)}, u32[]{:S(2)}, u32[]{:S(2)}) collective-permute-start(bf16[512,128]{1,0:T(8,128)(2,1)S(1)} %get-tuple-element.52), channel_id=1, source_target_pairs={{0,2},{2,0},{4,6},{6,4},{8,10},{10,8},{12,14},{14,12},{1,3},{3,1},... | collective-permute-start | bytes 393224 | tf_op jit(solution)/shard_map/ppermute | solution.py:477
  66.8 0.2 collective-permute-start.11
  67.0 4.1 %collective-permute-done.10.b_ref = bf16[512,128]{1,0:T(8,128)(2,1)S(1)} collective-permute-done((bf16[512,128]{1,0:T(8,128)(2,1)S(1)}, bf16[512,128]{1,0:T(8,128)(2,1)S(1)}, u32[]{:S(2)}, u32[]{:S(2)}) %collective-permute-start.10) | collective-permute-done | bytes 131104 | tf_op jit(solution)/shard_map/ppermute | solution.py:477
  71.1 0.0 collective-permute-start.12
  71.1 0.0 collective-permute-done.11.c_ref
  71.1 0.0 collective-permute-done.17.tp_ref
  71.1 1.3 %collective-permute-done.12.d_ref = bf16[512,128]{1,0:T(8,128)(2,1)S(1)} collective-permute-done((bf16[512,128]{1,0:T(8,128)(2,1)S(1)}, bf16[512,128]{1,0:T(8,128)(2,1)S(1)}, u32[]{:S(2)}, u32[]{:S(2)}) %collective-permute-start.12) | collective-permute-done | bytes 131104 | tf_op jit(solution)/shard_map/ppermute | solution.py:477
  72.5 2.8 %out_project.1 = bf16[512,1024]{1,0:T(8,128)(2,1)} custom-call(s32[4]{0:T(128)S(1)} %pad_add_fusion.sc_ref, bf16[512,128]{1,0:T(8,128)(2,1)S(1)} %get-tuple-element.51.a_ref, bf16[512,128]{1,0:T(8,128)(2,1)S(1)} %collective-permute-done.10.b_ref, bf16[512,128]{1,0:T(8,128)(2,1)S(1)} %collective-permute-done.11.c_ref, ...), custom_call_target="tpu_custom_call" | custom-call | flops 1073741824 | tf_op jit(solution)/shard_map/out_project/pallas_call | solution.py:464
  (13 shorter events, 0.2 us)
Async XLA Ops:
  0.0 8.7 %collective-permute-start = (bf16[256,2048]{1,0:T(8,128)(2,1)}, bf16[256,2048]{1,0:T(8,128)(2,1)S(1)}, u32[]{:S(2)}, u32[]{:S(2)}) collective-permute-start(bf16[256,2048]{1,0:T(8,128)(2,1)} %x_hbm.1), channel_id=1, source_target_pairs={{0,1},{1,0},{2,3},{3,2},{4,5},{5,4},{6,7},{7,6},{8,9},{9,8},{10,11... | collective-permute-start | bytes 3145736 | tf_op jit(solution)/shard_map/ppermute | solution.py:477
  0.7 8.1 %copy-start.2 = (bf16[2048,512]{1,0:T(8,128)(2,1)S(1)}, bf16[2048,512]{1,0:T(8,128)(2,1)}, u32[]{:S(2)}) copy-start(bf16[2048,512]{1,0:T(8,128)(2,1)} %w_ref.2) | copy-start | bytes 6291460
  4.2 18.1 %collective-permute-start.4 = (bf16[2,2,256,128]{3,2,1,0:T(8,128)(2,1)S(1)}, bf16[2,2,256,128]{3,2,1,0:T(8,128)(2,1)S(1)}, u32[]{:S(2)}, u32[]{:S(2)}) collective-permute-start(bf16[2,2,256,128]{3,2,1,0:T(8,128)(2,1)S(1)} %get-tuple-element.38.kva_ref), channel_id=1, source_target_pairs={{0,4},{2,6},{4,8},{6,10},{8,12},{10,14},{1,5},{3,7},{5,9},{7,11},{... | collective-permute-start | bytes 786440 | tf_op jit(solution)/shard_map/ppermute | solution.py:482
  8.7 4.1 %copy-start = (bf16[2048,512]{1,0:T(8,128)(2,1)S(1)}, bf16[2048,512]{1,0:T(8,128)(2,1)}, u32[]{:S(2)}) copy-start(bf16[2048,512]{1,0:T(8,128)(2,1)} %wk_ref.1) | copy-start | bytes 6291460
  8.7 4.1 %copy-start.1 = (bf16[2048,512]{1,0:T(8,128)(2,1)S(1)}, bf16[2048,512]{1,0:T(8,128)(2,1)}, u32[]{:S(2)}) copy-start(bf16[2048,512]{1,0:T(8,128)(2,1)} %wv_ref.1) | copy-start | bytes 6291460
  11.2 11.2 %collective-permute-start.1 = (bf16[2,512,128]{2,1,0:T(8,128)(2,1)S(1)}, bf16[2,512,128]{2,1,0:T(8,128)(2,1)S(1)}, u32[]{:S(2)}, u32[]{:S(2)}) collective-permute-start(bf16[2,512,128]{2,1,0:T(8,128)(2,1)S(1)} %get-tuple-element.37), channel_id=1, source_target_pairs={{0,2},{2,0},{4,6},{6,4},{8,10},{10,8},{12,14},{14,12},{1,3},{3,1},... | collective-permute-start | bytes 786440 | tf_op jit(solution)/shard_map/ppermute | solution.py:477
  15.1 22.2 %copy-start.7 = (f32[256,256]{1,0:T(8,128)S(1)}, f32[256,256]{1,0:T(8,128)}, u32[]{:S(2)}) copy-start(f32[256,256]{1,0:T(8,128)} %constant.50.clone.group_ref) | copy-start | bytes 786436
  15.1 22.2 %copy-start.8 = (f32[256,256]{1,0:T(8,128)S(1)}, f32[256,256]{1,0:T(8,128)}, u32[]{:S(2)}) copy-start(f32[256,256]{1,0:T(8,128)} %constant.51.clone.near0_ref) | copy-start | bytes 786436
  15.1 22.2 %copy-start.9 = (f32[128,256]{1,0:T(8,128)S(1)}, f32[128,256]{1,0:T(8,128)}, u32[]{:S(2)}) copy-start(f32[128,256]{1,0:T(8,128)} %constant.52.clone.near1_ref) | copy-start | bytes 393220
  15.1 9.3 %collective-permute-start.5 = (bf16[2,2,256,128]{3,2,1,0:T(8,128)(2,1)S(1)}, bf16[2,2,256,128]{3,2,1,0:T(8,128)(2,1)S(1)}, u32[]{:S(2)}, u32[]{:S(2)}) collective-permute-start(bf16[2,2,256,128]{3,2,1,0:T(8,128)(2,1)S(1)} %get-tuple-element.42.kvb_ref), channel_id=1, source_target_pairs={{0,4},{2,6},{4,8},{6,10},{8,12},{10,14},{1,5},{3,7},{5,9},{7,11},{... | collective-permute-start | bytes 786440 | tf_op jit(solution)/shard_map/ppermute | solution.py:482
  20.3 9.2 %collective-permute-start.3 = (bf16[2,2,256,128]{3,2,1,0:T(8,128)(2,1)S(1)}, bf16[2,2,256,128]{3,2,1,0:T(8,128)(2,1)S(1)}, u32[]{:S(2)}, u32[]{:S(2)}) collective-permute-start(bf16[2,2,256,128]{3,2,1,0:T(8,128)(2,1)S(1)} %shard_map.112), channel_id=1, source_target_pairs={{0,2},{2,0},{4,6},{6,4},{8,10},{10,8},{12,14},{14,12},{1,3},{3,1},... | collective-permute-start | bytes 786440 | tf_op jit(solution)/shard_map/ppermute | solution.py:477
  20.8 13.0 %collective-permute-start.2 = (bf16[2,2,256,128]{3,2,1,0:T(8,128)(2,1)S(1)}, bf16[2,2,256,128]{3,2,1,0:T(8,128)(2,1)S(1)}, u32[]{:S(2)}, u32[]{:S(2)}) collective-permute-start(bf16[2,2,256,128]{3,2,1,0:T(8,128)(2,1)S(1)} %get-tuple-element.43), channel_id=1, source_target_pairs={{0,2},{2,0},{4,6},{6,4},{8,10},{10,8},{12,14},{14,12},{1,3},{3,1},... | collective-permute-start | bytes 786440 | tf_op jit(solution)/shard_map/ppermute | solution.py:477
  22.4 18.0 %collective-permute-start.14 = (bf16[2,512,128]{2,1,0:T(8,128)(2,1)S(1)}, bf16[2,512,128]{2,1,0:T(8,128)(2,1)S(1)}, u32[]{:S(2)}, u32[]{:S(2)}) collective-permute-start(bf16[2,512,128]{2,1,0:T(8,128)(2,1)S(1)} %pad_maximum_fusion.2), channel_id=1, source_target_pairs={{4,0},{6,2},{8,4},{10,6},{12,8},{14,10},{5,1},{7,3},{9,5},{11,7},{... | collective-permute-start | bytes 786440 | tf_op jit(solution)/shard_map/ppermute | solution.py:529
  24.5 39.8 %collective-permute-start.8 = (bf16[2,2,256,128]{3,2,1,0:T(8,128)(2,1)S(1)}, bf16[2,2,256,128]{3,2,1,0:T(8,128)(2,1)S(1)}, u32[]{:S(2)}, u32[]{:S(2)}) collective-permute-start(bf16[2,2,256,128]{3,2,1,0:T(8,128)(2,1)S(1)} %pad_maximum_fusion), channel_id=1, source_target_pairs={{0,4},{2,6},{4,8},{6,10},{8,12},{10,14},{1,5},{3,7},{5,9},{7,11},{... | collective-permute-start | bytes 786440 | tf_op jit(solution)/shard_map/ppermute | solution.py:482
  29.5 11.6 %collective-permute-start.7 = (bf16[2,2,256,128]{3,2,1,0:T(8,128)(2,1)S(1)}, bf16[2,2,256,128]{3,2,1,0:T(8,128)(2,1)S(1)}, u32[]{:S(2)}, u32[]{:S(2)}) collective-permute-start(bf16[2,2,256,128]{3,2,1,0:T(8,128)(2,1)S(1)} %collective-permute-done.3.kvyb_ref), channel_id=1, source_target_pairs={{0,4},{2,6},{4,8},{6,10},{8,12},{10,14},{1,5},{3,7},{5,9},{7,11},{... | collective-permute-start | bytes 786440 | tf_op jit(solution)/shard_map/ppermute | solution.py:482
  33.8 11.1 %collective-permute-start.6 = (bf16[2,2,256,128]{3,2,1,0:T(8,128)(2,1)S(1)}, bf16[2,2,256,128]{3,2,1,0:T(8,128)(2,1)S(1)}, u32[]{:S(2)}, u32[]{:S(2)}) collective-permute-start(bf16[2,2,256,128]{3,2,1,0:T(8,128)(2,1)S(1)} %collective-permute-done.2.kvya_ref), channel_id=1, source_target_pairs={{0,4},{2,6},{4,8},{6,10},{8,12},{10,14},{1,5},{3,7},{5,9},{7,11},{... | collective-permute-start | bytes 786440 | tf_op jit(solution)/shard_map/ppermute | solution.py:482
  37.3 7.6 %copy-start.6 = (f32[128,128]{1,0:T(8,128)S(1)}, f32[128,128]{1,0:T(8,128)}, u32[]{:S(2)}) copy-start(f32[128,128]{1,0:T(8,128)} %constant.49.clone.pair_ref) | copy-start | bytes 196612
  40.4 16.1 %copy-start.4 = (f32[256,256]{1,0:T(8,128)S(1)}, f32[256,256]{1,0:T(8,128)}, u32[]{:S(2)}) copy-start(f32[256,256]{1,0:T(8,128)} %constant.53.clone.group_ref) | copy-start | bytes 786436
  40.4 16.1 %copy-start.5 = (f32[256,256]{1,0:T(8,128)S(1)}, f32[256,256]{1,0:T(8,128)}, u32[]{:S(2)}) copy-start(f32[256,256]{1,0:T(8,128)} %constant.54.clone.near_ref) | copy-start | bytes 786436
  46.2 12.9 %collective-permute-start.15 = (bf16[560,128]{1,0:T(8,128)(2,1)S(1)}, bf16[560,128]{1,0:T(8,128)(2,1)S(1)}, u32[]{:S(2)}, u32[]{:S(2)}) collective-permute-start(bf16[560,128]{1,0:T(8,128)(2,1)S(1)} %get-tuple-element.55), channel_id=1, source_target_pairs={{0,4},{2,6},{4,8},{6,10},{8,12},{10,14},{1,5},{3,7},{5,9},{7,11},{... | collective-permute-start | bytes 430088 | tf_op jit(solution)/shard_map/ppermute | solution.py:482
  50.6 8.5 %collective-permute-start.16 = (bf16[560,128]{1,0:T(8,128)(2,1)S(1)}, bf16[560,128]{1,0:T(8,128)(2,1)S(1)}, u32[]{:S(2)}, u32[]{:S(2)}) collective-permute-start(bf16[560,128]{1,0:T(8,128)(2,1)S(1)} %get-tuple-element.56), channel_id=1, source_target_pairs={{0,6},{2,4},{4,10},{6,8},{8,14},{10,12},{1,7},{3,5},{5,11},{7,9},{... | collective-permute-start | bytes 430088 | tf_op jit(solution)/shard_map/ppermute | solution.py:541
  54.0 10.3 %collective-permute-start.9 = (bf16[2,2,256,128]{3,2,1,0:T(8,128)(2,1)S(1)}, bf16[2,2,256,128]{3,2,1,0:T(8,128)(2,1)S(1)}, u32[]{:S(2)}, u32[]{:S(2)}) collective-permute-start(bf16[2,2,256,128]{3,2,1,0:T(8,128)(2,1)S(1)} %pad_maximum_fusion.1), channel_id=1, source_target_pairs={{0,4},{2,6},{4,8},{6,10},{8,12},{10,14},{1,5},{3,7},{5,9},{7,11},{... | collective-permute-start | bytes 786440 | tf_op jit(solution)/shard_map/ppermute | solution.py:482
  57.4 5.2 %collective-permute-start.13 = (bf16[560,128]{1,0:T(8,128)(2,1)S(1)}, bf16[560,128]{1,0:T(8,128)(2,1)S(1)}, u32[]{:S(2)}, u32[]{:S(2)}) collective-permute-start(bf16[560,128]{1,0:T(8,128)(2,1)S(1)} %get-tuple-element.53), channel_id=1, source_target_pairs={{0,2},{2,0},{4,6},{6,4},{8,10},{10,8},{12,14},{14,12},{1,3},{3,1},... | collective-permute-start | bytes 430088 | tf_op jit(solution)/shard_map/ppermute | solution.py:477
  64.2 8.3 %copy-start.3 = (bf16[1024,1024]{1,0:T(8,128)(2,1)S(1)}, bf16[1024,1024]{1,0:T(8,128)(2,1)}, u32[]{:S(2)}) copy-start(bf16[1024,1024]{1,0:T(8,128)(2,1)} %w_ref.3) | copy-start | bytes 6291460
  64.2 6.9 %collective-permute-start.17 = (bf16[2,512,128]{2,1,0:T(8,128)(2,1)S(1)}, bf16[2,512,128]{2,1,0:T(8,128)(2,1)S(1)}, u32[]{:S(2)}, u32[]{:S(2)}) collective-permute-start(bf16[2,512,128]{2,1,0:T(8,128)(2,1)S(1)} %shard_map.117.own_ref), channel_id=1, source_target_pairs={{0,1},{1,0},{2,3},{3,2},{4,5},{5,4},{6,7},{7,6},{8,9},{9,8},{10,11... | collective-permute-start | bytes 786440 | tf_op jit(solution)/shard_map/ppermute | solution.py:477
  65.2 5.9 %collective-permute-start.10 = (bf16[512,128]{1,0:T(8,128)(2,1)S(1)}, bf16[512,128]{1,0:T(8,128)(2,1)S(1)}, u32[]{:S(2)}, u32[]{:S(2)}) collective-permute-start(bf16[512,128]{1,0:T(8,128)(2,1)S(1)} %get-tuple-element.52), channel_id=1, source_target_pairs={{0,2},{2,0},{4,6},{6,4},{8,10},{10,8},{12,14},{14,12},{1,3},{3,1},... | collective-permute-start | bytes 393224 | tf_op jit(solution)/shard_map/ppermute | solution.py:477
  66.8 4.3 %collective-permute-start.11 = (bf16[512,128]{1,0:T(8,128)(2,1)S(1)}, bf16[512,128]{1,0:T(8,128)(2,1)S(1)}, u32[]{:S(2)}, u32[]{:S(2)}) collective-permute-start(bf16[512,128]{1,0:T(8,128)(2,1)S(1)} %get-tuple-element.51.a_ref), channel_id=1, source_target_pairs={{0,1},{1,0},{2,3},{3,2},{4,5},{5,4},{6,7},{7,6},{8,9},{9,8},{10,11... | collective-permute-start | bytes 393224 | tf_op jit(solution)/shard_map/ppermute | solution.py:477
  71.1 1.3 %collective-permute-start.12 = (bf16[512,128]{1,0:T(8,128)(2,1)S(1)}, bf16[512,128]{1,0:T(8,128)(2,1)S(1)}, u32[]{:S(2)}, u32[]{:S(2)}) collective-permute-start(bf16[512,128]{1,0:T(8,128)(2,1)S(1)} %collective-permute-done.10.b_ref), channel_id=1, source_target_pairs={{0,1},{1,0},{2,3},{3,2},{4,5},{5,4},{6,7},{7,6},{8,9},{9,8},{10,11... | collective-permute-start | bytes 393224 | tf_op jit(solution)/shard_map/ppermute | solution.py:477

commit v5 on v4

--- a/solution.py
+++ b/solution.py
@@ -104,10 +104,10 @@
     kv_part(x_ref, (wk_ref.at[:, column], wv_ref.at[:, column]), out_ref, cos_ref.at[part], sin_ref.at[part], buf_ref)
 
 
-def q_kernel(sc_ref, xo_ref, xp_ref, cos_ref, sin_ref, w_ref, keepa_ref, keepb_ref, send_ref,
+def q_kernel(sc_ref, xo_ref, xp_ref, cos_ref, sin_ref, w_ref, keepa_ref, keepb_ref, send0_ref, send1_ref,
              back_ref, buf_ref):
     tp, par = sc_ref[0], sc_ref[1]
-    heads = send_ref.shape[0]
+    heads = keepa_ref.shape[0]
     width = heads * HEAD
     slot = 0
     for side in (1, 0):
@@ -117,7 +117,7 @@
             for h in range(heads):
                 val = rotated(acc[:, h * HEAD:(h + 1) * HEAD], cos_ref[part], sin_ref[part])
                 if side:
-                    place(send_ref, (h,), val, buf_ref, slot, tp if part == 0 else 1 - tp)
+                    place((send0_ref, send1_ref)[h], (), val, buf_ref, slot, tp if part == 0 else 1 - tp)
                 else:
                     place((keepa_ref, keepb_ref)[part], (h,), val, buf_ref, slot, None)
                 if h >= RELAYED and not side:
@@ -247,13 +247,13 @@
     return [bias_of(np.asarray(x, int)) for x in (group0, group1, near0, near1, upper, pair2)]
 
 
-def local_kernel(sc_ref, qa_ref, qb_ref, qy_ref, kva_ref, kvb_ref, kvya_ref, kvyb_ref, group_ref, near0_ref, near1_ref,
+def local_kernel(sc_ref, qa_ref, qb_ref, qy0_ref, qy1_ref, kva_ref, kvb_ref, kvya_ref, kvyb_ref, group_ref, near0_ref, near1_ref,
                  q_ref, m_ref, l_ref, o_ref, k_s, v_s, s_s):
     tp, par = sc_ref[0], sc_ref[1]
-    nq = qy_ref.shape[1] // FAR_DILATION
+    nq = qy0_ref.shape[0] // FAR_DILATION
     for h in range(q_ref.shape[0]):
         q, m, l, o, k, v, sh = (x.at[h] for x in (q_ref, m_ref, l_ref, o_ref, k_s, v_s, s_s))
-        gather(q, nq, [(qa_ref.at[h], par, tp), (qb_ref.at[h], par, 1 - tp), (qy_ref.at[h], 1 - par, None)])
+        gather(q, nq, [(qa_ref.at[h], par, tp), (qb_ref.at[h], par, 1 - tp), ((qy0_ref, qy1_ref)[h], 1 - par, None)])
         gather_kv(k, v, [x.at[h] for x in (kva_ref, kvb_ref, kvya_ref, kvyb_ref)], nq, tp, par)
         at = 0
         items = []
@@ -498,7 +498,7 @@
     group0, group1, near0, near1, upper, pair2 = biases(nq)
     shape = jax.ShapeDtypeStruct
     kv = shape((heads, 2, half, HEAD), BF16)
-    q_shape, q_half = shape((heads, rows, HEAD), BF16), shape((heads, half, HEAD), BF16)
+    q_shape, q_half = shape((rows, HEAD), BF16), shape((heads, half, HEAD), BF16)
     table = shape((2, half, HEAD), F32)
     buffers = pltpu.VMEM((4 * heads, half, HEAD), F32)
 
@@ -520,11 +520,12 @@
                    flops)
     kv_yb = swap(send_b, "sp")
     back = shape((heads - RELAYED, 2, half, HEAD), BF16)
-    q_a, q_b, q_send, back_own = call(
-        q_kernel, scalars, [own, partner, cosine, sine, query_weight], [q_half, q_half, q_shape, back],
+    q_a, q_b, q_send0, q_send1, back_own = call(
+        q_kernel, scalars, [own, partner, cosine, sine, query_weight], [q_half, q_half, q_shape, q_shape, back],
         [buffers], 2 * flops)
-    q_y = swap(q_send, "sp")
-    behind = jnp.stack([back_own.reshape(rows, HEAD), q_y[RELAYED]])
+    q_y1 = swap(q_send1, "sp")
+    q_y0 = swap(q_send0, "sp")
+    behind = jnp.stack([back_own.reshape(rows, HEAD), q_y1])
     n = lax.axis_size("sp")
     q_next = lax.ppermute(behind, "sp", [(i, i - 2) for i in range(2, n)])
     kv1_ya = onward(kv_ya)
@@ -543,7 +544,7 @@
     state = shape((heads, group, HEAD), F32)
     kv_scratch = [pltpu.VMEM((heads, group, HEAD), BF16)] * 2
     q, m, l, o = call(
-        local_kernel, scalars, [q_a, q_b, q_y, kv_a, kv_b, kv_ya, kv_yb, group0, near0, upper],
+        local_kernel, scalars, [q_a, q_b, q_y0, q_y1, kv_a, kv_b, kv_ya, kv_yb, group0, near0, upper],
         [shape((heads, group, HEAD), BF16), state, state, state],
         kv_scratch + [pltpu.VMEM((heads, 3 * group, 2 * HEAD), F32)], 3 * 10 ** 9)
     m, l, o, state_y = call(

time: 75.6 us -> 76.6 us (1.013)
  starting transfers between devices: 38.7 us -> 41 us
  waiting for transfers between devices: 15.7 us -> 13.6 us
    ppermute x7, starting transfers between devices: 26.3 us -> 29 us  [onward(): return lax.ppermute(x, 'sp', [(i, i + 2) for i in range(n - 2)])]
    ppermute x9 -> x10, waiting for transfers between devices: 10.5 us -> 7.95 us  [swap(): lax.ppermute(x, axis, [(i, i ^ 1) for i in range(lax.axis_size(axis))])]
    ppermute x1, waiting for transfers between devices: 0.01 us -> 2.33 us  [body(): lax.ppermute(piece_diag, 'sp', [(i, (i ^ 1) + 2) for i in range(n - 2)])]
    ppermute x7, waiting for transfers between devices: 5.17 us -> 3.35 us  [onward(): return lax.ppermute(x, 'sp', [(i, i + 2) for i in range(n - 2)])]
    ppermute x1, starting transfers between devices: 3.38 us -> 2.5 us  [body(): lax.ppermute(piece_diag, 'sp', [(i, (i ^ 1) + 2) for i in range(n - 2)])]
    ppermute x9 -> x10, starting transfers between devices: 7.67 us -> 8.18 us  [swap(): lax.ppermute(x, axis, [(i, i ^ 1) for i in range(lax.axis_size(axis))])]
  transfers between devices with their start and end apart: 18 -> 19, of which waited for: 8 -> 7; matrix products, arithmetic and copies ran while one was open for 0% -> 0% of each run, Pallas kernels for 23% -> 23%
where the time goes in v5:
time: 76.6 us; the launch traced here: 75.6 us
  starting transfers between devices  41 us (54%)
  Pallas kernels  20.3 us (27%)
  waiting for transfers between devices  13.6 us (18%)
    ppermute x7, starting transfers between devices, onward(): return lax.ppermute(x, 'sp', [(i, i + 2) for i in range(n - 2)])  29 us
    pallas_call x9, Pallas kernels, call(): pl.pallas_call(kernel, in_specs=[pl.BlockSpec(memory_space=pltpu.SMEM)] +...  17.5 us
    ppermute x10, starting transfers between devices, swap(): lax.ppermute(x, axis, [(i, i ^ 1) for i in range(lax.axis_size(axis))])  8.18 us
    ppermute x10, waiting for transfers between devices, swap(): lax.ppermute(x, axis, [(i, i ^ 1) for i in range(lax.axis_size(axis))])  7.95 us
    ppermute x7, waiting for transfers between devices, onward(): return lax.ppermute(x, 'sp', [(i, i + 2) for i in range(n - 2)])  3.35 us
    pallas_call x1, Pallas kernels, out_project(): pl.pallas_call(out_kernel, grid=(steps,), in_specs=[pl.BlockSpec(memory_s...  2.79 us
    ppermute x1, starting transfers between devices, body(): lax.ppermute(piece_diag, 'sp', [(i, (i ^ 1) + 2) for i in range(n - 2)])  2.5 us
    ppermute x1, waiting for transfers between devices, body(): lax.ppermute(piece_diag, 'sp', [(i, (i ^ 1) + 2) for i in range(n - 2)])  2.33 us
  transfers between devices with their start and end apart: 19, of which 7 were waited for; matrix products, arithmetic and copies ran while one was open for 0% of the time, Pallas kernels for 23%

profile of v5, /device:TPU:0, one launch (start us, length us, event | category | flops | bytes accessed | tf_op | source)
XLA Modules:
  0.0 75.6 jit_solution(2250681120741961651)
XLA Ops:
  0.0 0.5 collective-permute-start
  0.5 0.1 maximum_bitcast_fusion.inv_ref
  0.6 0.1 pad_add_fusion.sc_ref
  0.7 3.7 %shard_map.109 = (bf16[2,2,256,128]{3,2,1,0:T(8,128)(2,1)S(1)}, bf16[256,2048]{1,0:T(8,128)(2,1)S(1)}, bf16[2,2048,256]{2,1,0:T(8,128)(2,1)S(1)}, f32[2,256,128]{2,1,0:T(8,128)S(1)}, f32[2,256,128]{2,1,0:T(8,128)S(1)}) custom-call(s32[4]{0:T(128)S(1)} %pad_add_fusion.sc_ref, bf16[256,2048]{1,0:T(8,128)(2,1)} %x_hbm.1, bf16[2048,512]{1,0:T(8,128)(2,1)} %wk_ref.1, ...), custom_call_target="tpu_custom_call" | custom-call | flops 536870912 | tf_op jit(solution)/shard_map/pallas_call | solution.py:130
  4.4 4.5 %collective-permute-start.5 = (bf16[2,2,256,128]{3,2,1,0:T(8,128)(2,1)S(1)}, bf16[2,2,256,128]{3,2,1,0:T(8,128)(2,1)S(1)}, u32[]{:S(2)}, u32[]{:S(2)}) collective-permute-start(bf16[2,2,256,128]{3,2,1,0:T(8,128)(2,1)S(1)} %get-tuple-element.40.kva_ref), channel_id=1, source_target_pairs={{0,4},{2,6},{4,8},{6,10},{8,12},{10,14},{1,5},{3,7},{5,9},{7,11},{... | collective-permute-start | bytes 786440 | tf_op jit(solution)/shard_map/ppermute | solution.py:482
  8.9 0.0 collective-permute-done.xp_ref.x_ref
  8.9 0.0 copy-done
  8.9 0.0 copy-done.1
  8.9 0.0 copy-start.2
  8.9 2.3 %shard_map.111 = (bf16[2,2,256,128]{3,2,1,0:T(8,128)(2,1)S(1)}, bf16[2,2,256,128]{3,2,1,0:T(8,128)(2,1)S(1)}) custom-call(s32[4]{0:T(128)S(1)} %pad_add_fusion.sc_ref, bf16[256,2048]{1,0:T(8,128)(2,1)S(1)} %get-tuple-element.33.xo_ref, bf16[256,2048]{1,0:T(8,128)(2,1)S(1)} %collective-permute-done.xp_ref.x_ref, bf16[2048,512]{1,0:T(8,128)(2,1)S(1)} %copy-done, ...), custom_call_target="tpu_custom_call" | custom-call | flops 1073741824 | tf_op jit(solution)/shard_map/pallas_call | solution.py:130
  11.2 3.5 %collective-permute-start.6 = (bf16[2,2,256,128]{3,2,1,0:T(8,128)(2,1)S(1)}, bf16[2,2,256,128]{3,2,1,0:T(8,128)(2,1)S(1)}, u32[]{:S(2)}, u32[]{:S(2)}) collective-permute-start(bf16[2,2,256,128]{3,2,1,0:T(8,128)(2,1)S(1)} %get-tuple-element.44.kvb_ref), channel_id=1, source_target_pairs={{0,4},{2,6},{4,8},{6,10},{8,12},{10,14},{1,5},{3,7},{5,9},{7,11},{... | collective-permute-start | bytes 786440 | tf_op jit(solution)/shard_map/ppermute | solution.py:482
  14.7 0.0 copy-done.2
  14.7 2.5 %shard_map.110 = (bf16[2,256,128]{2,1,0:T(8,128)(2,1)S(1)}, bf16[2,256,128]{2,1,0:T(8,128)(2,1)S(1)}, bf16[512,128]{1,0:T(8,128)(2,1)S(1)}, bf16[512,128]{1,0:T(8,128)(2,1)S(1)}, bf16[1,2,256,128]{3,2,1,0:T(8,128)(2,1)S(1)}) custom-call(s32[4]{0:T(128)S(1)} %pad_add_fusion.sc_ref, bf16[256,2048]{1,0:T(8,128)(2,1)S(1)} %get-tuple-element.33.xo_ref, ...), custom_call_target="tpu_custom_call" | custom-call | flops 1073741824 | tf_op jit(solution)/shard_map/pallas_call | solution.py:130
  17.3 1.6 %collective-permute-start.2 = (bf16[512,128]{1,0:T(8,128)(2,1)S(1)}, bf16[512,128]{1,0:T(8,128)(2,1)S(1)}, u32[]{:S(2)}, u32[]{:S(2)}) collective-permute-start(bf16[512,128]{1,0:T(8,128)(2,1)S(1)} %get-tuple-element.39), channel_id=1, source_target_pairs={{0,2},{2,0},{4,6},{6,4},{8,10},{10,8},{12,14},{14,12},{1,3},{3,1},... | collective-permute-start | bytes 393224 | tf_op jit(solution)/shard_map/ppermute | solution.py:477
  18.9 0.5 collective-permute-start.3
  19.4 1.5 %shard_map.112 = bf16[2,2,256,128]{3,2,1,0:T(8,128)(2,1)S(1)} custom-call(s32[4]{0:T(128)S(1)} %pad_add_fusion.sc_ref, bf16[256,2048]{1,0:T(8,128)(2,1)S(1)} %collective-permute-done.xp_ref.x_ref, bf16[2048,512]{1,0:T(8,128)(2,1)S(1)} %copy-done, bf16[2048,512]{1,0:T(8,128)(2,1)S(1)} %copy-done.1, f32[2,256,128]{2,1,0:T(8,128)S(1)} %get-tuple-element.34.cos_ref, ...), custom_call_target="tpu_custom_call" | custom-call | flops 536870912 | tf_op jit(solution)/shard_map/pallas_call | solution.py:130
  20.9 1.6 %collective-permute-start.4 = (bf16[2,2,256,128]{3,2,1,0:T(8,128)(2,1)S(1)}, bf16[2,2,256,128]{3,2,1,0:T(8,128)(2,1)S(1)}, u32[]{:S(2)}, u32[]{:S(2)}) collective-permute-start(bf16[2,2,256,128]{3,2,1,0:T(8,128)(2,1)S(1)} %shard_map.112), channel_id=1, source_target_pairs={{0,2},{2,0},{4,6},{6,4},{8,10},{10,8},{12,14},{14,12},{1,3},{3,1},... | collective-permute-start | bytes 786440 | tf_op jit(solution)/shard_map/ppermute | solution.py:477
  22.5 0.0 collective-permute-done.5.kva_ref
  22.5 0.6 collective-permute-start.1
  23.0 0.7 collective-permute-done.2.qy1_ref
  23.7 1.3 %collective-permute-start.15 = (bf16[2,512,128]{2,1,0:T(8,128)(2,1)S(1)}, bf16[2,512,128]{2,1,0:T(8,128)(2,1)S(1)}, u32[]{:S(2)}, u32[]{:S(2)}) collective-permute-start(bf16[2,512,128]{2,1,0:T(8,128)(2,1)S(1)} %pad_maximum_fusion.2), channel_id=1, source_target_pairs={{4,0},{6,2},{8,4},{10,6},{12,8},{14,10},{5,1},{7,3},{9,5},{11,7},{... | collective-permute-start | bytes 786440 | tf_op jit(solution)/shard_map/ppermute | solution.py:530
  25.0 0.0 collective-permute-done.6.kvb_ref
  25.1 4.6 %collective-permute-start.9 = (bf16[2,2,256,128]{3,2,1,0:T(8,128)(2,1)S(1)}, bf16[2,2,256,128]{3,2,1,0:T(8,128)(2,1)S(1)}, u32[]{:S(2)}, u32[]{:S(2)}) collective-permute-start(bf16[2,2,256,128]{3,2,1,0:T(8,128)(2,1)S(1)} %pad_maximum_fusion), channel_id=1, source_target_pairs={{0,4},{2,6},{4,8},{6,10},{8,12},{10,14},{1,5},{3,7},{5,9},{7,11},{... | collective-permute-start | bytes 786440 | tf_op jit(solution)/shard_map/ppermute | solution.py:482
  29.7 0.0 collective-permute-done.3.kvya_ref
  29.7 3.5 %collective-permute-start.7 = (bf16[2,2,256,128]{3,2,1,0:T(8,128)(2,1)S(1)}, bf16[2,2,256,128]{3,2,1,0:T(8,128)(2,1)S(1)}, u32[]{:S(2)}, u32[]{:S(2)}) collective-permute-start(bf16[2,2,256,128]{3,2,1,0:T(8,128)(2,1)S(1)} %collective-permute-done.3.kvya_ref), channel_id=1, source_target_pairs={{0,4},{2,6},{4,8},{6,10},{8,12},{10,14},{1,5},{3,7},{5,9},{7,11},{... | collective-permute-start | bytes 786440 | tf_op jit(solution)/shard_map/ppermute | solution.py:482
  33.2 1.8 %collective-permute-done.4.kvyb_ref = bf16[2,2,256,128]{3,2,1,0:T(8,128)(2,1)S(1)} collective-permute-done((bf16[2,2,256,128]{3,2,1,0:T(8,128)(2,1)S(1)}, bf16[2,2,256,128]{3,2,1,0:T(8,128)(2,1)S(1)}, u32[]{:S(2)}, u32[]{:S(2)}) %collective-permute-start.4) | collective-permute-done | bytes 262176 | tf_op jit(solution)/shard_map/ppermute | solution.py:477
  34.9 3.5 %collective-permute-start.8 = (bf16[2,2,256,128]{3,2,1,0:T(8,128)(2,1)S(1)}, bf16[2,2,256,128]{3,2,1,0:T(8,128)(2,1)S(1)}, u32[]{:S(2)}, u32[]{:S(2)}) collective-permute-start(bf16[2,2,256,128]{3,2,1,0:T(8,128)(2,1)S(1)} %collective-permute-done.4.kvyb_ref), channel_id=1, source_target_pairs={{0,4},{2,6},{4,8},{6,10},{8,12},{10,14},{1,5},{3,7},{5,9},{7,11},{... | collective-permute-start | bytes 786440 | tf_op jit(solution)/shard_map/ppermute | solution.py:482
  38.4 0.0 collective-permute-done.1.qy0_ref
  38.4 0.0 copy-done.7
  38.4 0.0 copy-done.8
  38.4 0.0 copy-done.9
  38.5 0.0 copy-start.4
  38.5 0.0 copy-start.5
  38.5 3.0 %shard_map.113 = (bf16[2,1024,128]{2,1,0:T(8,128)(2,1)S(1)}, f32[2,1024,128]{2,1,0:T(8,128)S(1)}, f32[2,1024,128]{2,1,0:T(8,128)S(1)}, f32[2,1024,128]{2,1,0:T(8,128)S(1)}) custom-call(s32[4]{0:T(128)S(1)} %pad_add_fusion.sc_ref, bf16[2,256,128]{2,1,0:T(8,128)(2,1)S(1)} %get-tuple-element.36.qa_ref, bf16[2,256,128]{2,1,0:T(8,128)(2,1)S(1)} %get-tuple-element.37.qb_ref, ...), custom_call_target="tpu_custom_call" | custom-call | flops 3000000000 | tf_op jit(solution)/shard_map/pallas_call | solution.py:130
  41.5 3.2 %collective-permute-done.8.kvyb_ref = bf16[2,2,256,128]{3,2,1,0:T(8,128)(2,1)S(1)} collective-permute-done((bf16[2,2,256,128]{3,2,1,0:T(8,128)(2,1)S(1)}, bf16[2,2,256,128]{3,2,1,0:T(8,128)(2,1)S(1)}, u32[]{:S(2)}, u32[]{:S(2)}) %collective-permute-start.8) | collective-permute-done | bytes 262176 | tf_op jit(solution)/shard_map/ppermute | solution.py:482
  44.8 0.0 collective-permute-done.7.kvya_ref
  44.8 4.4 %collective-permute-start.10 = (bf16[2,2,256,128]{3,2,1,0:T(8,128)(2,1)S(1)}, bf16[2,2,256,128]{3,2,1,0:T(8,128)(2,1)S(1)}, u32[]{:S(2)}, u32[]{:S(2)}) collective-permute-start(bf16[2,2,256,128]{3,2,1,0:T(8,128)(2,1)S(1)} %pad_maximum_fusion.1), channel_id=1, source_target_pairs={{0,4},{2,6},{4,8},{6,10},{8,12},{10,14},{1,5},{3,7},{5,9},{7,11},{... | collective-permute-start | bytes 786440 | tf_op jit(solution)/shard_map/ppermute | solution.py:482
  49.2 0.0 copy-done.4
  49.3 0.0 copy-done.5
  49.3 0.0 copy-start.6
  49.3 0.7 shard_map.114
  50.0 1.6 %collective-permute-start.14 = (bf16[560,128]{1,0:T(8,128)(2,1)S(1)}, bf16[560,128]{1,0:T(8,128)(2,1)S(1)}, u32[]{:S(2)}, u32[]{:S(2)}) collective-permute-start(bf16[560,128]{1,0:T(8,128)(2,1)S(1)} %get-tuple-element.55), channel_id=1, source_target_pairs={{0,2},{2,0},{4,6},{6,4},{8,10},{10,8},{12,14},{14,12},{1,3},{3,1},... | collective-permute-start | bytes 430088 | tf_op jit(solution)/shard_map/ppermute | solution.py:477
  51.6 0.0 collective-permute-done.15.qn_ref
  51.6 1.2 %shard_map.116 = (bf16[560,128]{1,0:T(8,128)(2,1)S(1)}, bf16[560,128]{1,0:T(8,128)(2,1)S(1)}) custom-call(s32[4]{0:T(128)S(1)} %pad_add_fusion.sc_ref, bf16[2,512,128]{2,1,0:T(8,128)(2,1)S(1)} %collective-permute-done.15.qn_ref, bf16[2,2,256,128]{3,2,1,0:T(8,128)(2,1)S(1)} %collective-permute-done.5.kva_ref, ...), custom_call_target="tpu_custom_call" | custom-call | flops 1000000000 | tf_op jit(solution)/shard_map/pallas_call | solution.py:130
  52.8 5.2 %collective-permute-start.16 = (bf16[560,128]{1,0:T(8,128)(2,1)S(1)}, bf16[560,128]{1,0:T(8,128)(2,1)S(1)}, u32[]{:S(2)}, u32[]{:S(2)}) collective-permute-start(bf16[560,128]{1,0:T(8,128)(2,1)S(1)} %get-tuple-element.57), channel_id=1, source_target_pairs={{0,4},{2,6},{4,8},{6,10},{8,12},{10,14},{1,5},{3,7},{5,9},{7,11},{... | collective-permute-start | bytes 430088 | tf_op jit(solution)/shard_map/ppermute | solution.py:482
  58.0 2.5 %collective-permute-start.17 = (bf16[560,128]{1,0:T(8,128)(2,1)S(1)}, bf16[560,128]{1,0:T(8,128)(2,1)S(1)}, u32[]{:S(2)}, u32[]{:S(2)}) collective-permute-start(bf16[560,128]{1,0:T(8,128)(2,1)S(1)} %get-tuple-element.58), channel_id=1, source_target_pairs={{0,6},{2,4},{4,10},{6,8},{8,14},{10,12},{1,7},{3,5},{5,11},{7,9},{... | collective-permute-start | bytes 430088 | tf_op jit(solution)/shard_map/ppermute | solution.py:542
  60.5 0.0 collective-permute-done.14.state_ref
  60.5 0.1 collective-permute-done.16.own_ref
  60.6 2.3 %collective-permute-done.17.diag_ref = bf16[560,128]{1,0:T(8,128)(2,1)S(1)} collective-permute-done((bf16[560,128]{1,0:T(8,128)(2,1)S(1)}, bf16[560,128]{1,0:T(8,128)(2,1)S(1)}, u32[]{:S(2)}, u32[]{:S(2)}) %collective-permute-start.17) | collective-permute-done | bytes 143392 | tf_op jit(solution)/shard_map/ppermute | solution.py:542
  63.0 1.6 %shard_map.117.own_ref = bf16[2,512,128]{2,1,0:T(8,128)(2,1)S(1)} custom-call(s32[4]{0:T(128)S(1)} %pad_add_fusion.sc_ref, f32[2,1024,128]{2,1,0:T(8,128)S(1)} %get-tuple-element.50.m_ref, f32[2,1024,128]{2,1,0:T(8,128)S(1)} %get-tuple-element.51.l_ref, f32[2,1024,128]{2,1,0:T(8,128)S(1)} %get-tuple-element.52.o_ref, ...), custom_call_target="tpu_custom_call" | custom-call | flops 1000000000 | tf_op jit(solution)/shard_map/pallas_call | solution.py:130
  64.5 0.0 copy-start.3
  64.6 0.1 collective-permute-start.18
  64.6 0.0 collective-permute-done.9.kvo_ref
  64.6 0.0 collective-permute-done.10.kvy_ref
  64.7 0.9 %shard_map.115 = (bf16[512,128]{1,0:T(8,128)(2,1)S(1)}, bf16[512,128]{1,0:T(8,128)(2,1)S(1)}) custom-call(s32[4]{0:T(128)S(1)} %pad_add_fusion.sc_ref, bf16[2,1024,128]{2,1,0:T(8,128)(2,1)S(1)} %get-tuple-element.46.q_ref, f32[2,1024,128]{2,1,0:T(8,128)S(1)} %get-tuple-element.50.m_ref, f32[2,1024,128]{2,1,0:T(8,128)S(1)} %get-tuple-element.51.l_ref, ...), custom_call_target="tpu_custom_call" | custom-call | flops 1000000000 | tf_op jit(solution)/shard_map/pallas_call | solution.py:130
  65.5 1.6 %collective-permute-start.11 = (bf16[512,128]{1,0:T(8,128)(2,1)S(1)}, bf16[512,128]{1,0:T(8,128)(2,1)S(1)}, u32[]{:S(2)}, u32[]{:S(2)}) collective-permute-start(bf16[512,128]{1,0:T(8,128)(2,1)S(1)} %get-tuple-element.54), channel_id=1, source_target_pairs={{0,2},{2,0},{4,6},{6,4},{8,10},{10,8},{12,14},{14,12},{1,3},{3,1},... | collective-permute-start | bytes 393224 | tf_op jit(solution)/shard_map/ppermute | solution.py:477
  67.1 0.2 collective-permute-start.12
  67.3 4.2 %collective-permute-done.11.b_ref = bf16[512,128]{1,0:T(8,128)(2,1)S(1)} collective-permute-done((bf16[512,128]{1,0:T(8,128)(2,1)S(1)}, bf16[512,128]{1,0:T(8,128)(2,1)S(1)}, u32[]{:S(2)}, u32[]{:S(2)}) %collective-permute-start.11) | collective-permute-done | bytes 131104 | tf_op jit(solution)/shard_map/ppermute | solution.py:477
  71.5 0.0 collective-permute-start.13
  71.5 0.0 collective-permute-done.12.c_ref
  71.5 0.0 collective-permute-done.18.tp_ref
  71.5 1.3 %collective-permute-done.13.d_ref = bf16[512,128]{1,0:T(8,128)(2,1)S(1)} collective-permute-done((bf16[512,128]{1,0:T(8,128)(2,1)S(1)}, bf16[512,128]{1,0:T(8,128)(2,1)S(1)}, u32[]{:S(2)}, u32[]{:S(2)}) %collective-permute-start.13) | collective-permute-done | bytes 131104 | tf_op jit(solution)/shard_map/ppermute | solution.py:477
  72.8 0.0 copy-done.3
  72.8 2.8 %out_project.1 = bf16[512,1024]{1,0:T(8,128)(2,1)} custom-call(s32[4]{0:T(128)S(1)} %pad_add_fusion.sc_ref, bf16[512,128]{1,0:T(8,128)(2,1)S(1)} %get-tuple-element.53.a_ref, bf16[512,128]{1,0:T(8,128)(2,1)S(1)} %collective-permute-done.11.b_ref, bf16[512,128]{1,0:T(8,128)(2,1)S(1)} %collective-permute-done.12.c_ref, ...), custom_call_target="tpu_custom_call" | custom-call | flops 1073741824 | tf_op jit(solution)/shard_map/out_project/pallas_call | solution.py:464
  (14 shorter events, 0.1 us)
Async XLA Ops:
  0.0 8.9 %collective-permute-start = (bf16[256,2048]{1,0:T(8,128)(2,1)}, bf16[256,2048]{1,0:T(8,128)(2,1)S(1)}, u32[]{:S(2)}, u32[]{:S(2)}) collective-permute-start(bf16[256,2048]{1,0:T(8,128)(2,1)} %x_hbm.1), channel_id=1, source_target_pairs={{0,1},{1,0},{2,3},{3,2},{4,5},{5,4},{6,7},{7,6},{8,9},{9,8},{10,11... | collective-permute-start | bytes 3145736 | tf_op jit(solution)/shard_map/ppermute | solution.py:477
  0.7 8.3 %copy-start = (bf16[2048,512]{1,0:T(8,128)(2,1)S(1)}, bf16[2048,512]{1,0:T(8,128)(2,1)}, u32[]{:S(2)}) copy-start(bf16[2048,512]{1,0:T(8,128)(2,1)} %wk_ref.1) | copy-start | bytes 6291460
  0.7 8.3 %copy-start.1 = (bf16[2048,512]{1,0:T(8,128)(2,1)S(1)}, bf16[2048,512]{1,0:T(8,128)(2,1)}, u32[]{:S(2)}) copy-start(bf16[2048,512]{1,0:T(8,128)(2,1)} %wv_ref.1) | copy-start | bytes 6291460
  4.4 18.1 %collective-permute-start.5 = (bf16[2,2,256,128]{3,2,1,0:T(8,128)(2,1)S(1)}, bf16[2,2,256,128]{3,2,1,0:T(8,128)(2,1)S(1)}, u32[]{:S(2)}, u32[]{:S(2)}) collective-permute-start(bf16[2,2,256,128]{3,2,1,0:T(8,128)(2,1)S(1)} %get-tuple-element.40.kva_ref), channel_id=1, source_target_pairs={{0,4},{2,6},{4,8},{6,10},{8,12},{10,14},{1,5},{3,7},{5,9},{7,11},{... | collective-permute-start | bytes 786440 | tf_op jit(solution)/shard_map/ppermute | solution.py:482
  8.9 5.8 %copy-start.2 = (bf16[2048,512]{1,0:T(8,128)(2,1)S(1)}, bf16[2048,512]{1,0:T(8,128)(2,1)}, u32[]{:S(2)}) copy-start(bf16[2048,512]{1,0:T(8,128)(2,1)} %w_ref.2) | copy-start | bytes 6291460
  11.2 13.8 %collective-permute-start.6 = (bf16[2,2,256,128]{3,2,1,0:T(8,128)(2,1)S(1)}, bf16[2,2,256,128]{3,2,1,0:T(8,128)(2,1)S(1)}, u32[]{:S(2)}, u32[]{:S(2)}) collective-permute-start(bf16[2,2,256,128]{3,2,1,0:T(8,128)(2,1)S(1)} %get-tuple-element.44.kvb_ref), channel_id=1, source_target_pairs={{0,4},{2,6},{4,8},{6,10},{8,12},{10,14},{1,5},{3,7},{5,9},{7,11},{... | collective-permute-start | bytes 786440 | tf_op jit(solution)/shard_map/ppermute | solution.py:482
  17.3 6.4 %collective-permute-start.2 = (bf16[512,128]{1,0:T(8,128)(2,1)S(1)}, bf16[512,128]{1,0:T(8,128)(2,1)S(1)}, u32[]{:S(2)}, u32[]{:S(2)}) collective-permute-start(bf16[512,128]{1,0:T(8,128)(2,1)S(1)} %get-tuple-element.39), channel_id=1, source_target_pairs={{0,2},{2,0},{4,6},{6,4},{8,10},{10,8},{12,14},{14,12},{1,3},{3,1},... | collective-permute-start | bytes 393224 | tf_op jit(solution)/shard_map/ppermute | solution.py:477
  18.9 19.6 %copy-start.7 = (f32[256,256]{1,0:T(8,128)S(1)}, f32[256,256]{1,0:T(8,128)}, u32[]{:S(2)}) copy-start(f32[256,256]{1,0:T(8,128)} %constant.50.clone.group_ref) | copy-start | bytes 786436
  18.9 19.6 %copy-start.8 = (f32[256,256]{1,0:T(8,128)S(1)}, f32[256,256]{1,0:T(8,128)}, u32[]{:S(2)}) copy-start(f32[256,256]{1,0:T(8,128)} %constant.51.clone.near0_ref) | copy-start | bytes 786436
  18.9 19.6 %copy-start.9 = (f32[128,256]{1,0:T(8,128)S(1)}, f32[128,256]{1,0:T(8,128)}, u32[]{:S(2)}) copy-start(f32[128,256]{1,0:T(8,128)} %constant.52.clone.near1_ref) | copy-start | bytes 393220
  18.9 10.8 %collective-permute-start.3 = (bf16[2,2,256,128]{3,2,1,0:T(8,128)(2,1)S(1)}, bf16[2,2,256,128]{3,2,1,0:T(8,128)(2,1)S(1)}, u32[]{:S(2)}, u32[]{:S(2)}) collective-permute-start(bf16[2,2,256,128]{3,2,1,0:T(8,128)(2,1)S(1)} %get-tuple-element.45), channel_id=1, source_target_pairs={{0,2},{2,0},{4,6},{6,4},{8,10},{10,8},{12,14},{14,12},{1,3},{3,1},... | collective-permute-start | bytes 786440 | tf_op jit(solution)/shard_map/ppermute | solution.py:477
  20.9 14.1 %collective-permute-start.4 = (bf16[2,2,256,128]{3,2,1,0:T(8,128)(2,1)S(1)}, bf16[2,2,256,128]{3,2,1,0:T(8,128)(2,1)S(1)}, u32[]{:S(2)}, u32[]{:S(2)}) collective-permute-start(bf16[2,2,256,128]{3,2,1,0:T(8,128)(2,1)S(1)} %shard_map.112), channel_id=1, source_target_pairs={{0,2},{2,0},{4,6},{6,4},{8,10},{10,8},{12,14},{14,12},{1,3},{3,1},... | collective-permute-start | bytes 786440 | tf_op jit(solution)/shard_map/ppermute | solution.py:477
  22.5 15.9 %collective-permute-start.1 = (bf16[512,128]{1,0:T(8,128)(2,1)S(1)}, bf16[512,128]{1,0:T(8,128)(2,1)S(1)}, u32[]{:S(2)}, u32[]{:S(2)}) collective-permute-start(bf16[512,128]{1,0:T(8,128)(2,1)S(1)} %get-tuple-element.38), channel_id=1, source_target_pairs={{0,2},{2,0},{4,6},{6,4},{8,10},{10,8},{12,14},{14,12},{1,3},{3,1},... | collective-permute-start | bytes 393224 | tf_op jit(solution)/shard_map/ppermute | solution.py:477
  23.7 27.8 %collective-permute-start.15 = (bf16[2,512,128]{2,1,0:T(8,128)(2,1)S(1)}, bf16[2,512,128]{2,1,0:T(8,128)(2,1)S(1)}, u32[]{:S(2)}, u32[]{:S(2)}) collective-permute-start(bf16[2,512,128]{2,1,0:T(8,128)(2,1)S(1)} %pad_maximum_fusion.2), channel_id=1, source_target_pairs={{4,0},{6,2},{8,4},{10,6},{12,8},{14,10},{5,1},{7,3},{9,5},{11,7},{... | collective-permute-start | bytes 786440 | tf_op jit(solution)/shard_map/ppermute | solution.py:530
  25.1 39.5 %collective-permute-start.9 = (bf16[2,2,256,128]{3,2,1,0:T(8,128)(2,1)S(1)}, bf16[2,2,256,128]{3,2,1,0:T(8,128)(2,1)S(1)}, u32[]{:S(2)}, u32[]{:S(2)}) collective-permute-start(bf16[2,2,256,128]{3,2,1,0:T(8,128)(2,1)S(1)} %pad_maximum_fusion), channel_id=1, source_target_pairs={{0,4},{2,6},{4,8},{6,10},{8,12},{10,14},{1,5},{3,7},{5,9},{7,11},{... | collective-permute-start | bytes 786440 | tf_op jit(solution)/shard_map/ppermute | solution.py:482
  29.7 15.1 %collective-permute-start.7 = (bf16[2,2,256,128]{3,2,1,0:T(8,128)(2,1)S(1)}, bf16[2,2,256,128]{3,2,1,0:T(8,128)(2,1)S(1)}, u32[]{:S(2)}, u32[]{:S(2)}) collective-permute-start(bf16[2,2,256,128]{3,2,1,0:T(8,128)(2,1)S(1)} %collective-permute-done.3.kvya_ref), channel_id=1, source_target_pairs={{0,4},{2,6},{4,8},{6,10},{8,12},{10,14},{1,5},{3,7},{5,9},{7,11},{... | collective-permute-start | bytes 786440 | tf_op jit(solution)/shard_map/ppermute | solution.py:482
  34.9 9.8 %collective-permute-start.8 = (bf16[2,2,256,128]{3,2,1,0:T(8,128)(2,1)S(1)}, bf16[2,2,256,128]{3,2,1,0:T(8,128)(2,1)S(1)}, u32[]{:S(2)}, u32[]{:S(2)}) collective-permute-start(bf16[2,2,256,128]{3,2,1,0:T(8,128)(2,1)S(1)} %collective-permute-done.4.kvyb_ref), channel_id=1, source_target_pairs={{0,4},{2,6},{4,8},{6,10},{8,12},{10,14},{1,5},{3,7},{5,9},{7,11},{... | collective-permute-start | bytes 786440 | tf_op jit(solution)/shard_map/ppermute | solution.py:482
  38.5 10.8 %copy-start.4 = (f32[256,256]{1,0:T(8,128)S(1)}, f32[256,256]{1,0:T(8,128)}, u32[]{:S(2)}) copy-start(f32[256,256]{1,0:T(8,128)} %constant.53.clone.group_ref) | copy-start | bytes 786436
  38.5 10.8 %copy-start.5 = (f32[256,256]{1,0:T(8,128)S(1)}, f32[256,256]{1,0:T(8,128)}, u32[]{:S(2)}) copy-start(f32[256,256]{1,0:T(8,128)} %constant.54.clone.near_ref) | copy-start | bytes 786436
  44.8 19.8 %collective-permute-start.10 = (bf16[2,2,256,128]{3,2,1,0:T(8,128)(2,1)S(1)}, bf16[2,2,256,128]{3,2,1,0:T(8,128)(2,1)S(1)}, u32[]{:S(2)}, u32[]{:S(2)}) collective-permute-start(bf16[2,2,256,128]{3,2,1,0:T(8,128)(2,1)S(1)} %pad_maximum_fusion.1), channel_id=1, source_target_pairs={{0,4},{2,6},{4,8},{6,10},{8,12},{10,14},{1,5},{3,7},{5,9},{7,11},{... | collective-permute-start | bytes 786440 | tf_op jit(solution)/shard_map/ppermute | solution.py:482
  49.3 2.3 %copy-start.6 = (f32[128,128]{1,0:T(8,128)S(1)}, f32[128,128]{1,0:T(8,128)}, u32[]{:S(2)}) copy-start(f32[128,128]{1,0:T(8,128)} %constant.49.clone.pair_ref) | copy-start | bytes 196612
  50.0 10.5 %collective-permute-start.14 = (bf16[560,128]{1,0:T(8,128)(2,1)S(1)}, bf16[560,128]{1,0:T(8,128)(2,1)S(1)}, u32[]{:S(2)}, u32[]{:S(2)}) collective-permute-start(bf16[560,128]{1,0:T(8,128)(2,1)S(1)} %get-tuple-element.55), channel_id=1, source_target_pairs={{0,2},{2,0},{4,6},{6,4},{8,10},{10,8},{12,14},{14,12},{1,3},{3,1},... | collective-permute-start | bytes 430088 | tf_op jit(solution)/shard_map/ppermute | solution.py:477
  52.8 7.8 %collective-permute-start.16 = (bf16[560,128]{1,0:T(8,128)(2,1)S(1)}, bf16[560,128]{1,0:T(8,128)(2,1)S(1)}, u32[]{:S(2)}, u32[]{:S(2)}) collective-permute-start(bf16[560,128]{1,0:T(8,128)(2,1)S(1)} %get-tuple-element.57), channel_id=1, source_target_pairs={{0,4},{2,6},{4,8},{6,10},{8,12},{10,14},{1,5},{3,7},{5,9},{7,11},{... | collective-permute-start | bytes 430088 | tf_op jit(solution)/shard_map/ppermute | solution.py:482
  58.0 4.9 %collective-permute-start.17 = (bf16[560,128]{1,0:T(8,128)(2,1)S(1)}, bf16[560,128]{1,0:T(8,128)(2,1)S(1)}, u32[]{:S(2)}, u32[]{:S(2)}) collective-permute-start(bf16[560,128]{1,0:T(8,128)(2,1)S(1)} %get-tuple-element.58), channel_id=1, source_target_pairs={{0,6},{2,4},{4,10},{6,8},{8,14},{10,12},{1,7},{3,5},{5,11},{7,9},{... | collective-permute-start | bytes 430088 | tf_op jit(solution)/shard_map/ppermute | solution.py:542
  64.5 8.3 %copy-start.3 = (bf16[1024,1024]{1,0:T(8,128)(2,1)S(1)}, bf16[1024,1024]{1,0:T(8,128)(2,1)}, u32[]{:S(2)}) copy-start(bf16[1024,1024]{1,0:T(8,128)(2,1)} %w_ref.3) | copy-start | bytes 6291460
  64.6 6.9 %collective-permute-start.18 = (bf16[2,512,128]{2,1,0:T(8,128)(2,1)S(1)}, bf16[2,512,128]{2,1,0:T(8,128)(2,1)S(1)}, u32[]{:S(2)}, u32[]{:S(2)}) collective-permute-start(bf16[2,512,128]{2,1,0:T(8,128)(2,1)S(1)} %shard_map.117.own_ref), channel_id=1, source_target_pairs={{0,1},{1,0},{2,3},{3,2},{4,5},{5,4},{6,7},{7,6},{8,9},{9,8},{10,11... | collective-permute-start | bytes 786440 | tf_op jit(solution)/shard_map/ppermute | solution.py:477
  65.5 5.9 %collective-permute-start.11 = (bf16[512,128]{1,0:T(8,128)(2,1)S(1)}, bf16[512,128]{1,0:T(8,128)(2,1)S(1)}, u32[]{:S(2)}, u32[]{:S(2)}) collective-permute-start(bf16[512,128]{1,0:T(8,128)(2,1)S(1)} %get-tuple-element.54), channel_id=1, source_target_pairs={{0,2},{2,0},{4,6},{6,4},{8,10},{10,8},{12,14},{14,12},{1,3},{3,1},... | collective-permute-start | bytes 393224 | tf_op jit(solution)/shard_map/ppermute | solution.py:477
  67.1 4.4 %collective-permute-start.12 = (bf16[512,128]{1,0:T(8,128)(2,1)S(1)}, bf16[512,128]{1,0:T(8,128)(2,1)S(1)}, u32[]{:S(2)}, u32[]{:S(2)}) collective-permute-start(bf16[512,128]{1,0:T(8,128)(2,1)S(1)} %get-tuple-element.53.a_ref), channel_id=1, source_target_pairs={{0,1},{1,0},{2,3},{3,2},{4,5},{5,4},{6,7},{7,6},{8,9},{9,8},{10,11... | collective-permute-start | bytes 393224 | tf_op jit(solution)/shard_map/ppermute | solution.py:477
  71.5 1.3 %collective-permute-start.13 = (bf16[512,128]{1,0:T(8,128)(2,1)S(1)}, bf16[512,128]{1,0:T(8,128)(2,1)S(1)}, u32[]{:S(2)}, u32[]{:S(2)}) collective-permute-start(bf16[512,128]{1,0:T(8,128)(2,1)S(1)} %collective-permute-done.11.b_ref), channel_id=1, source_target_pairs={{0,1},{1,0},{2,3},{3,2},{4,5},{5,4},{6,7},{7,6},{8,9},{9,8},{10,11... | collective-permute-start | bytes 393224 | tf_op jit(solution)/shard_map/ppermute | solution.py:477

commit v6 on v5

--- a/solution.py
+++ b/solution.py
@@ -282,43 +282,45 @@
 
 
 def one_kernel(sc_ref, q_ref, m_in, l_in, o_in, kva_ref, kvb_ref, kvya_ref, kvyb_ref, group_ref, near_ref,
-               m_ref, l_ref, o_ref, state_ref, k_s, v_s, s_s, n_s, piece_s, stat_s):
+               m_ref, l_ref, o_ref, *refs, head):
+    packs = head >= RELAYED
+    k, v, sh, n = refs[packs:packs + 4]
     tp, par = sc_ref[0], sc_ref[1]
     nq = kvya_ref.shape[2] // FAR_DILATION * 2
 
     @pl.when(sc_ref[2] >= 1)
     def _():
-        for h in range(q_ref.shape[0]):
-            q, mi, li, oi, m, l, o, k, v, sh, n = (x.at[h] for x in (
-                q_ref, m_in, l_in, o_in, m_ref, l_ref, o_ref, k_s, v_s, s_s, n_s))
-            gather_kv(k, v, [x.at[h] for x in (kva_ref, kvb_ref, kvya_ref, kvyb_ref)], nq, tp, par)
-            near = (near_rows(0, nq), near_rows(2 * nq // TILE - 1, nq), near_ref[...], 0)
-            at = length(near[0])
-            items = []
-            for r4 in range(MIDDLE_DILATION):
-                rows = group_rows(r4, nq)
-                items.append((rows, rows, group_ref[...], at))
-                scored(items[-1], q, k, sh, n, True)
-                at += length(rows)
-            scored(near, q, k, sh, n, False)
-            for item in items:
-                rows = item[0]
-                old = take(mi, rows)
-                new = jnp.maximum(old, take(n, rows))
-                keep = jnp.exp2((old - new) * SCALE)
-                put(m, rows, new)
-                ol = weighed(item, v, sh, m, length(item[1]))
-                put(o, rows, take(oi, rows) * keep + ol[:, :HEAD])
-                put(l, rows, take(li, rows) * keep + ol[:, HEAD:])
-            ol = weighed(near, v, sh, m, length(near[1]))
-            put(o, near[0], take(o, near[0]) + ol[:, :HEAD])
-            put(l, near[0], take(l, near[0]) + ol[:, HEAD:])
-
-    for i in range(FAR_DILATION // 2):
-        rows = pair_rows(i, nq)
-        m, l, o = (take(x.at[RELAYED], rows) for x in (m_ref, l_ref, o_ref))
-        pack_rows(piece_s, stat_s, i, o / l, m, l)
-    pack_out(state_ref, piece_s, stat_s, 1 - par)
+        q, mi, li, oi, m, l, o = (x.at[head] for x in (q_ref, m_in, l_in, o_in, m_ref, l_ref, o_ref))
+        gather_kv(k, v, [x.at[head] for x in (kva_ref, kvb_ref, kvya_ref, kvyb_ref)], nq, tp, par)
+        near = (near_rows(0, nq), near_rows(2 * nq // TILE - 1, nq), near_ref[...], 0)
+        at = length(near[0])
+        items = []
+        for r4 in range(MIDDLE_DILATION):
+            rows = group_rows(r4, nq)
+            items.append((rows, rows, group_ref[...], at))
+            scored(items[-1], q, k, sh, n, True)
+            at += length(rows)
+        scored(near, q, k, sh, n, False)
+        for item in items:
+            rows = item[0]
+            old = take(mi, rows)
+            new = jnp.maximum(old, take(n, rows))
+            keep = jnp.exp2((old - new) * SCALE)
+            put(m, rows, new)
+            ol = weighed(item, v, sh, m, length(item[1]))
+            put(o, rows, take(oi, rows) * keep + ol[:, :HEAD])
+            put(l, rows, take(li, rows) * keep + ol[:, HEAD:])
+        ol = weighed(near, v, sh, m, length(near[1]))
+        put(o, near[0], take(o, near[0]) + ol[:, :HEAD])
+        put(l, near[0], take(l, near[0]) + ol[:, HEAD:])
+
+    if packs:
+        state_ref, piece_s, stat_s = refs[0], *refs[5:]
+        for i in range(FAR_DILATION // 2):
+            rows = pair_rows(i, nq)
+            m, l, o = (take(x.at[head], rows) for x in (m_ref, l_ref, o_ref))
+            pack_rows(piece_s, stat_s, i, o / l, m, l)
+        pack_out(state_ref, piece_s, stat_s, 1 - par)
 
 
 def two_kernel(sc_ref, q_ref, m_ref, l_ref, o_ref, kvo_ref, kvy_ref, pair_ref,
@@ -547,10 +549,15 @@
         local_kernel, scalars, [q_a, q_b, q_y0, q_y1, kv_a, kv_b, kv_ya, kv_yb, group0, near0, upper],
         [shape((heads, group, HEAD), BF16), state, state, state],
         kv_scratch + [pltpu.VMEM((heads, 3 * group, 2 * HEAD), F32)], 3 * 10 ** 9)
+    one_scratch = [pltpu.VMEM((group, HEAD), BF16)] * 2 + [
+        pltpu.VMEM((2 * group, 2 * HEAD), F32), pltpu.VMEM((group, HEAD), F32)]
+    known = [kv1_a, kv1_b, kv1_ya, kv1_yb, group1, near1]
     m, l, o, state_y = call(
-        one_kernel, scalars, [q, m, l, o, kv1_a, kv1_b, kv1_ya, kv1_yb, group1, near1], [state, state, state, packed],
-        kv_scratch + [pltpu.VMEM((heads, 2 * group, 2 * HEAD), F32), pltpu.VMEM((heads, group, HEAD), F32)]
-        + packing, 10 ** 9, {2: 0, 3: 1, 4: 2})
+        functools.partial(one_kernel, head=1), scalars, [q, m, l, o, *known], [state, state, state, packed],
+        one_scratch + packing, 10 ** 9, {2: 0, 3: 1, 4: 2})
+    m, l, o = call(
+        functools.partial(one_kernel, head=0), scalars, [q, m, l, o, *known], [state, state, state],
+        one_scratch, 10 ** 9, {2: 0, 3: 1, 4: 2})
     state_y = swap(state_y, "sp")
     mixed = shape((rows, HEAD), BF16)
     keep, send = call(

time: 76.6 us -> 75.7 us (0.988)
  starting transfers between devices: 41 us -> 39.9 us
    ppermute x7, starting transfers between devices: 29 us -> 28.1 us  [onward(): return lax.ppermute(x, 'sp', [(i, i + 2) for i in range(n - 2)])]
    pallas_call x9 -> x10, Pallas kernels: 17.5 us -> 18.2 us  [call(): pl.pallas_call(kernel, in_specs=[pl.BlockSpec(memory_space=pltpu.SMEM)] +...]
  transfers between devices with their start and end apart: 19 -> 19, of which waited for: 7 -> 6; matrix products, arithmetic and copies ran while one was open for 0% -> 0% of each run, Pallas kernels for 23% -> 24%
where the time goes in v6:
time: 75.7 us; the launch traced here: 74.7 us
  starting transfers between devices  39.9 us (53%)
  Pallas kernels  21 us (28%)
  waiting for transfers between devices  13.1 us (17%)
    ppermute x7, starting transfers between devices, onward(): return lax.ppermute(x, 'sp', [(i, i + 2) for i in range(n - 2)])  28.1 us
    pallas_call x10, Pallas kernels, call(): pl.pallas_call(kernel, in_specs=[pl.BlockSpec(memory_space=pltpu.SMEM)] +...  18.2 us
    ppermute x10, starting transfers between devices, swap(): lax.ppermute(x, axis, [(i, i ^ 1) for i in range(lax.axis_size(axis))])  8.17 us
    ppermute x10, waiting for transfers between devices, swap(): lax.ppermute(x, axis, [(i, i ^ 1) for i in range(lax.axis_size(axis))])  7.95 us
    ppermute x7, waiting for transfers between devices, onward(): return lax.ppermute(x, 'sp', [(i, i + 2) for i in range(n - 2)])  3.26 us
    pallas_call x1, Pallas kernels, out_project(): pl.pallas_call(out_kernel, grid=(steps,), in_specs=[pl.BlockSpec(memory_s...  2.79 us
    ppermute x1, starting transfers between devices, body(): lax.ppermute(piece_diag, 'sp', [(i, (i ^ 1) + 2) for i in range(n - 2)])  2.32 us
    ppermute x1, waiting for transfers between devices, body(): lax.ppermute(piece_diag, 'sp', [(i, (i ^ 1) + 2) for i in range(n - 2)])  1.84 us
  transfers between devices with their start and end apart: 19, of which 6 were waited for; matrix products, arithmetic and copies ran while one was open for 0% of the time, Pallas kernels for 24%

profile of v6, /device:TPU:0, one launch (start us, length us, event | category | flops | bytes accessed | tf_op | source)
XLA Modules:
  0.0 74.7 jit_solution(2369852783774000729)
XLA Ops:
  0.0 0.5 collective-permute-start
  0.5 0.1 maximum_bitcast_fusion.inv_ref
  0.6 0.1 pad_add_fusion.sc_ref
  0.7 3.7 %shard_map.109 = (bf16[2,2,256,128]{3,2,1,0:T(8,128)(2,1)S(1)}, bf16[256,2048]{1,0:T(8,128)(2,1)S(1)}, bf16[2,2048,256]{2,1,0:T(8,128)(2,1)S(1)}, f32[2,256,128]{2,1,0:T(8,128)S(1)}, f32[2,256,128]{2,1,0:T(8,128)S(1)}) custom-call(s32[4]{0:T(128)S(1)} %pad_add_fusion.sc_ref, bf16[256,2048]{1,0:T(8,128)(2,1)} %x_hbm.1, bf16[2048,512]{1,0:T(8,128)(2,1)} %wk_ref.1, ...), custom_call_target="tpu_custom_call" | custom-call | flops 536870912 | tf_op jit(solution)/shard_map/pallas_call | solution.py:130
  4.4 4.5 %collective-permute-start.5 = (bf16[2,2,256,128]{3,2,1,0:T(8,128)(2,1)S(1)}, bf16[2,2,256,128]{3,2,1,0:T(8,128)(2,1)S(1)}, u32[]{:S(2)}, u32[]{:S(2)}) collective-permute-start(bf16[2,2,256,128]{3,2,1,0:T(8,128)(2,1)S(1)} %get-tuple-element.43.kva_ref), channel_id=1, source_target_pairs={{0,4},{2,6},{4,8},{6,10},{8,12},{10,14},{1,5},{3,7},{5,9},{7,11},{... | collective-permute-start | bytes 786440 | tf_op jit(solution)/shard_map/ppermute | solution.py:484
  8.9 0.0 collective-permute-done.xp_ref.x_ref
  8.9 0.0 copy-done
  8.9 0.0 copy-done.1
  8.9 0.0 copy-start.2
  8.9 2.3 %shard_map.111 = (bf16[2,2,256,128]{3,2,1,0:T(8,128)(2,1)S(1)}, bf16[2,2,256,128]{3,2,1,0:T(8,128)(2,1)S(1)}) custom-call(s32[4]{0:T(128)S(1)} %pad_add_fusion.sc_ref, bf16[256,2048]{1,0:T(8,128)(2,1)S(1)} %get-tuple-element.36.xo_ref, bf16[256,2048]{1,0:T(8,128)(2,1)S(1)} %collective-permute-done.xp_ref.x_ref, bf16[2048,512]{1,0:T(8,128)(2,1)S(1)} %copy-done, ...), custom_call_target="tpu_custom_call" | custom-call | flops 1073741824 | tf_op jit(solution)/shard_map/pallas_call | solution.py:130
  11.2 3.5 %collective-permute-start.6 = (bf16[2,2,256,128]{3,2,1,0:T(8,128)(2,1)S(1)}, bf16[2,2,256,128]{3,2,1,0:T(8,128)(2,1)S(1)}, u32[]{:S(2)}, u32[]{:S(2)}) collective-permute-start(bf16[2,2,256,128]{3,2,1,0:T(8,128)(2,1)S(1)} %get-tuple-element.47.kvb_ref), channel_id=1, source_target_pairs={{0,4},{2,6},{4,8},{6,10},{8,12},{10,14},{1,5},{3,7},{5,9},{7,11},{... | collective-permute-start | bytes 786440 | tf_op jit(solution)/shard_map/ppermute | solution.py:484
  14.7 0.0 copy-done.2
  14.7 2.5 %shard_map.110 = (bf16[2,256,128]{2,1,0:T(8,128)(2,1)S(1)}, bf16[2,256,128]{2,1,0:T(8,128)(2,1)S(1)}, bf16[512,128]{1,0:T(8,128)(2,1)S(1)}, bf16[512,128]{1,0:T(8,128)(2,1)S(1)}, bf16[1,2,256,128]{3,2,1,0:T(8,128)(2,1)S(1)}) custom-call(s32[4]{0:T(128)S(1)} %pad_add_fusion.sc_ref, bf16[256,2048]{1,0:T(8,128)(2,1)S(1)} %get-tuple-element.36.xo_ref, ...), custom_call_target="tpu_custom_call" | custom-call | flops 1073741824 | tf_op jit(solution)/shard_map/pallas_call | solution.py:130
  17.3 1.6 %collective-permute-start.2 = (bf16[512,128]{1,0:T(8,128)(2,1)S(1)}, bf16[512,128]{1,0:T(8,128)(2,1)S(1)}, u32[]{:S(2)}, u32[]{:S(2)}) collective-permute-start(bf16[512,128]{1,0:T(8,128)(2,1)S(1)} %get-tuple-element.42), channel_id=1, source_target_pairs={{0,2},{2,0},{4,6},{6,4},{8,10},{10,8},{12,14},{14,12},{1,3},{3,1},... | collective-permute-start | bytes 393224 | tf_op jit(solution)/shard_map/ppermute | solution.py:479
  18.9 0.5 collective-permute-start.3
  19.4 1.5 %shard_map.112 = bf16[2,2,256,128]{3,2,1,0:T(8,128)(2,1)S(1)} custom-call(s32[4]{0:T(128)S(1)} %pad_add_fusion.sc_ref, bf16[256,2048]{1,0:T(8,128)(2,1)S(1)} %collective-permute-done.xp_ref.x_ref, bf16[2048,512]{1,0:T(8,128)(2,1)S(1)} %copy-done, bf16[2048,512]{1,0:T(8,128)(2,1)S(1)} %copy-done.1, f32[2,256,128]{2,1,0:T(8,128)S(1)} %get-tuple-element.37.cos_ref, ...), custom_call_target="tpu_custom_call" | custom-call | flops 536870912 | tf_op jit(solution)/shard_map/pallas_call | solution.py:130
  20.9 1.6 %collective-permute-start.4 = (bf16[2,2,256,128]{3,2,1,0:T(8,128)(2,1)S(1)}, bf16[2,2,256,128]{3,2,1,0:T(8,128)(2,1)S(1)}, u32[]{:S(2)}, u32[]{:S(2)}) collective-permute-start(bf16[2,2,256,128]{3,2,1,0:T(8,128)(2,1)S(1)} %shard_map.112), channel_id=1, source_target_pairs={{0,2},{2,0},{4,6},{6,4},{8,10},{10,8},{12,14},{14,12},{1,3},{3,1},... | collective-permute-start | bytes 786440 | tf_op jit(solution)/shard_map/ppermute | solution.py:479
  22.5 0.0 collective-permute-done.5.kva_ref
  22.5 0.6 collective-permute-start.1
  23.0 0.7 collective-permute-done.2.qy1_ref
  23.7 1.3 %collective-permute-start.15 = (bf16[2,512,128]{2,1,0:T(8,128)(2,1)S(1)}, bf16[2,512,128]{2,1,0:T(8,128)(2,1)S(1)}, u32[]{:S(2)}, u32[]{:S(2)}) collective-permute-start(bf16[2,512,128]{2,1,0:T(8,128)(2,1)S(1)} %pad_maximum_fusion.2), channel_id=1, source_target_pairs={{4,0},{6,2},{8,4},{10,6},{12,8},{14,10},{5,1},{7,3},{9,5},{11,7},{... | collective-permute-start | bytes 786440 | tf_op jit(solution)/shard_map/ppermute | solution.py:532
  25.0 0.0 collective-permute-done.6.kvb_ref
  25.1 4.6 %collective-permute-start.9 = (bf16[2,2,256,128]{3,2,1,0:T(8,128)(2,1)S(1)}, bf16[2,2,256,128]{3,2,1,0:T(8,128)(2,1)S(1)}, u32[]{:S(2)}, u32[]{:S(2)}) collective-permute-start(bf16[2,2,256,128]{3,2,1,0:T(8,128)(2,1)S(1)} %pad_maximum_fusion), channel_id=1, source_target_pairs={{0,4},{2,6},{4,8},{6,10},{8,12},{10,14},{1,5},{3,7},{5,9},{7,11},{... | collective-permute-start | bytes 786440 | tf_op jit(solution)/shard_map/ppermute | solution.py:484
  29.7 0.0 collective-permute-done.3.kvya_ref
  29.7 3.5 %collective-permute-start.7 = (bf16[2,2,256,128]{3,2,1,0:T(8,128)(2,1)S(1)}, bf16[2,2,256,128]{3,2,1,0:T(8,128)(2,1)S(1)}, u32[]{:S(2)}, u32[]{:S(2)}) collective-permute-start(bf16[2,2,256,128]{3,2,1,0:T(8,128)(2,1)S(1)} %collective-permute-done.3.kvya_ref), channel_id=1, source_target_pairs={{0,4},{2,6},{4,8},{6,10},{8,12},{10,14},{1,5},{3,7},{5,9},{7,11},{... | collective-permute-start | bytes 786440 | tf_op jit(solution)/shard_map/ppermute | solution.py:484
  33.2 1.8 %collective-permute-done.4.kvyb_ref = bf16[2,2,256,128]{3,2,1,0:T(8,128)(2,1)S(1)} collective-permute-done((bf16[2,2,256,128]{3,2,1,0:T(8,128)(2,1)S(1)}, bf16[2,2,256,128]{3,2,1,0:T(8,128)(2,1)S(1)}, u32[]{:S(2)}, u32[]{:S(2)}) %collective-permute-start.4) | collective-permute-done | bytes 262176 | tf_op jit(solution)/shard_map/ppermute | solution.py:479
  34.9 3.5 %collective-permute-start.8 = (bf16[2,2,256,128]{3,2,1,0:T(8,128)(2,1)S(1)}, bf16[2,2,256,128]{3,2,1,0:T(8,128)(2,1)S(1)}, u32[]{:S(2)}, u32[]{:S(2)}) collective-permute-start(bf16[2,2,256,128]{3,2,1,0:T(8,128)(2,1)S(1)} %collective-permute-done.4.kvyb_ref), channel_id=1, source_target_pairs={{0,4},{2,6},{4,8},{6,10},{8,12},{10,14},{1,5},{3,7},{5,9},{7,11},{... | collective-permute-start | bytes 786440 | tf_op jit(solution)/shard_map/ppermute | solution.py:484
  38.4 0.0 collective-permute-done.1.qy0_ref
  38.4 0.0 copy-done.7
  38.4 0.0 copy-done.8
  38.4 0.0 copy-done.9
  38.5 0.0 copy-start.4
  38.5 0.0 copy-start.5
  38.5 3.0 %shard_map.113 = (bf16[2,1024,128]{2,1,0:T(8,128)(2,1)S(1)}, f32[2,1024,128]{2,1,0:T(8,128)S(1)}, f32[2,1024,128]{2,1,0:T(8,128)S(1)}, f32[2,1024,128]{2,1,0:T(8,128)S(1)}) custom-call(s32[4]{0:T(128)S(1)} %pad_add_fusion.sc_ref, bf16[2,256,128]{2,1,0:T(8,128)(2,1)S(1)} %get-tuple-element.39.qa_ref, bf16[2,256,128]{2,1,0:T(8,128)(2,1)S(1)} %get-tuple-element.40.qb_ref, ...), custom_call_target="tpu_custom_call" | custom-call | flops 3000000000 | tf_op jit(solution)/shard_map/pallas_call | solution.py:130
  41.5 3.2 %collective-permute-done.8.kvyb_ref = bf16[2,2,256,128]{3,2,1,0:T(8,128)(2,1)S(1)} collective-permute-done((bf16[2,2,256,128]{3,2,1,0:T(8,128)(2,1)S(1)}, bf16[2,2,256,128]{3,2,1,0:T(8,128)(2,1)S(1)}, u32[]{:S(2)}, u32[]{:S(2)}) %collective-permute-start.8) | collective-permute-done | bytes 262176 | tf_op jit(solution)/shard_map/ppermute | solution.py:484
  44.8 0.0 collective-permute-done.7.kvya_ref
  44.8 4.4 %collective-permute-start.10 = (bf16[2,2,256,128]{3,2,1,0:T(8,128)(2,1)S(1)}, bf16[2,2,256,128]{3,2,1,0:T(8,128)(2,1)S(1)}, u32[]{:S(2)}, u32[]{:S(2)}) collective-permute-start(bf16[2,2,256,128]{3,2,1,0:T(8,128)(2,1)S(1)} %pad_maximum_fusion.1), channel_id=1, source_target_pairs={{0,4},{2,6},{4,8},{6,10},{8,12},{10,14},{1,5},{3,7},{5,9},{7,11},{... | collective-permute-start | bytes 786440 | tf_op jit(solution)/shard_map/ppermute | solution.py:484
  49.2 0.0 copy-done.4
  49.3 0.0 copy-start.6
  49.3 0.7 shard_map.114
  50.0 1.6 %collective-permute-start.14 = (bf16[560,128]{1,0:T(8,128)(2,1)S(1)}, bf16[560,128]{1,0:T(8,128)(2,1)S(1)}, u32[]{:S(2)}, u32[]{:S(2)}) collective-permute-start(bf16[560,128]{1,0:T(8,128)(2,1)S(1)} %get-tuple-element.61), channel_id=1, source_target_pairs={{0,2},{2,0},{4,6},{6,4},{8,10},{10,8},{12,14},{14,12},{1,3},{3,1},... | collective-permute-start | bytes 430088 | tf_op jit(solution)/shard_map/ppermute | solution.py:479
  51.6 0.0 collective-permute-done.15.qn_ref
  51.6 0.0 copy-done.6
  51.6 1.2 %shard_map.117 = (bf16[560,128]{1,0:T(8,128)(2,1)S(1)}, bf16[560,128]{1,0:T(8,128)(2,1)S(1)}) custom-call(s32[4]{0:T(128)S(1)} %pad_add_fusion.sc_ref, bf16[2,512,128]{2,1,0:T(8,128)(2,1)S(1)} %collective-permute-done.15.qn_ref, bf16[2,2,256,128]{3,2,1,0:T(8,128)(2,1)S(1)} %collective-permute-done.5.kva_ref, ...), custom_call_target="tpu_custom_call" | custom-call | flops 1000000000 | tf_op jit(solution)/shard_map/pallas_call | solution.py:130
  52.8 4.3 %collective-permute-start.16 = (bf16[560,128]{1,0:T(8,128)(2,1)S(1)}, bf16[560,128]{1,0:T(8,128)(2,1)S(1)}, u32[]{:S(2)}, u32[]{:S(2)}) collective-permute-start(bf16[560,128]{1,0:T(8,128)(2,1)S(1)} %get-tuple-element.63), channel_id=1, source_target_pairs={{0,4},{2,6},{4,8},{6,10},{8,12},{10,14},{1,5},{3,7},{5,9},{7,11},{... | collective-permute-start | bytes 430088 | tf_op jit(solution)/shard_map/ppermute | solution.py:484
  57.1 2.3 %collective-permute-start.17 = (bf16[560,128]{1,0:T(8,128)(2,1)S(1)}, bf16[560,128]{1,0:T(8,128)(2,1)S(1)}, u32[]{:S(2)}, u32[]{:S(2)}) collective-permute-start(bf16[560,128]{1,0:T(8,128)(2,1)S(1)} %get-tuple-element.64), channel_id=1, source_target_pairs={{0,6},{2,4},{4,10},{6,8},{8,14},{10,12},{1,7},{3,5},{5,11},{7,9},{... | collective-permute-start | bytes 430088 | tf_op jit(solution)/shard_map/ppermute | solution.py:544
  59.4 0.7 shard_map.115
  60.2 0.0 collective-permute-done.14.state_ref
  60.2 0.0 collective-permute-done.16.own_ref
  60.2 1.8 %collective-permute-done.17.diag_ref = bf16[560,128]{1,0:T(8,128)(2,1)S(1)} collective-permute-done((bf16[560,128]{1,0:T(8,128)(2,1)S(1)}, bf16[560,128]{1,0:T(8,128)(2,1)S(1)}, u32[]{:S(2)}, u32[]{:S(2)}) %collective-permute-start.17) | collective-permute-done | bytes 143392 | tf_op jit(solution)/shard_map/ppermute | solution.py:544
  62.1 1.6 %shard_map.118.own_ref = bf16[2,512,128]{2,1,0:T(8,128)(2,1)S(1)} custom-call(s32[4]{0:T(128)S(1)} %pad_add_fusion.sc_ref, f32[2,1024,128]{2,1,0:T(8,128)S(1)} %get-tuple-element.56.m_ref, f32[2,1024,128]{2,1,0:T(8,128)S(1)} %get-tuple-element.57.l_ref, f32[2,1024,128]{2,1,0:T(8,128)S(1)} %get-tuple-element.58.o_ref, ...), custom_call_target="tpu_custom_call" | custom-call | flops 1000000000 | tf_op jit(solution)/shard_map/pallas_call | solution.py:130
  63.6 0.0 copy-start.3
  63.7 0.1 collective-permute-start.18
  63.7 0.0 collective-permute-done.9.kvo_ref
  63.8 0.0 collective-permute-done.10.kvy_ref
  63.8 0.9 %shard_map.116 = (bf16[512,128]{1,0:T(8,128)(2,1)S(1)}, bf16[512,128]{1,0:T(8,128)(2,1)S(1)}) custom-call(s32[4]{0:T(128)S(1)} %pad_add_fusion.sc_ref, bf16[2,1024,128]{2,1,0:T(8,128)(2,1)S(1)} %get-tuple-element.49.q_ref, f32[2,1024,128]{2,1,0:T(8,128)S(1)} %get-tuple-element.56.m_ref, f32[2,1024,128]{2,1,0:T(8,128)S(1)} %get-tuple-element.57.l_ref, ...), custom_call_target="tpu_custom_call" | custom-call | flops 1000000000 | tf_op jit(solution)/shard_map/pallas_call | solution.py:130
  64.6 1.6 %collective-permute-start.11 = (bf16[512,128]{1,0:T(8,128)(2,1)S(1)}, bf16[512,128]{1,0:T(8,128)(2,1)S(1)}, u32[]{:S(2)}, u32[]{:S(2)}) collective-permute-start(bf16[512,128]{1,0:T(8,128)(2,1)S(1)} %get-tuple-element.60), channel_id=1, source_target_pairs={{0,2},{2,0},{4,6},{6,4},{8,10},{10,8},{12,14},{14,12},{1,3},{3,1},... | collective-permute-start | bytes 393224 | tf_op jit(solution)/shard_map/ppermute | solution.py:479
  66.2 0.2 collective-permute-start.12
  66.4 4.2 %collective-permute-done.11.b_ref = bf16[512,128]{1,0:T(8,128)(2,1)S(1)} collective-permute-done((bf16[512,128]{1,0:T(8,128)(2,1)S(1)}, bf16[512,128]{1,0:T(8,128)(2,1)S(1)}, u32[]{:S(2)}, u32[]{:S(2)}) %collective-permute-start.11) | collective-permute-done | bytes 131104 | tf_op jit(solution)/shard_map/ppermute | solution.py:479
  70.6 0.0 collective-permute-start.13
  70.6 0.0 collective-permute-done.12.c_ref
  70.6 0.0 collective-permute-done.18.tp_ref
  70.6 1.3 %collective-permute-done.13.d_ref = bf16[512,128]{1,0:T(8,128)(2,1)S(1)} collective-permute-done((bf16[512,128]{1,0:T(8,128)(2,1)S(1)}, bf16[512,128]{1,0:T(8,128)(2,1)S(1)}, u32[]{:S(2)}, u32[]{:S(2)}) %collective-permute-start.13) | collective-permute-done | bytes 131104 | tf_op jit(solution)/shard_map/ppermute | solution.py:479
  71.9 2.8 %out_project.1 = bf16[512,1024]{1,0:T(8,128)(2,1)} custom-call(s32[4]{0:T(128)S(1)} %pad_add_fusion.sc_ref, bf16[512,128]{1,0:T(8,128)(2,1)S(1)} %get-tuple-element.59.a_ref, bf16[512,128]{1,0:T(8,128)(2,1)S(1)} %collective-permute-done.11.b_ref, bf16[512,128]{1,0:T(8,128)(2,1)S(1)} %collective-permute-done.12.c_ref, ...), custom_call_target="tpu_custom_call" | custom-call | flops 1073741824 | tf_op jit(solution)/shard_map/out_project/pallas_call | solution.py:466
  (15 shorter events, 0.1 us)
Async XLA Ops:
  0.0 8.9 %collective-permute-start = (bf16[256,2048]{1,0:T(8,128)(2,1)}, bf16[256,2048]{1,0:T(8,128)(2,1)S(1)}, u32[]{:S(2)}, u32[]{:S(2)}) collective-permute-start(bf16[256,2048]{1,0:T(8,128)(2,1)} %x_hbm.1), channel_id=1, source_target_pairs={{0,1},{1,0},{2,3},{3,2},{4,5},{5,4},{6,7},{7,6},{8,9},{9,8},{10,11... | collective-permute-start | bytes 3145736 | tf_op jit(solution)/shard_map/ppermute | solution.py:479
  0.7 8.3 %copy-start = (bf16[2048,512]{1,0:T(8,128)(2,1)S(1)}, bf16[2048,512]{1,0:T(8,128)(2,1)}, u32[]{:S(2)}) copy-start(bf16[2048,512]{1,0:T(8,128)(2,1)} %wk_ref.1) | copy-start | bytes 6291460
  0.7 8.3 %copy-start.1 = (bf16[2048,512]{1,0:T(8,128)(2,1)S(1)}, bf16[2048,512]{1,0:T(8,128)(2,1)}, u32[]{:S(2)}) copy-start(bf16[2048,512]{1,0:T(8,128)(2,1)} %wv_ref.1) | copy-start | bytes 6291460
  4.4 18.1 %collective-permute-start.5 = (bf16[2,2,256,128]{3,2,1,0:T(8,128)(2,1)S(1)}, bf16[2,2,256,128]{3,2,1,0:T(8,128)(2,1)S(1)}, u32[]{:S(2)}, u32[]{:S(2)}) collective-permute-start(bf16[2,2,256,128]{3,2,1,0:T(8,128)(2,1)S(1)} %get-tuple-element.43.kva_ref), channel_id=1, source_target_pairs={{0,4},{2,6},{4,8},{6,10},{8,12},{10,14},{1,5},{3,7},{5,9},{7,11},{... | collective-permute-start | bytes 786440 | tf_op jit(solution)/shard_map/ppermute | solution.py:484
  8.9 5.8 %copy-start.2 = (bf16[2048,512]{1,0:T(8,128)(2,1)S(1)}, bf16[2048,512]{1,0:T(8,128)(2,1)}, u32[]{:S(2)}) copy-start(bf16[2048,512]{1,0:T(8,128)(2,1)} %w_ref.2) | copy-start | bytes 6291460
  11.2 13.8 %collective-permute-start.6 = (bf16[2,2,256,128]{3,2,1,0:T(8,128)(2,1)S(1)}, bf16[2,2,256,128]{3,2,1,0:T(8,128)(2,1)S(1)}, u32[]{:S(2)}, u32[]{:S(2)}) collective-permute-start(bf16[2,2,256,128]{3,2,1,0:T(8,128)(2,1)S(1)} %get-tuple-element.47.kvb_ref), channel_id=1, source_target_pairs={{0,4},{2,6},{4,8},{6,10},{8,12},{10,14},{1,5},{3,7},{5,9},{7,11},{... | collective-permute-start | bytes 786440 | tf_op jit(solution)/shard_map/ppermute | solution.py:484
  17.3 6.4 %collective-permute-start.2 = (bf16[512,128]{1,0:T(8,128)(2,1)S(1)}, bf16[512,128]{1,0:T(8,128)(2,1)S(1)}, u32[]{:S(2)}, u32[]{:S(2)}) collective-permute-start(bf16[512,128]{1,0:T(8,128)(2,1)S(1)} %get-tuple-element.42), channel_id=1, source_target_pairs={{0,2},{2,0},{4,6},{6,4},{8,10},{10,8},{12,14},{14,12},{1,3},{3,1},... | collective-permute-start | bytes 393224 | tf_op jit(solution)/shard_map/ppermute | solution.py:479
  18.9 19.6 %copy-start.7 = (f32[256,256]{1,0:T(8,128)S(1)}, f32[256,256]{1,0:T(8,128)}, u32[]{:S(2)}) copy-start(f32[256,256]{1,0:T(8,128)} %constant.50.clone.group_ref) | copy-start | bytes 786436
  18.9 19.6 %copy-start.8 = (f32[256,256]{1,0:T(8,128)S(1)}, f32[256,256]{1,0:T(8,128)}, u32[]{:S(2)}) copy-start(f32[256,256]{1,0:T(8,128)} %constant.51.clone.near0_ref) | copy-start | bytes 786436
  18.9 19.6 %copy-start.9 = (f32[128,256]{1,0:T(8,128)S(1)}, f32[128,256]{1,0:T(8,128)}, u32[]{:S(2)}) copy-start(f32[128,256]{1,0:T(8,128)} %constant.52.clone.near1_ref) | copy-start | bytes 393220
  18.9 10.8 %collective-permute-start.3 = (bf16[2,2,256,128]{3,2,1,0:T(8,128)(2,1)S(1)}, bf16[2,2,256,128]{3,2,1,0:T(8,128)(2,1)S(1)}, u32[]{:S(2)}, u32[]{:S(2)}) collective-permute-start(bf16[2,2,256,128]{3,2,1,0:T(8,128)(2,1)S(1)} %get-tuple-element.48), channel_id=1, source_target_pairs={{0,2},{2,0},{4,6},{6,4},{8,10},{10,8},{12,14},{14,12},{1,3},{3,1},... | collective-permute-start | bytes 786440 | tf_op jit(solution)/shard_map/ppermute | solution.py:479
  20.9 14.1 %collective-permute-start.4 = (bf16[2,2,256,128]{3,2,1,0:T(8,128)(2,1)S(1)}, bf16[2,2,256,128]{3,2,1,0:T(8,128)(2,1)S(1)}, u32[]{:S(2)}, u32[]{:S(2)}) collective-permute-start(bf16[2,2,256,128]{3,2,1,0:T(8,128)(2,1)S(1)} %shard_map.112), channel_id=1, source_target_pairs={{0,2},{2,0},{4,6},{6,4},{8,10},{10,8},{12,14},{14,12},{1,3},{3,1},... | collective-permute-start | bytes 786440 | tf_op jit(solution)/shard_map/ppermute | solution.py:479
  22.5 15.9 %collective-permute-start.1 = (bf16[512,128]{1,0:T(8,128)(2,1)S(1)}, bf16[512,128]{1,0:T(8,128)(2,1)S(1)}, u32[]{:S(2)}, u32[]{:S(2)}) collective-permute-start(bf16[512,128]{1,0:T(8,128)(2,1)S(1)} %get-tuple-element.41), channel_id=1, source_target_pairs={{0,2},{2,0},{4,6},{6,4},{8,10},{10,8},{12,14},{14,12},{1,3},{3,1},... | collective-permute-start | bytes 393224 | tf_op jit(solution)/shard_map/ppermute | solution.py:479
  23.7 27.8 %collective-permute-start.15 = (bf16[2,512,128]{2,1,0:T(8,128)(2,1)S(1)}, bf16[2,512,128]{2,1,0:T(8,128)(2,1)S(1)}, u32[]{:S(2)}, u32[]{:S(2)}) collective-permute-start(bf16[2,512,128]{2,1,0:T(8,128)(2,1)S(1)} %pad_maximum_fusion.2), channel_id=1, source_target_pairs={{4,0},{6,2},{8,4},{10,6},{12,8},{14,10},{5,1},{7,3},{9,5},{11,7},{... | collective-permute-start | bytes 786440 | tf_op jit(solution)/shard_map/ppermute | solution.py:532
  25.1 38.6 %collective-permute-start.9 = (bf16[2,2,256,128]{3,2,1,0:T(8,128)(2,1)S(1)}, bf16[2,2,256,128]{3,2,1,0:T(8,128)(2,1)S(1)}, u32[]{:S(2)}, u32[]{:S(2)}) collective-permute-start(bf16[2,2,256,128]{3,2,1,0:T(8,128)(2,1)S(1)} %pad_maximum_fusion), channel_id=1, source_target_pairs={{0,4},{2,6},{4,8},{6,10},{8,12},{10,14},{1,5},{3,7},{5,9},{7,11},{... | collective-permute-start | bytes 786440 | tf_op jit(solution)/shard_map/ppermute | solution.py:484
  29.7 15.1 %collective-permute-start.7 = (bf16[2,2,256,128]{3,2,1,0:T(8,128)(2,1)S(1)}, bf16[2,2,256,128]{3,2,1,0:T(8,128)(2,1)S(1)}, u32[]{:S(2)}, u32[]{:S(2)}) collective-permute-start(bf16[2,2,256,128]{3,2,1,0:T(8,128)(2,1)S(1)} %collective-permute-done.3.kvya_ref), channel_id=1, source_target_pairs={{0,4},{2,6},{4,8},{6,10},{8,12},{10,14},{1,5},{3,7},{5,9},{7,11},{... | collective-permute-start | bytes 786440 | tf_op jit(solution)/shard_map/ppermute | solution.py:484
  34.9 9.8 %collective-permute-start.8 = (bf16[2,2,256,128]{3,2,1,0:T(8,128)(2,1)S(1)}, bf16[2,2,256,128]{3,2,1,0:T(8,128)(2,1)S(1)}, u32[]{:S(2)}, u32[]{:S(2)}) collective-permute-start(bf16[2,2,256,128]{3,2,1,0:T(8,128)(2,1)S(1)} %collective-permute-done.4.kvyb_ref), channel_id=1, source_target_pairs={{0,4},{2,6},{4,8},{6,10},{8,12},{10,14},{1,5},{3,7},{5,9},{7,11},{... | collective-permute-start | bytes 786440 | tf_op jit(solution)/shard_map/ppermute | solution.py:484
  38.5 10.8 %copy-start.4 = (f32[256,256]{1,0:T(8,128)S(1)}, f32[256,256]{1,0:T(8,128)}, u32[]{:S(2)}) copy-start(f32[256,256]{1,0:T(8,128)} %constant.53.clone.group_ref) | copy-start | bytes 786436
  38.5 10.8 %copy-start.5 = (f32[256,256]{1,0:T(8,128)S(1)}, f32[256,256]{1,0:T(8,128)}, u32[]{:S(2)}) copy-start(f32[256,256]{1,0:T(8,128)} %constant.54.clone.near_ref) | copy-start | bytes 786436
  44.8 18.9 %collective-permute-start.10 = (bf16[2,2,256,128]{3,2,1,0:T(8,128)(2,1)S(1)}, bf16[2,2,256,128]{3,2,1,0:T(8,128)(2,1)S(1)}, u32[]{:S(2)}, u32[]{:S(2)}) collective-permute-start(bf16[2,2,256,128]{3,2,1,0:T(8,128)(2,1)S(1)} %pad_maximum_fusion.1), channel_id=1, source_target_pairs={{0,4},{2,6},{4,8},{6,10},{8,12},{10,14},{1,5},{3,7},{5,9},{7,11},{... | collective-permute-start | bytes 786440 | tf_op jit(solution)/shard_map/ppermute | solution.py:484
  49.3 2.3 %copy-start.6 = (f32[128,128]{1,0:T(8,128)S(1)}, f32[128,128]{1,0:T(8,128)}, u32[]{:S(2)}) copy-start(f32[128,128]{1,0:T(8,128)} %constant.49.clone.pair_ref) | copy-start | bytes 196612
  50.0 10.2 %collective-permute-start.14 = (bf16[560,128]{1,0:T(8,128)(2,1)S(1)}, bf16[560,128]{1,0:T(8,128)(2,1)S(1)}, u32[]{:S(2)}, u32[]{:S(2)}) collective-permute-start(bf16[560,128]{1,0:T(8,128)(2,1)S(1)} %get-tuple-element.61), channel_id=1, source_target_pairs={{0,2},{2,0},{4,6},{6,4},{8,10},{10,8},{12,14},{14,12},{1,3},{3,1},... | collective-permute-start | bytes 430088 | tf_op jit(solution)/shard_map/ppermute | solution.py:479
  52.8 7.4 %collective-permute-start.16 = (bf16[560,128]{1,0:T(8,128)(2,1)S(1)}, bf16[560,128]{1,0:T(8,128)(2,1)S(1)}, u32[]{:S(2)}, u32[]{:S(2)}) collective-permute-start(bf16[560,128]{1,0:T(8,128)(2,1)S(1)} %get-tuple-element.63), channel_id=1, source_target_pairs={{0,4},{2,6},{4,8},{6,10},{8,12},{10,14},{1,5},{3,7},{5,9},{7,11},{... | collective-permute-start | bytes 430088 | tf_op jit(solution)/shard_map/ppermute | solution.py:484
  57.1 4.9 %collective-permute-start.17 = (bf16[560,128]{1,0:T(8,128)(2,1)S(1)}, bf16[560,128]{1,0:T(8,128)(2,1)S(1)}, u32[]{:S(2)}, u32[]{:S(2)}) collective-permute-start(bf16[560,128]{1,0:T(8,128)(2,1)S(1)} %get-tuple-element.64), channel_id=1, source_target_pairs={{0,6},{2,4},{4,10},{6,8},{8,14},{10,12},{1,7},{3,5},{5,11},{7,9},{... | collective-permute-start | bytes 430088 | tf_op jit(solution)/shard_map/ppermute | solution.py:544
  63.6 8.3 %copy-start.3 = (bf16[1024,1024]{1,0:T(8,128)(2,1)S(1)}, bf16[1024,1024]{1,0:T(8,128)(2,1)}, u32[]{:S(2)}) copy-start(bf16[1024,1024]{1,0:T(8,128)(2,1)} %w_ref.3) | copy-start | bytes 6291460
  63.7 6.9 %collective-permute-start.18 = (bf16[2,512,128]{2,1,0:T(8,128)(2,1)S(1)}, bf16[2,512,128]{2,1,0:T(8,128)(2,1)S(1)}, u32[]{:S(2)}, u32[]{:S(2)}) collective-permute-start(bf16[2,512,128]{2,1,0:T(8,128)(2,1)S(1)} %shard_map.118.own_ref), channel_id=1, source_target_pairs={{0,1},{1,0},{2,3},{3,2},{4,5},{5,4},{6,7},{7,6},{8,9},{9,8},{10,11... | collective-permute-start | bytes 786440 | tf_op jit(solution)/shard_map/ppermute | solution.py:479
  64.6 5.9 %collective-permute-start.11 = (bf16[512,128]{1,0:T(8,128)(2,1)S(1)}, bf16[512,128]{1,0:T(8,128)(2,1)S(1)}, u32[]{:S(2)}, u32[]{:S(2)}) collective-permute-start(bf16[512,128]{1,0:T(8,128)(2,1)S(1)} %get-tuple-element.60), channel_id=1, source_target_pairs={{0,2},{2,0},{4,6},{6,4},{8,10},{10,8},{12,14},{14,12},{1,3},{3,1},... | collective-permute-start | bytes 393224 | tf_op jit(solution)/shard_map/ppermute | solution.py:479
  66.2 4.4 %collective-permute-start.12 = (bf16[512,128]{1,0:T(8,128)(2,1)S(1)}, bf16[512,128]{1,0:T(8,128)(2,1)S(1)}, u32[]{:S(2)}, u32[]{:S(2)}) collective-permute-start(bf16[512,128]{1,0:T(8,128)(2,1)S(1)} %get-tuple-element.59.a_ref), channel_id=1, source_target_pairs={{0,1},{1,0},{2,3},{3,2},{4,5},{5,4},{6,7},{7,6},{8,9},{9,8},{10,11... | collective-permute-start | bytes 393224 | tf_op jit(solution)/shard_map/ppermute | solution.py:479
  70.6 1.3 %collective-permute-start.13 = (bf16[512,128]{1,0:T(8,128)(2,1)S(1)}, bf16[512,128]{1,0:T(8,128)(2,1)S(1)}, u32[]{:S(2)}, u32[]{:S(2)}) collective-permute-start(bf16[512,128]{1,0:T(8,128)(2,1)S(1)} %collective-permute-done.11.b_ref), channel_id=1, source_target_pairs={{0,1},{1,0},{2,3},{3,2},{4,5},{5,4},{6,7},{7,6},{8,9},{9,8},{10,11... | collective-permute-start | bytes 393224 | tf_op jit(solution)/shard_map/ppermute | solution.py:479
